TPU v7x, 512 devices: a whole 4x4x16 slice. The times are simulated.
512 devices in a mesh: sp: 16 (over z), fs: 4 (over y), tp: 8 (over x, core).
Axes of the slice: x: 4, y: 4, z: 16, core: 2. Of those that a mesh axis runs over, the one named last changes fastest.
Arguments:
- tokens: bfloat16 [8, 8192, 2048], P('fs', ('sp', 'tp')), may hold values from -6 to 6
- norm_gain: float32 [2048], replicated, may hold values from 0.1 to 1.9
- w_pool_in: bfloat16 [2048, 1024], P('fs', 'tp'), may hold values from -0.125 to 0.125
- pool_mix: bfloat16 [8, 128, 128], replicated, may hold values from -0.5 to 0.5
- pool_scale: float32 [1024], replicated, may hold values from 0.1 to 1.9
- w_query: bfloat16 [2048, 1024], P('fs', 'tp'), may hold values from -0.13258252 to 0.13258252
- w_key: bfloat16 [2048, 1024], P('fs', 'tp'), may hold values from -0.508233 to 0.508233
- w_value: bfloat16 [2048, 1024], P('fs', 'tp'), may hold values from -0.125 to 0.125
- gate_cache: float32 [8, 8, 8192], P('fs', 'tp'), may hold values from -1026 to 0, as said below
- w_out_pool: bfloat16 [1024, 2048], P('tp', 'fs'), may hold values from -0.125 to 0.125
- w_out_attn: bfloat16 [1024, 2048], P('tp', 'fs'), may hold values from -0.75 to 0.75
Outputs:
- mixed: bfloat16 [8, 8192, 2048], P('fs', ('sp', 'tp'))
Inputs may be any that keep to these rules, and one draw needn't show every extreme that they name: `gate_cache`: each head's values never rise along the positions.
All inputs are finite; a program needn't handle non-finite values.
Results may differ from a plain program's by a relative error of at most 0.014.
Values may be sent and summed in bfloat16 or wider, within the bound.
No kernel may reach another device: no remote copies, remote signals or barrier semaphores. Data moves between devices by JAX's collectives and lax.ppermute only.
A program may use at most 128 MiB of HBM per device.

v0:
```python
import jax
import jax.numpy as jnp
from jax import lax
from jax.sharding import Mesh
from jax.sharding import PartitionSpec as P

HEAD_DIM = 128
GROUP_WIDTH = 128
TP = ("tp_0", "tp_1")
SP_TP = ("sp", "tp_0", "tp_1")


norm_eps = 1e-06
widest = 16
masked_score = -1e30


def shifted(x, axis, by):
    length = lax.axis_size(axis)
    pairs = [(i, i + by) for i in range(length) if 0 <= i + by < length]
    return lax.ppermute(x, axis, pairs)


def sent_together(arrays, axis, dim, along):
    both = jnp.concatenate(arrays, axis=along)
    result, at, outs = (lax.all_gather(both, axis, axis=dim, tiled=True), 0, [])
    for a in arrays:
        outs.append(lax.slice_in_dim(result, at, at + a.shape[along], axis=along))
        at += a.shape[along]
    return tuple(outs)


def in_blocks(x, dim, length):
    before, after = (x.shape[:dim], x.shape[dim + 1 :])
    return jnp.moveaxis(x.reshape(*before, length, -1, *after), dim, 0)


def in_order(blocks, dim):
    dims = list(blocks.shape[1:])
    dims[dim] *= blocks.shape[0]
    return jnp.moveaxis(blocks, 0, dim).reshape(dims)


def exchange_in_order(blocks, axes, sequence):
    dims = [lax.axis_size(a) for a in axes]
    blocks = blocks.reshape(*dims, *blocks.shape[1:])
    for k in sequence:
        blocks = lax.all_to_all(blocks, axes[k], split_axis=k, concat_axis=k, tiled=True)
    return blocks.reshape(-1, *blocks.shape[len(axes) :])


def stepwise_exchange(x, axes, sequence, split_dim, concat_dim):
    blocks = in_blocks(x, split_dim, lax.axis_size(axes))
    return in_order(exchange_in_order(blocks, axes, sequence), concat_dim)


def window_sums(extended):
    outcome = []
    current = extended
    offset = 1
    for doubling in range(4):
        padding = jnp.zeros((offset, extended.shape[1]), jnp.float32)
        current = current + jnp.concatenate([padding, current[:-offset]], axis=0)
        offset = offset * 2
        outcome.append(current[widest - 1 :])
    return outcome


def pool_branch(projected, border, first_group, first_position, mixing, scaling):
    row_count = projected.shape[0]
    channels = projected.shape[1]
    widened = projected.astype(jnp.float32)
    totals = window_sums(jnp.concatenate([border.astype(jnp.float32), widened], axis=0))
    token_positions = first_position + jnp.arange(row_count)
    window_index = (first_group + jnp.arange(channels) // GROUP_WIDTH) % 4
    averaged = jnp.zeros((row_count, channels), jnp.float32)
    for doubling in range(4):
        counted = jnp.minimum(token_positions + 1, 2 ** (doubling + 1)).astype(jnp.float32)
        picked = (window_index == doubling).astype(jnp.float32)
        averaged = averaged + picked[None, :] * totals[doubling] / counted[:, None]
    departure = (averaged - widened).astype(jnp.bfloat16)
    group_count = channels // GROUP_WIDTH
    mixed_rows = jnp.einsum(
        "tgc,gcd->tgd",
        departure.reshape(row_count, group_count, GROUP_WIDTH),
        mixing,
        preferred_element_type=jnp.float32,
    )
    return (mixed_rows.reshape(row_count, channels) * scaling[None, :]).astype(jnp.bfloat16)


def on_device(
    tokens,
    norm_gain,
    w_pool_in,
    pool_mix,
    pool_scale,
    w_query,
    w_key,
    w_value,
    gate_cache,
    w_out_pool,
    w_out_attn,
):
    tp_index = lax.axis_index(TP)
    tp_count = lax.axis_size(TP)
    seq_count = tokens.shape[0]
    own_count = tokens.shape[1]
    token_count = own_count * tp_count
    first_position = lax.axis_index("sp") * token_count
    own_rows = tokens.astype(jnp.float32)
    normed = (
        own_rows
        * lax.rsqrt(jnp.mean(own_rows * own_rows, axis=-1, keepdims=True) + norm_eps)
        * norm_gain[None, None, :]
    ).astype(jnp.bfloat16)
    pool_full, query_full, key_full, value_full, out_pool_full, out_attn_full = (
        lax.all_gather(w_pool_in, "fs", axis=0, tiled=True),
        lax.all_gather(w_query, "fs", axis=0, tiled=True),
        lax.all_gather(w_key, "fs", axis=0, tiled=True),
        lax.all_gather(w_value, "fs", axis=0, tiled=True),
        lax.all_gather(w_out_pool, "fs", axis=1, tiled=True),
        lax.all_gather(w_out_attn, "fs", axis=1, tiled=True),
    )
    pool_cols = w_pool_in.shape[1]
    attn_cols = w_query.shape[1]
    shard_rows = lax.all_gather(normed, TP, axis=1, tiled=True)
    projected = jnp.concatenate(
        [
            jnp.dot(shard_rows, pool_full, preferred_element_type=jnp.float32).astype(jnp.bfloat16),
            jnp.dot(shard_rows, query_full, preferred_element_type=jnp.float32).astype(
                jnp.bfloat16
            ),
            jnp.dot(shard_rows, key_full, preferred_element_type=jnp.float32).astype(jnp.bfloat16),
            jnp.dot(shard_rows, value_full, preferred_element_type=jnp.float32).astype(
                jnp.bfloat16
            ),
        ],
        axis=2,
    )
    pool_in = projected[:, :, :pool_cols]
    query_proj = projected[:, :, pool_cols : pool_cols + attn_cols]
    key_proj = projected[:, :, pool_cols + attn_cols : pool_cols + 2 * attn_cols]
    value_proj = projected[:, :, pool_cols + 2 * attn_cols :]
    group_local = pool_cols // GROUP_WIDTH
    mixing = lax.dynamic_slice_in_dim(pool_mix, tp_index * group_local, group_local, 0)
    scaling = lax.dynamic_slice_in_dim(pool_scale, tp_index * pool_cols, pool_cols, 0)
    borders = shifted(pool_in[:, token_count - (widest - 1) :], "sp", 1)
    pool_out = jnp.stack(
        [
            pool_branch(
                pool_in[member],
                borders[member],
                tp_index * group_local,
                first_position,
                mixing,
                scaling,
            )
            for member in range(seq_count)
        ],
        axis=0,
    )
    head_count = attn_cols // HEAD_DIM
    query_heads = query_proj.reshape(seq_count, token_count, head_count, HEAD_DIM)
    query_gates = jnp.transpose(
        lax.dynamic_slice_in_dim(gate_cache, first_position, token_count, 2), (0, 2, 1)
    )
    query_positions = first_position + jnp.arange(token_count)
    last_position = first_position + token_count - 1
    score_scale = HEAD_DIM ** (-0.5)
    start_state = (
        jnp.full((seq_count, token_count, head_count), masked_score, jnp.float32),
        jnp.zeros((seq_count, token_count, head_count), jnp.float32),
        jnp.zeros((seq_count, token_count, head_count, HEAD_DIM), jnp.float32),
    )
    key_shard, value_shard = sent_together((key_proj, value_proj), "sp", 1, 0)
    key_total = key_shard.shape[1]
    block_rows = 512

    def one_block(block_state, block_index):
        key_start = block_index * block_rows

        def compute(inner_state):
            running_top, running_sum, running_out = inner_state
            key_block = lax.dynamic_slice_in_dim(key_shard, block_index * block_rows, block_rows, 1)
            value_block = lax.dynamic_slice_in_dim(
                value_shard, block_index * block_rows, block_rows, 1
            )
            key_block = key_block.reshape(seq_count, block_rows, head_count, HEAD_DIM)
            value_block = value_block.reshape(seq_count, block_rows, head_count, HEAD_DIM)
            key_gates = lax.dynamic_slice_in_dim(gate_cache, key_start, block_rows, 2)
            scores = (
                jnp.einsum(
                    "sqhd,skhd->sqhk", query_heads, key_block, preferred_element_type=jnp.float32
                )
                * score_scale
            )
            scores = scores + query_gates[:, :, :, None] - key_gates[:, None, :, :]
            allowed = ((key_start + jnp.arange(block_rows))[None, :] <= query_positions[:, None])[
                None, :, None, :
            ]
            scores = jnp.where(allowed, scores, masked_score)
            new_top = jnp.maximum(running_top, jnp.max(scores, axis=3))
            weights = jnp.where(allowed, jnp.exp(scores - new_top[:, :, :, None]), 0.0)
            shrink = jnp.exp(running_top - new_top)
            running_sum = running_sum * shrink + jnp.sum(weights, axis=3)
            running_out = running_out * shrink[:, :, :, None] + jnp.einsum(
                "sqhk,skhd->sqhd",
                weights.astype(jnp.bfloat16),
                value_block,
                preferred_element_type=jnp.float32,
            )
            return (new_top, running_sum, running_out)

        def unchanged(inner_state):
            return inner_state

        return (lax.cond(key_start <= last_position, compute, unchanged, block_state), None)

    result, unused = lax.scan(one_block, start_state, jnp.arange(key_total // block_rows))
    final_top, final_sum, final_out = result
    attn_out = (
        (final_out / final_sum[:, :, :, None])
        .astype(jnp.bfloat16)
        .reshape(seq_count, token_count, attn_cols)
    )
    joined = jnp.concatenate([pool_out, attn_out], axis=2)
    arrived = stepwise_exchange(joined, TP, (1, 0), 1, 2)
    local_rows = jnp.concatenate([out_pool_full, out_attn_full], axis=0)
    all_rows = lax.all_gather(local_rows, TP, axis=0, tiled=True)
    width_each = pool_cols + attn_cols
    pieces = arrived.reshape(seq_count, own_count, tp_count, width_each)
    stacked = all_rows.reshape(tp_count, width_each, all_rows.shape[1])
    terms = jnp.einsum("snjc,jcd->snjd", pieces, stacked, preferred_element_type=jnp.float32)
    summed = jnp.sum(terms.astype(jnp.bfloat16).astype(jnp.float32), axis=2)
    return summed.astype(jnp.bfloat16)


def solution(mesh):
    torus = Mesh(
        mesh.devices.reshape(mesh.shape["sp"], mesh.shape["fs"], 4, 2), ("sp", "fs", "tp_0", "tp_1")
    )
    return jax.shard_map(
        on_device,
        mesh=torus,
        in_specs=(
            P("fs", SP_TP, None),
            P(),
            P("fs", TP),
            P(),
            P(),
            P("fs", TP),
            P("fs", TP),
            P("fs", TP),
            P("fs", TP, None),
            P(TP, "fs"),
            P(TP, "fs"),
        ),
        out_specs=P("fs", SP_TP, None),
        check_vma=False,
    )
```

profile of v0, /device:TPU:480, one launch (start us, length us, event | category | flops | bytes accessed | tf_op | source)
XLA Modules:
  0.0 305.3 jit_solution(2292655128198487671)
XLA Ops:
  7.8 2.0 fusion.21
  9.9 13.5 %all_gather.32 = bf16[2048,128]{1,0:T(8,128)(2,1)S(1)} all-gather(bf16[512,128]{1,0:T(8,128)(2,1)} %param.21), channel_id=1, replica_groups=mesh['sp'=16,'fs'=4,'tp_0'=4,'tp_1'=2] {'fs'}, dimensions={0}, use_global_device_ids=true | all-gather | bytes 655360 | tf_op jit(solution)/shard_map/all_gather | solution.py:120
  23.4 13.1 %all_gather.33 = bf16[2048,128]{1,0:T(8,128)(2,1)S(1)} all-gather(bf16[512,128]{1,0:T(8,128)(2,1)} %param.22), channel_id=1, replica_groups=mesh['sp'=16,'fs'=4,'tp_0'=4,'tp_1'=2] {'fs'}, dimensions={0}, use_global_device_ids=true | all-gather | bytes 655360 | tf_op jit(solution)/shard_map/all_gather | solution.py:121
  36.5 12.2 %all-gather.6.cloned.1.call-done = bf16[2,512,2048]{2,1,0:T(8,128)(2,1)} async-done(((bf16[2,64,2048]{2,1,0:T(8,128)(2,1)}), bf16[2,512,2048]{2,1,0:T(8,128)(2,1)}) %all-gather.6.cloned.1.call-update) | async-done | bytes 4194320 | tf_op jit(solution)/shard_map/all_gather | solution.py:127
  48.8 3.6 %convolution_convert_fusion.2 = bf16[2,512,128]{2,1,0:T(8,128)(2,1)S(1)} fusion(bf16[2,512,2048]{2,1,0:T(8,128)(2,1)} %all-gather.6.cloned.1.call-done, bf16[2048,128]{1,0:T(8,128)(2,1)S(1)} %all_gather.32), kind=kOutput, calls=%fused_computation.32 | convolution fusion | flops 537001984 | bytes 4980736 | tf_op jit(solution)/shard_map/dot_general | solution.py:134
  54.6 13.1 %all_gather.27 = bf16[128,2048]{1,0:T(8,128)(2,1)S(1)} all-gather(bf16[128,512]{1,0:T(8,128)(2,1)S(1)} %copy-done.1), channel_id=1, replica_groups=mesh['sp'=16,'fs'=4,'tp_0'=4,'tp_1'=2] {'fs'}, dimensions={1}, use_global_device_ids=true | all-gather | bytes 655360 | tf_op jit(solution)/shard_map/all_gather | solution.py:122
  67.7 13.1 %all_gather.28 = bf16[128,2048]{1,0:T(8,128)(2,1)S(1)} all-gather(bf16[128,512]{1,0:T(8,128)(2,1)S(1)} %copy-done.2), channel_id=1, replica_groups=mesh['sp'=16,'fs'=4,'tp_0'=4,'tp_1'=2] {'fs'}, dimensions={1}, use_global_device_ids=true | all-gather | bytes 655360 | tf_op jit(solution)/shard_map/all_gather | solution.py:123
  83.1 13.4 %all_gather.31 = bf16[2048,128]{1,0:T(8,128)(2,1)S(1)} all-gather(bf16[512,128]{1,0:T(8,128)(2,1)S(1)} %copy-done.3), channel_id=1, replica_groups=mesh['sp'=16,'fs'=4,'tp_0'=4,'tp_1'=2] {'fs'}, dimensions={0}, use_global_device_ids=true | all-gather | bytes 655360 | tf_op jit(solution)/shard_map/all_gather | solution.py:118
  96.5 12.8 %all_gather.35 = bf16[2048,128]{1,0:T(8,128)(2,1)S(1)} all-gather(bf16[512,128]{1,0:T(8,128)(2,1)S(1)} %copy-done.4), channel_id=1, replica_groups=mesh['sp'=16,'fs'=4,'tp_0'=4,'tp_1'=2] {'fs'}, dimensions={0}, use_global_device_ids=true | all-gather | bytes 655360 | tf_op jit(solution)/shard_map/all_gather | solution.py:119
  109.2 3.5 %convolution_convert_fusion.3 = bf16[2,512,128]{2,1,0:T(8,128)(2,1)S(1)} fusion(bf16[2,512,2048]{2,1,0:T(8,128)(2,1)} %all-gather.6.cloned.1.call-done, bf16[2048,128]{1,0:T(8,128)(2,1)S(1)} %all_gather.31), kind=kOutput, calls=%fused_computation.33 | convolution fusion | flops 537001984 | bytes 4980736 | tf_op jit(solution)/shard_map/dot_general | solution.py:130
  115.3 3.2 %collective-permute-done = bf16[2,15,128]{2,1,0:T(8,128)(2,1)S(1)} collective-permute-done((bf16[2,15,128]{2,1,0:T(8,128)(2,1)S(1)}, bf16[2,15,128]{2,1,0:T(8,128)(2,1)S(1)}, u32[]{:S(2)}, u32[]{:S(2)}) %collective-permute-start) | collective-permute-done | bytes 7712 | tf_op jit(solution)/shard_map/ppermute | solution.py:21
  120.4 37.7 %all-gather.8.cloned.1.call-done = bf16[4,8192,128]{2,1,0:T(8,128)(2,1)} async-done(((bf16[4,512,128]{2,1,0:T(8,128)(2,1)}), bf16[4,8192,128]{2,1,0:T(8,128)(2,1)}) %all-gather.8.cloned.1.call-update) | async-done | bytes 8388624 | tf_op jit(solution)/shard_map/all_gather | solution.py:26
  158.1 5.8 %fusion.67 = (bf16[2,8192,128]{2,1,0:T(8,128)(2,1)}, bf16[2,8192,128]{2,1,0:T(8,128)(2,1)}) fusion(bf16[4,8192,128]{2,1,0:T(8,128)(2,1)} %all-gather.8.cloned.1.call-done), kind=kLoop, calls=%fused_computation.123 | loop fusion | bytes 16777216 | tf_op jit(solution)/shard_map/slice | solution.py:28
  163.9 6.4 %copy.39 = bf16[2,8192,128]{1,2,0:T(8,128)(2,1)} copy(bf16[2,8192,128]{2,1,0:T(8,128)(2,1)} %get-tuple-element.223) | data formatting | bytes 8388608
  170.4 98.3 %while.15 = (s32[]{:T(128)}, f32[2,512,1]{1,0,2:T(2,128)S(1)}, f32[2,512,1]{1,0,2:T(2,128)S(1)}, f32[2,512,1,128]{1,3,0,2:T(8,128)S(1)}, s32[16]{0:T(128)S(1)}, ...) while((s32[]{:T(128)}, f32[2,512,1]{1,0,2:T(2,128)S(1)}, ...), condition=%wide.region_6.7_spmd.clone, body=%wide.region_1.6_spmd.clone.sunk | while | flops 274731008 | bytes 9269679 | solution.py:220
  171.7 4.9 %conditional.3 = ((f32[2,512,1]{1,0,2:T(2,128)S(1)}, f32[2,512,1]{1,0,2:T(2,128)S(1)}, f32[2,512,1,128]{1,3,0,2:T(8,128)S(1)})) conditional(s32[]{:T(128)} %convert_element_type.218, (f32[2,512,1]{1,0,2:T(2,128)S(1)}, f32[2,512,1]{1,0,2:T(2,128)S(1)}, f32[2,512,1,128]{1,3,0,2:T(8,128)S(1)}) %tuple.48, (s32[]{:T(128)}, s32[]{:T(128)}, s32[]{:T(128)}, ...), branch_computations={%region_2.2_spmd, %region_3.5_spmd} | conditional | flops 274731008 | bytes 9267332 | solution.py:218
  177.8 4.9 %conditional.3 = ((f32[2,512,1]{1,0,2:T(2,128)S(1)}, f32[2,512,1]{1,0,2:T(2,128)S(1)}, f32[2,512,1,128]{1,3,0,2:T(8,128)S(1)})) conditional(s32[]{:T(128)} %convert_element_type.218, (f32[2,512,1]{1,0,2:T(2,128)S(1)}, f32[2,512,1]{1,0,2:T(2,128)S(1)}, f32[2,512,1,128]{1,3,0,2:T(8,128)S(1)}) %tuple.48, (s32[]{:T(128)}, s32[]{:T(128)}, s32[]{:T(128)}, ...), branch_computations={%region_2.2_spmd, %region_3.5_spmd} | conditional | flops 274731008 | bytes 9267332 | solution.py:218
  180.5 1.7 fusion.5
  184.0 4.9 %conditional.3 = ((f32[2,512,1]{1,0,2:T(2,128)S(1)}, f32[2,512,1]{1,0,2:T(2,128)S(1)}, f32[2,512,1,128]{1,3,0,2:T(8,128)S(1)})) conditional(s32[]{:T(128)} %convert_element_type.218, (f32[2,512,1]{1,0,2:T(2,128)S(1)}, f32[2,512,1]{1,0,2:T(2,128)S(1)}, f32[2,512,1,128]{1,3,0,2:T(8,128)S(1)}) %tuple.48, (s32[]{:T(128)}, s32[]{:T(128)}, s32[]{:T(128)}, ...), branch_computations={%region_2.2_spmd, %region_3.5_spmd} | conditional | flops 274731008 | bytes 9267332 | solution.py:218
  186.7 1.7 fusion.5
  190.1 4.9 %conditional.3 = ((f32[2,512,1]{1,0,2:T(2,128)S(1)}, f32[2,512,1]{1,0,2:T(2,128)S(1)}, f32[2,512,1,128]{1,3,0,2:T(8,128)S(1)})) conditional(s32[]{:T(128)} %convert_element_type.218, (f32[2,512,1]{1,0,2:T(2,128)S(1)}, f32[2,512,1]{1,0,2:T(2,128)S(1)}, f32[2,512,1,128]{1,3,0,2:T(8,128)S(1)}) %tuple.48, (s32[]{:T(128)}, s32[]{:T(128)}, s32[]{:T(128)}, ...), branch_computations={%region_2.2_spmd, %region_3.5_spmd} | conditional | flops 274731008 | bytes 9267332 | solution.py:218
  192.8 1.7 fusion.5
  196.3 4.9 %conditional.3 = ((f32[2,512,1]{1,0,2:T(2,128)S(1)}, f32[2,512,1]{1,0,2:T(2,128)S(1)}, f32[2,512,1,128]{1,3,0,2:T(8,128)S(1)})) conditional(s32[]{:T(128)} %convert_element_type.218, (f32[2,512,1]{1,0,2:T(2,128)S(1)}, f32[2,512,1]{1,0,2:T(2,128)S(1)}, f32[2,512,1,128]{1,3,0,2:T(8,128)S(1)}) %tuple.48, (s32[]{:T(128)}, s32[]{:T(128)}, s32[]{:T(128)}, ...), branch_computations={%region_2.2_spmd, %region_3.5_spmd} | conditional | flops 274731008 | bytes 9267332 | solution.py:218
  202.4 4.9 %conditional.3 = ((f32[2,512,1]{1,0,2:T(2,128)S(1)}, f32[2,512,1]{1,0,2:T(2,128)S(1)}, f32[2,512,1,128]{1,3,0,2:T(8,128)S(1)})) conditional(s32[]{:T(128)} %convert_element_type.218, (f32[2,512,1]{1,0,2:T(2,128)S(1)}, f32[2,512,1]{1,0,2:T(2,128)S(1)}, f32[2,512,1,128]{1,3,0,2:T(8,128)S(1)}) %tuple.48, (s32[]{:T(128)}, s32[]{:T(128)}, s32[]{:T(128)}, ...), branch_computations={%region_2.2_spmd, %region_3.5_spmd} | conditional | flops 274731008 | bytes 9267332 | solution.py:218
  208.6 4.9 %conditional.3 = ((f32[2,512,1]{1,0,2:T(2,128)S(1)}, f32[2,512,1]{1,0,2:T(2,128)S(1)}, f32[2,512,1,128]{1,3,0,2:T(8,128)S(1)})) conditional(s32[]{:T(128)} %convert_element_type.218, (f32[2,512,1]{1,0,2:T(2,128)S(1)}, f32[2,512,1]{1,0,2:T(2,128)S(1)}, f32[2,512,1,128]{1,3,0,2:T(8,128)S(1)}) %tuple.48, (s32[]{:T(128)}, s32[]{:T(128)}, s32[]{:T(128)}, ...), branch_computations={%region_2.2_spmd, %region_3.5_spmd} | conditional | flops 274731008 | bytes 9267332 | solution.py:218
  211.3 1.7 fusion.5
  214.7 4.9 %conditional.3 = ((f32[2,512,1]{1,0,2:T(2,128)S(1)}, f32[2,512,1]{1,0,2:T(2,128)S(1)}, f32[2,512,1,128]{1,3,0,2:T(8,128)S(1)})) conditional(s32[]{:T(128)} %convert_element_type.218, (f32[2,512,1]{1,0,2:T(2,128)S(1)}, f32[2,512,1]{1,0,2:T(2,128)S(1)}, f32[2,512,1,128]{1,3,0,2:T(8,128)S(1)}) %tuple.48, (s32[]{:T(128)}, s32[]{:T(128)}, s32[]{:T(128)}, ...), branch_computations={%region_2.2_spmd, %region_3.5_spmd} | conditional | flops 274731008 | bytes 9267332 | solution.py:218
  217.4 1.7 fusion.5
  220.9 4.9 %conditional.3 = ((f32[2,512,1]{1,0,2:T(2,128)S(1)}, f32[2,512,1]{1,0,2:T(2,128)S(1)}, f32[2,512,1,128]{1,3,0,2:T(8,128)S(1)})) conditional(s32[]{:T(128)} %convert_element_type.218, (f32[2,512,1]{1,0,2:T(2,128)S(1)}, f32[2,512,1]{1,0,2:T(2,128)S(1)}, f32[2,512,1,128]{1,3,0,2:T(8,128)S(1)}) %tuple.48, (s32[]{:T(128)}, s32[]{:T(128)}, s32[]{:T(128)}, ...), branch_computations={%region_2.2_spmd, %region_3.5_spmd} | conditional | flops 274731008 | bytes 9267332 | solution.py:218
  223.5 1.7 fusion.5
  227.0 4.9 %conditional.3 = ((f32[2,512,1]{1,0,2:T(2,128)S(1)}, f32[2,512,1]{1,0,2:T(2,128)S(1)}, f32[2,512,1,128]{1,3,0,2:T(8,128)S(1)})) conditional(s32[]{:T(128)} %convert_element_type.218, (f32[2,512,1]{1,0,2:T(2,128)S(1)}, f32[2,512,1]{1,0,2:T(2,128)S(1)}, f32[2,512,1,128]{1,3,0,2:T(8,128)S(1)}) %tuple.48, (s32[]{:T(128)}, s32[]{:T(128)}, s32[]{:T(128)}, ...), branch_computations={%region_2.2_spmd, %region_3.5_spmd} | conditional | flops 274731008 | bytes 9267332 | solution.py:218
  229.7 1.7 fusion.5
  233.1 4.9 %conditional.3 = ((f32[2,512,1]{1,0,2:T(2,128)S(1)}, f32[2,512,1]{1,0,2:T(2,128)S(1)}, f32[2,512,1,128]{1,3,0,2:T(8,128)S(1)})) conditional(s32[]{:T(128)} %convert_element_type.218, (f32[2,512,1]{1,0,2:T(2,128)S(1)}, f32[2,512,1]{1,0,2:T(2,128)S(1)}, f32[2,512,1,128]{1,3,0,2:T(8,128)S(1)}) %tuple.48, (s32[]{:T(128)}, s32[]{:T(128)}, s32[]{:T(128)}, ...), branch_computations={%region_2.2_spmd, %region_3.5_spmd} | conditional | flops 274731008 | bytes 9267332 | solution.py:218
  235.8 1.7 fusion.5
  239.3 4.9 %conditional.3 = ((f32[2,512,1]{1,0,2:T(2,128)S(1)}, f32[2,512,1]{1,0,2:T(2,128)S(1)}, f32[2,512,1,128]{1,3,0,2:T(8,128)S(1)})) conditional(s32[]{:T(128)} %convert_element_type.218, (f32[2,512,1]{1,0,2:T(2,128)S(1)}, f32[2,512,1]{1,0,2:T(2,128)S(1)}, f32[2,512,1,128]{1,3,0,2:T(8,128)S(1)}) %tuple.48, (s32[]{:T(128)}, s32[]{:T(128)}, s32[]{:T(128)}, ...), branch_computations={%region_2.2_spmd, %region_3.5_spmd} | conditional | flops 274731008 | bytes 9267332 | solution.py:218
  242.0 1.7 fusion.5
  245.4 4.9 %conditional.3 = ((f32[2,512,1]{1,0,2:T(2,128)S(1)}, f32[2,512,1]{1,0,2:T(2,128)S(1)}, f32[2,512,1,128]{1,3,0,2:T(8,128)S(1)})) conditional(s32[]{:T(128)} %convert_element_type.218, (f32[2,512,1]{1,0,2:T(2,128)S(1)}, f32[2,512,1]{1,0,2:T(2,128)S(1)}, f32[2,512,1,128]{1,3,0,2:T(8,128)S(1)}) %tuple.48, (s32[]{:T(128)}, s32[]{:T(128)}, s32[]{:T(128)}, ...), branch_computations={%region_2.2_spmd, %region_3.5_spmd} | conditional | flops 274731008 | bytes 9267332 | solution.py:218
  248.1 1.7 fusion.5
  251.6 4.9 %conditional.3 = ((f32[2,512,1]{1,0,2:T(2,128)S(1)}, f32[2,512,1]{1,0,2:T(2,128)S(1)}, f32[2,512,1,128]{1,3,0,2:T(8,128)S(1)})) conditional(s32[]{:T(128)} %convert_element_type.218, (f32[2,512,1]{1,0,2:T(2,128)S(1)}, f32[2,512,1]{1,0,2:T(2,128)S(1)}, f32[2,512,1,128]{1,3,0,2:T(8,128)S(1)}) %tuple.48, (s32[]{:T(128)}, s32[]{:T(128)}, s32[]{:T(128)}, ...), branch_computations={%region_2.2_spmd, %region_3.5_spmd} | conditional | flops 274731008 | bytes 9267332 | solution.py:218
  254.2 1.7 fusion.5
  257.7 4.9 %conditional.3 = ((f32[2,512,1]{1,0,2:T(2,128)S(1)}, f32[2,512,1]{1,0,2:T(2,128)S(1)}, f32[2,512,1,128]{1,3,0,2:T(8,128)S(1)})) conditional(s32[]{:T(128)} %convert_element_type.218, (f32[2,512,1]{1,0,2:T(2,128)S(1)}, f32[2,512,1]{1,0,2:T(2,128)S(1)}, f32[2,512,1,128]{1,3,0,2:T(8,128)S(1)}) %tuple.48, (s32[]{:T(128)}, s32[]{:T(128)}, s32[]{:T(128)}, ...), branch_computations={%region_2.2_spmd, %region_3.5_spmd} | conditional | flops 274731008 | bytes 9267332 | solution.py:218
  260.4 1.7 fusion.5
  263.8 4.9 %conditional.3 = ((f32[2,512,1]{1,0,2:T(2,128)S(1)}, f32[2,512,1]{1,0,2:T(2,128)S(1)}, f32[2,512,1,128]{1,3,0,2:T(8,128)S(1)})) conditional(s32[]{:T(128)} %convert_element_type.218, (f32[2,512,1]{1,0,2:T(2,128)S(1)}, f32[2,512,1]{1,0,2:T(2,128)S(1)}, f32[2,512,1,128]{1,3,0,2:T(8,128)S(1)}) %tuple.48, (s32[]{:T(128)}, s32[]{:T(128)}, s32[]{:T(128)}, ...), branch_computations={%region_2.2_spmd, %region_3.5_spmd} | conditional | flops 274731008 | bytes 9267332 | solution.py:218
  269.3 4.2 %all_to_all.10 = bf16[4,2,2,64,256]{4,3,2,0,1:T(8,128)(2,1)S(1)} all-to-all(bf16[4,2,2,64,256]{4,3,2,0,1:T(8,128)(2,1)S(1)} %copy.41), channel_id=1, replica_groups=mesh['sp'=16,'fs'=4,'tp_0'=4,'tp_1'=2] {'tp_1'}, dimensions={1} | all-to-all | bytes 1048576 | tf_op jit(solution)/shard_map/all_to_all | solution.py:48
  274.2 4.3 %all-to-all-start.1 = ((bf16[4,2,2,64,256]{4,3,2,1,0:T(8,128)(2,1)}), bf16[4,2,2,64,256]{4,3,2,1,0:T(8,128)(2,1)S(1)}, u32[]{:S(2)}, u32[]{:S(2)}) async-start(bf16[4,2,2,64,256]{4,3,2,1,0:T(8,128)(2,1)} %copy.42), calls=%async_computation.1 | async-start | bytes 1048576 | tf_op jit(solution)/shard_map/all_to_all | solution.py:48
  278.5 9.8 %all-to-all-done.1 = bf16[4,2,2,64,256]{4,3,2,1,0:T(8,128)(2,1)S(1)} async-done(((bf16[4,2,2,64,256]{4,3,2,1,0:T(8,128)(2,1)}), bf16[4,2,2,64,256]{4,3,2,1,0:T(8,128)(2,1)S(1)}, u32[]{:S(2)}, u32[]{:S(2)}) %all-to-all-start.1) | async-done | bytes 524320 | tf_op jit(solution)/shard_map/all_to_all | solution.py:48
  288.3 6.6 %bitcast_convert_fusion = bf16[8,2048,2,64]{1,3,2,0:T(8,128)(2,1)} fusion(bf16[8,256,128]{1,2,0:T(8,128)(2,1)S(1)} %bitcast.118, bf16[8,256,2048]{2,1,0:T(8,128)(2,1)} %bitcast.117), kind=kOutput, calls=%fused_computation.27 | convolution fusion | flops 1075838976 | bytes 13107200
  294.9 3.8 %reduce_sum.35 = bf16[2048,2,64]{0,2,1:T(8,128)(2,1)} reduce(bf16[8,2048,2,64]{1,3,2,0:T(8,128)(2,1)} %bitcast_convert_fusion, bf16[]{:T(256)} %constant.119.clone.1), dimensions={0}, to_apply=%region_7.8 | reduce | flops 1835008 | bytes 4718594 | tf_op jit(solution)/shard_map/reduce_sum | solution.py:235
  (227 shorter events, 66.5 us)
Async XLA Ops:
  6.5 112.3 %copy-start = (bf16[8,128,128]{2,1,0:T(8,128)(2,1)S(1)}, bf16[8,128,128]{2,1,0:T(8,128)(2,1)}, u32[]{:S(2)}) copy-start(bf16[8,128,128]{2,1,0:T(8,128)(2,1)} %param.18) | copy-start | bytes 786436
  6.5 42.2 %all-gather.6.cloned.1.call-start = ((), (), s32[]{:S(2)}) async-start(), calls=%async_computation.3 | async-start | bytes 4718592 | tf_op jit(solution)/shard_map/all_gather | solution.py:127
  9.9 148.2 %all-gather.8.cloned.1.call-start = ((), (), s32[]{:S(2)}) async-start(), calls=%async_computation.4 | async-start | bytes 8912896 | tf_op jit(solution)/shard_map/all_gather | solution.py:26
  48.7 3.6 %copy-start.6 = (bf16[2,512,2048]{2,1,0:T(8,128)(2,1)S(1)}, bf16[2,512,2048]{2,1,0:T(8,128)(2,1)}, u32[]{:S(2)}) copy-start(bf16[2,512,2048]{2,1,0:T(8,128)(2,1)} %all-gather.6.cloned.1.call-done) | copy-start | bytes 12582916
  52.3 2.2 copy-start.1
  52.4 15.4 %copy-start.2 = (bf16[128,512]{1,0:T(8,128)(2,1)S(1)}, bf16[128,512]{1,0:T(8,128)(2,1)}, u32[]{:S(2)}) copy-start(bf16[128,512]{1,0:T(8,128)(2,1)} %param.25) | copy-start | bytes 393220
  53.6 28.4 %copy-start.5 = (f32[2,1,8192]{2,1,0:T(1,128)S(1)}, f32[2,1,8192]{2,1,0:T(1,128)}, u32[]{:S(2)}) copy-start(f32[2,1,8192]{2,1,0:T(1,128)} %param.23) | copy-start | bytes 196612
  53.6 29.5 %copy-start.3 = (bf16[512,128]{1,0:T(8,128)(2,1)S(1)}, bf16[512,128]{1,0:T(8,128)(2,1)}, u32[]{:S(2)}) copy-start(bf16[512,128]{1,0:T(8,128)(2,1)} %param.17) | copy-start | bytes 393220
  53.6 42.8 %copy-start.4 = (bf16[512,128]{1,0:T(8,128)(2,1)S(1)}, bf16[512,128]{1,0:T(8,128)(2,1)}, u32[]{:S(2)}) copy-start(bf16[512,128]{1,0:T(8,128)(2,1)} %param.20) | copy-start | bytes 393220
  54.5 224.0 %all-gather.4.cloned.1.call-start = ((), (), s32[]{:S(2)}) async-start(), calls=%async_computation.2 | async-start | bytes 9437184 | tf_op jit(solution)/shard_map/all_gather | solution.py:230
  82.1 32.0 %copy-start.7 = (bf16[2,512,2048]{2,1,0:T(8,128)(2,1)S(1)}, bf16[2,512,2048]{2,1,0:T(8,128)(2,1)}, u32[]{:S(2)}) copy-start(bf16[2,512,2048]{2,1,0:T(8,128)(2,1)} %all-gather.6.cloned.1.call-done) | copy-start | bytes 12582916
  112.7 5.8 %collective-permute-start = (bf16[2,15,128]{2,1,0:T(8,128)(2,1)S(1)}, bf16[2,15,128]{2,1,0:T(8,128)(2,1)S(1)}, u32[]{:S(2)}, u32[]{:S(2)}) collective-permute-start(bf16[2,15,128]{2,1,0:T(8,128)(2,1)S(1)} %slice.92), channel_id=1, source_target_pairs={{0,32},{32,64},{64,96},{96,128},{128,160},{160,192},{192,224},{224... | collective-permute-start | bytes 23048 | tf_op jit(solution)/shard_map/ppermute | solution.py:21
  274.2 14.0 %all-to-all-start.1 = ((bf16[4,2,2,64,256]{4,3,2,1,0:T(8,128)(2,1)}), bf16[4,2,2,64,256]{4,3,2,1,0:T(8,128)(2,1)S(1)}, u32[]{:S(2)}, u32[]{:S(2)}) async-start(bf16[4,2,2,64,256]{4,3,2,1,0:T(8,128)(2,1)} %copy.42), calls=%async_computation.1 | async-start | bytes 1048576 | tf_op jit(solution)/shard_map/all_to_all | solution.py:48
Sparse Core Ops, SparseCore 0:
  10.0 38.7 all-gather.5
  54.6 103.4 all-gather.7
  160.3 57.8 all-gather.3
where the time goes:
time: 307 us; the launch traced here: 305 us
  blocking collectives  83.1 us (27%)
  matrix products  71.4 us (23%)
  waiting for transfers between devices  63 us (21%)
  local copies, waits for them, and re-layouts  25.4 us (8%)
  loops' own time  22.7 us (7%)
  other arithmetic  20.7 us (7%)
  between operations  13.4 us (4%)
  starting transfers between devices  5.64 us (2%)
    all_gather x1, waiting for transfers between devices, sent_together(): result, at, outs = (lax.all_gather(both, axis, axis=dim, tiled=True), 0, [])  37.7 us
    dot_general x16, matrix products, compute(): jnp.einsum('sqhk,skhd->sqhd', weights.astype(jnp.bfloat16), value_block,...  27.4 us
    dot_general x16, matrix products, compute(): jnp.einsum('sqhd,skhd->sqhk', query_heads, key_block, preferred_element_t...  26.7 us
    all_gather x1, blocking collectives, on_device(): lax.all_gather(w_key, 'fs', axis=0, tiled=True)  13.5 us
    all_gather x1, blocking collectives, on_device(): lax.all_gather(w_pool_in, 'fs', axis=0, tiled=True)  13.4 us
    all_gather x1, blocking collectives, on_device(): lax.all_gather(w_out_pool, 'fs', axis=1, tiled=True)  13.1 us
    all_gather x1, blocking collectives, on_device(): lax.all_gather(w_out_attn, 'fs', axis=1, tiled=True)  13.1 us
    all_gather x1, blocking collectives, on_device(): lax.all_gather(w_value, 'fs', axis=0, tiled=True)  13.1 us
  transfers between devices with their start and end apart: 5, of which 4 were waited for; matrix products, arithmetic and copies ran while one was open for 32% of the time, Pallas kernels for 0%

commit v1 on v0

v1 whole, which is shorter than its diff:
```python
import jax
import jax.numpy as jnp
from jax import lax
from jax.experimental import pallas as pl
from jax.experimental.pallas import tpu as pltpu
from jax.sharding import Mesh
from jax.sharding import PartitionSpec as P

HD = 128
TP = ("tp_0", "tp_1")
SP_TP = ("sp", "tp_0", "tp_1")
EPS = 1e-06
MASKED = -1e30
LOG2E = 1.4426950408889634
F32 = jnp.float32
BF16 = jnp.bfloat16
VMEM_LIMIT = 56 * 1024 * 1024


def params(**kw):
    return pltpu.CompilerParams(vmem_limit_bytes=VMEM_LIMIT, **kw)


def whole(memory=pltpu.VMEM):
    return pl.BlockSpec(memory_space=memory)


def spread(x, axis):
    n = lax.axis_size(axis)
    return lax.all_to_all(jnp.broadcast_to(x[None], (n,) + x.shape), axis, 0, 0, tiled=True)


def sibling(x):
    return lax.ppermute(x, "tp_1", [(0, 1), (1, 0)])


def ring_of_four(x, axis):
    up = [(i, (i + 1) % 4) for i in range(4)]
    down = [(i, (i - 1) % 4) for i in range(4)]
    before = lax.ppermute(x, axis, up)
    after = lax.ppermute(x, axis, down)
    half = x.shape[0] // 2
    far_low = lax.ppermute(before[:half], axis, up)
    far_high = lax.ppermute(after[half:], axis, down)
    return x, before, after, far_low, far_high


def rms(x):
    wide = x.astype(F32)
    return lax.rsqrt(jnp.mean(wide * wide, axis=-1, keepdims=True) + EPS)


def factors_of(rows_of):
    seqs, rows, _ = rows_of[0].shape

    def body(x0, x1, x2, x3, x4, out_ref):
        at = 0
        for ref in (x0, x1, x2, x3, x4):
            for i in range(ref.shape[0]):
                out_ref[at : at + rows] = rms(ref[i])
                at += rows

    return pl.pallas_call(
        body,
        in_specs=[whole()] * 5,
        out_specs=whole(),
        out_shape=jax.ShapeDtypeStruct((4 * seqs * rows, 1), F32),
        compiler_params=params(),
        name="factors",
    )(*rows_of)


def project(places, norm, rows_of, own, other, half, factors, split):
    seqs, rows, depth = rows_of[0].shape
    kinds = len(factors)

    def body(p_ref, norm_ref, x0, x1, x2, x3, x4, own_ref, other_ref, *outs):
        x = jnp.concatenate(
            [x0[0], x0[1], x1[0], x1[1], x2[0], x2[1], x3[0], x4[0]], axis=0
        )
        r = norm_ref[...]
        for ref, head in ((own_ref, p_ref[0]), (other_ref, 1 - p_ref[0])):
            y = jnp.dot(x, ref[...], preferred_element_type=F32) * r
            for kind, factor in enumerate(factors):
                part = y[:, kind * HD : (kind + 1) * HD]
                if factor != 1.0:
                    part = part * factor
                part = part.astype(BF16)
                for a in range(4):
                    for i in range(seqs):
                        at = (a * seqs + i) * rows
                        if split:
                            outs[a][kind, 0, i, head] = part[at : at + rows]
                        else:
                            outs[0][p_ref[1 + a], i, head, kind] = part[at : at + rows]

    w_spec = pl.BlockSpec((depth, kinds * HD), lambda *_: (0, half))
    if split:
        shapes = [(kinds, 1, seqs, 2, rows, HD)] * 4
    else:
        shapes = [(4, seqs, 2, kinds, rows, HD)]
    outs = pl.pallas_call(
        body,
        grid=(1,),
        in_specs=[whole(pltpu.SMEM)] + [whole()] * 6 + [w_spec, w_spec],
        out_specs=[whole()] * len(shapes),
        out_shape=[jax.ShapeDtypeStruct(sh, BF16) for sh in shapes],
        compiler_params=params(),
        name="project",
    )(places, norm, *rows_of, own, other)
    return outs


def attend(q, own, other, gates, key_place, query_place):
    blocks, rows, _ = q.shape
    span = 8 * rows
    group = 4
    tall = group * rows
    count = blocks // group

    def body(q_ref, *refs):
        kvs, (gate_ref, kp_ref, qp_ref, out_ref, acc_ref, top_ref) = refs[:10], refs[10:]
        ones = jnp.ones((span, HD), BF16)

        def pieces(s, kind, late):
            out = []
            for side in (kvs[:5], kvs[5:]):
                out += [side[0][s, kind], side[1][s, kind], side[2][s, kind]]
                out.append(side[4][s - blocks // 2, kind] if late else side[3][s, kind])
            return jnp.concatenate(out, axis=0)

        def step(s, first_group, fresh, late):
            k = pieces(s, 0, late)
            v = jnp.concatenate([pieces(s, 1, late), ones], axis=1)
            gate = gate_ref[s]
            for g in range(first_group, count):
                at = pl.ds(g * tall, tall)
                qt = q_ref[g * group : (g + 1) * group].reshape(tall, HD)
                sc = lax.dot_general(
                    qt, k, (((1,), (1,)), ((), ())), preferred_element_type=F32
                )
                sc = sc - gate
                if g == first_group:
                    sc = jnp.where(kp_ref[...] + s * span <= qp_ref[at], sc, MASKED)
                new = jnp.max(sc, axis=1, keepdims=True)
                if fresh:
                    p = jnp.exp2(sc - new).astype(BF16)
                    acc_ref[at] = jnp.dot(p, v, preferred_element_type=F32)
                else:
                    top = top_ref[at]
                    new = jnp.maximum(top, new)
                    p = jnp.exp2(sc - new).astype(BF16)
                    acc_ref[at] = acc_ref[at] * jnp.exp2(top - new) + jnp.dot(
                        p, v, preferred_element_type=F32
                    )
                top_ref[at] = new

        step(0, 0, True, False)
        for r in range(count):

            def loop(s, carry, r=r):
                step(s, r, False, 2 * r >= count)
                return carry

            lax.fori_loop(max(1, r * group), (r + 1) * group, loop, 0)
        for g in range(count):
            acc = acc_ref[g * tall : (g + 1) * tall]
            out_ref[g * group : (g + 1) * group] = (
                (acc[:, :HD] / acc[:, HD:]).astype(BF16).reshape(group, rows, HD)
            )

    return pl.pallas_call(
        body,
        in_specs=[whole()] * 14,
        out_specs=whole(),
        out_shape=jax.ShapeDtypeStruct(q.shape, BF16),
        scratch_shapes=[
            pltpu.VMEM((blocks * rows, 2 * HD), F32),
            pltpu.VMEM((blocks * rows, 1), F32),
        ],
        compiler_params=params(),
        name="attend",
    )(q, *own, *other, gates, key_place, query_place)


def pool(first, rows_in, border, mix, scale):
    nx, seqs, two, rows, _ = rows_in.shape
    edge = border.shape[3]

    def body(first_ref, in_ref, edge_ref, mix_ref, scale_ref, out_ref):
        at = first_ref[0] + lax.broadcasted_iota(jnp.int32, (rows, 1), 0) + 1
        for x in range(nx):
            for c in range(two):
                group = 2 * x + c
                width = 2 ** (1 + group % 4)
                inverse = 1.0 / jnp.minimum(at, width).astype(F32)
                parts = []
                for i in range(seqs):
                    own = in_ref[x, i, c].astype(F32)
                    total = jnp.concatenate([edge_ref[x, i, c].astype(F32), own], axis=0)
                    by = 1
                    while by < width:
                        total = total + pltpu.roll(total, by, 0)
                        by *= 2
                    parts.append((total[edge:] * inverse - own).astype(BF16))
                mixed = jnp.dot(
                    jnp.concatenate(parts, axis=0), mix_ref[group], preferred_element_type=F32
                )
                mixed = (mixed * scale_ref[group : group + 1, :]).astype(BF16)
                for i in range(seqs):
                    out_ref[x, i, c] = mixed[i * rows : (i + 1) * rows]

    return pl.pallas_call(
        body,
        in_specs=[whole(pltpu.SMEM)] + [whole()] * 4,
        out_specs=whole(),
        out_shape=jax.ShapeDtypeStruct(rows_in.shape, BF16),
        compiler_params=params(),
        name="pool",
    )(first, rows_in, border, mix, scale)


def finish(places, pooled, attn, own, other):
    nx, seqs, _, rows, _ = pooled.shape
    ny, deep, wide = own[0].shape

    def body(p_ref, pool_ref, attn_ref, *refs):
        out_ref = refs[10]
        late = pl.program_id(0) >= ny // 2
        total = jnp.zeros((seqs * rows, wide), F32)
        for side, c in ((refs[:5], p_ref[0]), (refs[5:10], 1 - p_ref[0])):
            for a in range(nx):
                x = p_ref[1 + a]
                left = jnp.concatenate(
                    [
                        jnp.concatenate([pool_ref[x, i, c] for i in range(seqs)], axis=0),
                        jnp.concatenate([attn_ref[x, i, c] for i in range(seqs)], axis=0),
                    ],
                    axis=1,
                )
                right = side[a][0] if a < 3 else jnp.where(late, side[4][0], side[3][0])
                total = total + jnp.dot(left, right, preferred_element_type=F32)
        out_ref[...] = total.astype(BF16).reshape(seqs, rows, wide)

    half = ny // 2
    shape = (1, deep, wide)
    specs = [pl.BlockSpec(shape, lambda j: (j, 0, 0))] * 3 + [
        pl.BlockSpec(shape, lambda j: (jnp.minimum(j, half - 1), 0, 0)),
        pl.BlockSpec(shape, lambda j: (jnp.maximum(j - half, 0), 0, 0)),
    ]
    return pl.pallas_call(
        body,
        grid=(ny,),
        in_specs=[whole(pltpu.SMEM), whole(), whole()] + specs + specs,
        out_specs=pl.BlockSpec((seqs, rows, wide), lambda j: (0, 0, j)),
        out_shape=jax.ShapeDtypeStruct((seqs, rows, ny * wide), BF16),
        compiler_params=params(),
        name="finish",
    )(places, pooled, attn, *own, *other)


def after(x, *others):
    return lax.optimization_barrier((x,) + others)[0]


def placed(pieces, where, dim):
    shape = list(pieces[0].shape)
    shape[dim] = len(pieces)
    out = jnp.zeros(shape, pieces[0].dtype)
    for piece, at in zip(pieces, where):
        out = lax.dynamic_update_slice_in_dim(out, piece, at, dim)
    return out


def on_device(
    tokens,
    norm_gain,
    w_pool_in,
    pool_mix,
    pool_scale,
    w_query,
    w_key,
    w_value,
    gate_cache,
    w_out_pool,
    w_out_attn,
):
    z = lax.axis_index("sp")
    x = lax.axis_index("tp_0")
    y = lax.axis_index("fs")
    c = lax.axis_index("tp_1")
    planes = lax.axis_size("sp")
    chunks = lax.axis_size("tp_0")
    seqs, rows, depth = tokens.shape
    block = rows * chunks * 2
    seen = [x, (x + 3) % 4, (x + 1) % 4, (x + 2) % 4]
    places = jnp.stack([c] + seen).astype(jnp.int32)

    deep = w_key.shape[0]
    gain = lax.dynamic_slice_in_dim(norm_gain, y * deep, deep, 0)
    all_rows = ring_of_four(tokens, "tp_0")
    norm = factors_of(all_rows)
    weights = jnp.concatenate([w_key, w_value, w_query, w_pool_in], axis=1)
    weights = (weights.astype(F32) * gain[:, None]).astype(BF16)
    own_w = spread(weights, "fs").reshape(depth, -1)
    other_w = sibling(own_w)

    (kv,) = project(places, norm, all_rows, own_w, other_w, 0, (1.0, 1.0), False)
    kv_here = lax.all_to_all(kv, "tp_0", 0, 0, tiled=True)
    kv = lax.all_to_all(
        kv_here.reshape(planes, 2, rows, HD), "sp", 0, 0, tiled=True
    )
    qp = project(
        places, norm, all_rows, own_w, other_w, 1, (HD**-0.5 * LOG2E, 1.0), True
    )
    got = [qp[0]]
    for piece, by in zip(qp[1:], (-1, 1, 2)):
        got.append(
            lax.ppermute(piece, "tp_0", [(i, (i + by) % 4) for i in range(4)])
        )
    came = [x, (x + 1) % 4, (x + 3) % 4, (x + 2) % 4]
    qp = placed(got, came, 1)

    pair_seq = (z // 2) % 2
    pair_head = 2 * (z // 4) + z % 2
    gate_rows = lax.dynamic_index_in_dim(gate_cache[:, 0], pair_seq, 0, keepdims=False)
    gate_all = lax.all_gather(after(gate_rows, kv_here), TP, axis=0, tiled=False)
    gate = lax.dynamic_index_in_dim(gate_all, pair_head, 0, keepdims=False) * LOG2E
    gate = gate.reshape(planes, chunks, 2, rows).transpose(0, 2, 1, 3)
    gate = jnp.where(c == 0, gate, gate[:, ::-1])
    gate = jnp.concatenate([lax.dynamic_slice_in_dim(gate, at, 1, 2) for at in seen], axis=2)
    gate = gate.reshape(planes, 1, block)

    q = after(qp[0].reshape(planes, rows, HD), kv, gate)
    q = lax.all_to_all(q, "sp", 0, 0, tiled=True)
    pool_in = qp[1]
    total = planes * chunks * 2
    border = lax.ppermute(
        pool_in[:, :, :, rows - 16 :], SP_TP, [(i, i + 1) for i in range(total - 1)]
    )
    first = (z * block + (2 * x + c) * rows).reshape(1).astype(jnp.int32)
    pooled = pool(first, pool_in, border, pool_mix, pool_scale.reshape(-1, HD))

    kv_own = ring_of_four(kv, "tp_0")
    kv_other = [sibling(piece) for piece in kv_own]

    out_w = jnp.concatenate([w_out_pool, w_out_attn], axis=0)
    o = ring_of_four(after(out_w, own_w), "fs")
    o = [o[0], o[1], o[2], jnp.concatenate(o[3:], axis=0)]
    o = placed([w[None] for w in o], [y, (y + 3) % 4, (y + 1) % 4, (y + 2) % 4], 0)
    out_own = ring_of_four(after(o, kv_here), "tp_0")
    out_other = [sibling(piece) for piece in out_own]

    at = jnp.arange(rows, dtype=jnp.int32)
    key_place = jnp.concatenate(
        [((2 * s + cc) * rows + at) for cc in (c, 1 - c) for s in seen]
    ).reshape(1, -1).astype(jnp.int32)
    query_place = (
        jnp.arange(planes, dtype=jnp.int32)[:, None] * block + (2 * x + c) * rows + at[None]
    ).reshape(-1, 1)
    attn = attend(q, kv_own, kv_other, gate, key_place, query_place)
    attn = lax.all_to_all(attn, "sp", 0, 0, tiled=True)
    attn = attn.reshape(chunks, seqs, 2, rows, HD)
    return finish(places, pooled, attn, out_own, out_other)


def solution(mesh):
    torus = Mesh(
        mesh.devices.reshape(mesh.shape["sp"], mesh.shape["fs"], 4, 2), ("sp", "fs", "tp_0", "tp_1")
    )
    return jax.shard_map(
        on_device,
        mesh=torus,
        in_specs=(
            P("fs", SP_TP, None),
            P(),
            P("fs", TP),
            P(),
            P(),
            P("fs", TP),
            P("fs", TP),
            P("fs", TP),
            P("fs", TP, None),
            P(TP, "fs"),
            P(TP, "fs"),
        ),
        out_specs=P("fs", SP_TP, None),
        check_vma=False,
    )
```

time: 307 us -> 291 us (0.948)
  the two profiles are of different devices: /device:TPU:480 before, /device:TPU:32 now
where the time goes in v1:
time: 291 us; the launch traced here: 290 us
  starting transfers between devices  130 us (45%)
  blocking collectives  59.6 us (20%)
  Pallas kernels  39.7 us (14%)
  waiting for transfers between devices  36.8 us (13%)
  local copies, waits for them, and re-layouts  18.3 us (6%)
  other arithmetic  3.72 us (1%)
    all_to_all x1, blocking collectives, spread(): lax.all_to_all(jnp.broadcast_to(x[None], (n,) + x.shape), axis, 0, 0, til...  30.7 us
    all_gather x1, blocking collectives, on_device(): lax.all_gather(after(gate_rows, kv_here), TP, axis=0, tiled=False)  28.9 us
    ppermute x11, starting transfers between devices, sibling(): return lax.ppermute(x, 'tp_1', [(0, 1), (1, 0)])  25.1 us
    pallas_call x1, Pallas kernels, attend(): pl.pallas_call(body, in_specs=[whole()] * 14, out_specs=whole(), out_shap...  20.2 us
    ppermute x4, starting transfers between devices, ring_of_four(): far_high = lax.ppermute(after[half:], axis, down)  16.9 us
    all_to_all x1, starting transfers between devices, on_device(): lax.all_to_all(kv_here.reshape(planes, 2, rows, HD), 'sp', 0, 0, tiled=True)  15.2 us
    ppermute x4, starting transfers between devices, ring_of_four(): after = lax.ppermute(x, axis, down)  14.4 us
    all_to_all x1, starting transfers between devices, on_device(): attn = lax.all_to_all(attn, 'sp', 0, 0, tiled=True)  12.4 us
  transfers between devices with their start and end apart: 35, of which 7 were waited for; matrix products, arithmetic and copies ran while one was open for 7% of the time, Pallas kernels for 10%

profile of v1, /device:TPU:32, one launch (start us, length us, event | category | flops | bytes accessed | tf_op | source)
XLA Modules:
  0.0 289.7 jit_solution(761219182189514108)
XLA Ops:
  2.2 30.7 %all_to_all.25 = bf16[4,512,512]{2,1,0:T(8,128)(2,1)S(1)} all-to-all(bf16[4,512,512]{2,1,0:T(8,128)(2,1)S(1)} %broadcast_in_dim.28), channel_id=1, replica_groups=mesh['sp'=16,'fs'=4,'tp_0'=4,'tp_1'=2] {'fs'}, dimensions={0} | all-to-all | bytes 4194304 | tf_op jit(solution)/shard_map/all_to_all | solution.py:30
  33.0 1.9 collective-permute-start.4
  34.9 4.7 %collective-permute-start.1 = (bf16[2,64,2048]{2,1,0:T(8,128)(2,1)S(1)}, bf16[2,64,2048]{2,1,0:T(8,128)(2,1)S(1)}, u32[]{:S(2)}, u32[]{:S(2)}) collective-permute-start(bf16[2,64,2048]{2,1,0:T(8,128)(2,1)S(1)} %copy-done.4), channel_id=1, source_target_pairs={{0,6},{2,0},{4,2},{6,4},{1,7},{3,1},{5,3},{7,5},{8,14},{10,8},{12,... | collective-permute-start | bytes 1572872 | tf_op jit(solution)/shard_map/ppermute | solution.py:41
  39.6 1.9 collective-permute-start
  41.5 9.9 %collective-permute-done.1.x2 = bf16[2,64,2048]{2,1,0:T(8,128)(2,1)S(1)} collective-permute-done((bf16[2,64,2048]{2,1,0:T(8,128)(2,1)S(1)}, bf16[2,64,2048]{2,1,0:T(8,128)(2,1)S(1)}, u32[]{:S(2)}, u32[]{:S(2)}) %collective-permute-start.1) | collective-permute-done | bytes 524320 | tf_op jit(solution)/shard_map/ppermute | solution.py:41
  52.2 5.6 %collective-permute-start.3 = (bf16[1,64,2048]{2,1,0:T(8,128)(2,1)}, bf16[1,64,2048]{2,1,0:T(8,128)(2,1)S(1)}, u32[]{:S(2)}, u32[]{:S(2)}) collective-permute-start(bf16[1,64,2048]{2,1,0:T(8,128)(2,1)} %slice.45), channel_id=1, source_target_pairs={{0,6},{2,0},{4,2},{6,4},{1,7},{3,1},{5,3},{7,5},{8,14},{10,8},{12,... | collective-permute-start | bytes 786440 | tf_op jit(solution)/shard_map/ppermute | solution.py:44
  61.2 2.3 collective-permute-done.3.x4
  63.4 6.1 %collective-permute-done.2.x3 = bf16[1,64,2048]{2,1,0:T(8,128)(2,1)} collective-permute-done((bf16[1,64,2048]{2,1,0:T(8,128)(2,1)}, bf16[1,64,2048]{2,1,0:T(8,128)(2,1)}, u32[]{:S(2)}, u32[]{:S(2)}) %collective-permute-start.2) | collective-permute-done | bytes 262176 | tf_op jit(solution)/shard_map/ppermute | solution.py:43
  69.5 2.7 factors.1.norm_ref
  72.3 4.4 %project.3 = bf16[4,2,2,2,64,128]{5,4,3,2,1,0:T(8,128)(2,1)} custom-call(s32[5]{0:T(128)} %stack.23.p_ref, f32[512,1]{1,0:T(8,128)} %factors.1.norm_ref, bf16[2,64,2048]{2,1,0:T(8,128)(2,1)} %x0.5, bf16[2,64,2048]{2,1,0:T(8,128)(2,1)} %copy-done.3, bf16[2,64,2048]{2,1,0:T(8,128)(2,1)} %copy-done.2, bf16[1,64,2048]{2,1,0:T(8,128)(2,1)} %collective-permute-done.2.x3, ...), custom_call_target="tpu_custom_call" | custom-call | tf_op jit(solution)/shard_map/project/pallas_call | solution.py:102
  76.7 4.1 %all-to-all-start.1 = ((bf16[4,2,2,2,64,128]{5,4,3,2,1,0:T(8,128)(2,1)}), bf16[4,2,2,2,64,128]{5,4,3,2,1,0:T(8,128)(2,1)}, u32[]{:S(2)}, u32[]{:S(2)}) async-start(bf16[4,2,2,2,64,128]{5,4,3,2,1,0:T(8,128)(2,1)} %project.3), calls=%async_computation.1 | async-start | bytes 1048576 | tf_op jit(solution)/shard_map/all_to_all | solution.py:309
  80.9 3.1 %collective-permute-start.19 = (bf16[256,512]{1,0:T(8,128)(2,1)S(1)}, bf16[256,512]{1,0:T(8,128)(2,1)S(1)}, u32[]{:S(2)}, u32[]{:S(2)}) collective-permute-start(bf16[256,512]{1,0:T(8,128)(2,1)S(1)} %pad_maximum_fusion), channel_id=1, source_target_pairs={{0,24},{8,0},{16,8},{24,16},{1,25},{9,1},{17,9},{25,17},{2,26},{10... | collective-permute-start | bytes 786440 | tf_op jit(solution)/shard_map/ppermute | solution.py:41
  84.0 2.8 collective-permute-start.18
  86.7 2.5 all-to-all-done.1
  89.3 15.2 %all-to-all-start.2 = ((bf16[16,2,64,128]{3,2,1,0:T(8,128)(2,1)}), bf16[16,2,64,128]{3,2,1,0:T(8,128)(2,1)}, u32[]{:S(2)}, u32[]{:S(2)}) async-start(bf16[16,2,64,128]{3,2,1,0:T(8,128)(2,1)} %bitcast.10), calls=%async_computation.2 | async-start | bytes 1048576 | tf_op jit(solution)/shard_map/all_to_all | solution.py:310
  104.8 3.1 %collective-permute-start.21 = (bf16[128,512]{1,0:T(8,128)(2,1)S(1)}, bf16[128,512]{1,0:T(8,128)(2,1)S(1)}, u32[]{:S(2)}, u32[]{:S(2)}) collective-permute-start(bf16[128,512]{1,0:T(8,128)(2,1)S(1)} %slice.52), channel_id=1, source_target_pairs={{0,24},{8,0},{16,8},{24,16},{1,25},{9,1},{17,9},{25,17},{2,26},{10... | collective-permute-start | bytes 393224 | tf_op jit(solution)/shard_map/ppermute | solution.py:44
  107.9 2.8 collective-permute-start.20
  110.7 4.2 %project.2 = (bf16[2,1,2,2,64,128]{5,4,3,2,1,0:T(8,128)(2,1)}, bf16[2,1,2,2,64,128]{5,4,3,2,1,0:T(8,128)(2,1)}, bf16[2,1,2,2,64,128]{5,4,3,2,1,0:T(8,128)(2,1)}, bf16[2,1,2,2,64,128]{5,4,3,2,1,0:T(8,128)(2,1)}) custom-call(s32[5]{0:T(128)} %stack.23.p_ref, f32[512,1]{1,0:T(8,128)} %factors.1.norm_ref, bf16[2,64,2048]{2,1,0:T(8,128)(2,1)} %x0.5, ...), custom_call_target="tpu_custom_call" | custom-call | tf_op jit(solution)/shard_map/project/pallas_call | solution.py:102
  114.9 3.1 %collective-permute-start.5 = (bf16[2,1,2,2,64,128]{5,4,3,2,1,0:T(8,128)(2,1)}, bf16[2,1,2,2,64,128]{5,4,3,2,1,0:T(8,128)(2,1)S(1)}, u32[]{:S(2)}, u32[]{:S(2)}) collective-permute-start(bf16[2,1,2,2,64,128]{5,4,3,2,1,0:T(8,128)(2,1)} %get-tuple-element.14), channel_id=1, source_target_pairs={{0,6},{2,0},{4,2},{6,4},{1,7},{3,1},{5,3},{7,5},{8,14},{10,8},{12,... | collective-permute-start | bytes 393224 | tf_op jit(solution)/shard_map/ppermute | solution.py:319
  118.1 2.7 collective-permute-start.6
  120.8 3.2 %collective-permute-start.7 = (bf16[2,1,2,2,64,128]{5,4,3,2,1,0:T(8,128)(2,1)}, bf16[2,1,2,2,64,128]{5,4,3,2,1,0:T(8,128)(2,1)S(1)}, u32[]{:S(2)}, u32[]{:S(2)}) collective-permute-start(bf16[2,1,2,2,64,128]{5,4,3,2,1,0:T(8,128)(2,1)} %get-tuple-element.16), channel_id=1, source_target_pairs={{0,4},{2,6},{4,0},{6,2},{1,5},{3,7},{5,1},{7,3},{8,12},{10,14},{12... | collective-permute-start | bytes 393224 | tf_op jit(solution)/shard_map/ppermute | solution.py:319
  126.4 3.0 %collective-permute-done.7 = bf16[2,1,2,2,64,128]{5,4,3,2,1,0:T(8,128)(2,1)S(1)} collective-permute-done((bf16[2,1,2,2,64,128]{5,4,3,2,1,0:T(8,128)(2,1)}, bf16[2,1,2,2,64,128]{5,4,3,2,1,0:T(8,128)(2,1)S(1)}, u32[]{:S(2)}, u32[]{:S(2)}) %collective-permute-start.7) | collective-permute-done | bytes 131104 | tf_op jit(solution)/shard_map/ppermute | solution.py:319
  129.4 4.8 %collective-permute-start.23 = (bf16[4,256,512]{2,1,0:T(8,128)(2,1)S(1)}, bf16[4,256,512]{2,1,0:T(8,128)(2,1)S(1)}, u32[]{:S(2)}, u32[]{:S(2)}) collective-permute-start(bf16[4,256,512]{2,1,0:T(8,128)(2,1)S(1)} %fusion.refs_0_), channel_id=1, source_target_pairs={{0,6},{2,0},{4,2},{6,4},{1,7},{3,1},{5,3},{7,5},{8,14},{10,8},{12,... | collective-permute-start | bytes 3145736 | tf_op jit(solution)/shard_map/ppermute | solution.py:41
  134.2 1.9 collective-permute-start.22
  136.9 28.9 %all-gather = f32[65536]{0:T(1024)} all-gather(f32[8192]{0:T(1024)S(1)} %bitcast.33), channel_id=2, replica_groups=mesh['sp'=16,'fs'=4,'tp_0'=4,'tp_1'=2] {'tp_0','tp_1'}, dimensions={0}, use_global_device_ids=true | all-gather | bytes 294912 | tf_op jit(solution)/shard_map/all_gather | solution.py:327
  170.8 1.9 collective-permute-start.10
  172.7 3.9 %collective-permute-start.9 = (bf16[16,2,64,128]{3,2,1,0:T(8,128)(2,1)}, bf16[16,2,64,128]{3,2,1,0:T(8,128)(2,1)}, u32[]{:S(2)}, u32[]{:S(2)}) collective-permute-start(bf16[16,2,64,128]{3,2,1,0:T(8,128)(2,1)} %all-to-all-done.2.refs_0_), channel_id=1, source_target_pairs={{0,2},{2,4},{4,6},{6,0},{1,3},{3,5},{5,7},{7,1},{8,10},{10,12},{12... | collective-permute-start | bytes 1572872 | tf_op jit(solution)/shard_map/ppermute | solution.py:40
  177.5 11.7 %all-to-all-start.3 = ((bf16[16,64,128]{2,1,0:T(8,128)(2,1)}), bf16[16,64,128]{2,1,0:T(8,128)(2,1)}, u32[]{:S(2)}, u32[]{:S(2)}) async-start(bf16[16,64,128]{2,1,0:T(8,128)(2,1)} %bitcast.31), calls=%async_computation.3 | async-start | bytes 524288 | tf_op jit(solution)/shard_map/all_to_all | solution.py:335
  189.9 2.0 collective-permute-start.8
  193.5 3.4 %collective-permute-start.12 = (bf16[8,2,64,128]{3,2,1,0:T(8,128)(2,1)}, bf16[8,2,64,128]{3,2,1,0:T(8,128)(2,1)}, u32[]{:S(2)}, u32[]{:S(2)}) collective-permute-start(bf16[8,2,64,128]{3,2,1,0:T(8,128)(2,1)} %slice.50), channel_id=1, source_target_pairs={{0,6},{2,0},{4,2},{6,4},{1,7},{3,1},{5,3},{7,5},{8,14},{10,8},{12,... | collective-permute-start | bytes 786440 | tf_op jit(solution)/shard_map/ppermute | solution.py:44
  198.6 2.4 collective-permute-start.11
  201.1 3.8 %collective-permute-start.13 = (bf16[16,2,64,128]{3,2,1,0:T(8,128)(2,1)}, bf16[16,2,64,128]{3,2,1,0:T(8,128)(2,1)}, u32[]{:S(2)}, u32[]{:S(2)}) collective-permute-start(bf16[16,2,64,128]{3,2,1,0:T(8,128)(2,1)} %all-to-all-done.2.refs_0_), channel_id=1, source_target_pairs={{0,1},{1,0},{2,3},{3,2},{4,5},{5,4},{6,7},{7,6},{8,9},{9,8},{10,11... | collective-permute-start | bytes 1572872 | tf_op jit(solution)/shard_map/ppermute | solution.py:34
  204.9 1.9 collective-permute-start.15
  206.9 2.4 collective-permute-start.14
  209.4 1.9 collective-permute-start.17
  211.3 2.4 collective-permute-start.16
  217.3 1.9 collective-permute-start.26
  219.2 4.9 %collective-permute-start.25 = (bf16[2,256,512]{2,1,0:T(8,128)(2,1)}, bf16[2,256,512]{2,1,0:T(8,128)(2,1)}, u32[]{:S(2)}, u32[]{:S(2)}) collective-permute-start(bf16[2,256,512]{2,1,0:T(8,128)(2,1)} %slice.54), channel_id=1, source_target_pairs={{0,6},{2,0},{4,2},{6,4},{1,7},{3,1},{5,3},{7,5},{8,14},{10,8},{12,... | collective-permute-start | bytes 1572872 | tf_op jit(solution)/shard_map/ppermute | solution.py:44
  224.1 1.9 collective-permute-start.24
  226.0 2.1 collective-permute-start.28
  228.2 2.4 collective-permute-start.27
  231.9 20.2 %attend.1 = bf16[16,64,128]{2,1,0:T(8,128)(2,1)} custom-call(bf16[16,64,128]{2,1,0:T(8,128)(2,1)} %all-to-all-done.3.q_ref, bf16[16,2,64,128]{3,2,1,0:T(8,128)(2,1)} %all-to-all-done.2.refs_0_, bf16[16,2,64,128]{3,2,1,0:T(8,128)(2,1)} %collective-permute-done.9.refs_1_, bf16[16,2,64,128]{3,2,1,0:T(8,128)(2,1)} %collective-permute-done.10.refs_2_, ...), custom_call_target="tpu_custom_call" | custom-call | tf_op jit(solution)/shard_map/attend/pallas_call | solution.py:172
  252.2 12.4 %all-to-all-start.4 = ((bf16[16,64,128]{2,1,0:T(8,128)(2,1)}), bf16[16,64,128]{2,1,0:T(8,128)(2,1)S(1)}, u32[]{:S(2)}, u32[]{:S(2)}) async-start(bf16[16,64,128]{2,1,0:T(8,128)(2,1)} %attend.1), calls=%async_computation.4 | async-start | bytes 524288 | tf_op jit(solution)/shard_map/all_to_all | solution.py:362
  264.6 1.9 collective-permute-start.30
  266.5 2.4 collective-permute-start.29
  268.9 2.2 pool.1.pool_ref
  271.1 11.7 %all-to-all-done.4 = bf16[16,64,128]{2,1,0:T(8,128)(2,1)S(1)} async-done(((bf16[16,64,128]{2,1,0:T(8,128)(2,1)}), bf16[16,64,128]{2,1,0:T(8,128)(2,1)S(1)}, u32[]{:S(2)}, u32[]{:S(2)}) %all-to-all-start.4) | async-done | bytes 262176 | tf_op jit(solution)/shard_map/all_to_all | solution.py:362
  283.5 6.0 %finish.1 = bf16[2,64,2048]{2,1,0:T(8,128)(2,1)} custom-call(s32[5]{0:T(128)} %stack.23.p_ref, bf16[4,2,2,64,128]{4,3,2,1,0:T(8,128)(2,1)} %pool.1.pool_ref, bf16[4,2,2,64,128]{4,3,2,1,0:T(8,128)(2,1)} %bitcast.30, bf16[4,256,512]{2,1,0:T(8,128)(2,1)} %copy-done.5, bf16[4,256,512]{2,1,0:T(8,128)(2,1)} %copy-done.8, bf16[4,256,512]{2,1,0:T(8,128)(2,1)} %copy-done.7, ...), custom_call_target="tpu_custom_call" | custom-call | tf_op jit(solution)/shard_map/finish/pallas_call | solution.py:251
  (101 shorter events, 25.3 us)
Async XLA Ops:
  0.0 104.5 %copy-start = (f32[2,1,8192]{2,1,0:T(1,128)S(1)}, f32[2,1,8192]{2,1,0:T(1,128)}, u32[]{:S(2)}) copy-start(f32[2,1,8192]{2,1,0:T(1,128)} %param.19) | copy-start | bytes 196612
  2.2 32.7 %copy-start.4 = (bf16[2,64,2048]{2,1,0:T(8,128)(2,1)S(1)}, bf16[2,64,2048]{2,1,0:T(8,128)(2,1)}, u32[]{:S(2)}) copy-start(bf16[2,64,2048]{2,1,0:T(8,128)(2,1)} %x0.5) | copy-start | bytes 1572868
  33.0 39.3 %copy-start.1 = (bf16[4,512,512]{2,1,0:T(8,128)(2,1)}, bf16[4,512,512]{2,1,0:T(8,128)(2,1)S(1)}, u32[]{:S(2)}) copy-start(bf16[4,512,512]{2,1,0:T(8,128)(2,1)S(1)} %all_to_all.25) | copy-start | bytes 6291460
  33.0 39.3 %collective-permute-start.4 = (bf16[2048,512]{1,0:T(8,128)(2,1)S(1)}, bf16[2048,512]{1,0:T(8,128)(2,1)}, u32[]{:S(2)}, u32[]{:S(2)}) collective-permute-start(bf16[2048,512]{1,0:T(8,128)(2,1)S(1)} %bitcast.27), channel_id=1, source_target_pairs={{0,1},{1,0},{2,3},{3,2},{4,5},{5,4},{6,7},{7,6},{8,9},{9,8},{10,11... | collective-permute-start | bytes 6291464 | tf_op jit(solution)/shard_map/ppermute | solution.py:34
  34.9 16.5 %collective-permute-start.1 = (bf16[2,64,2048]{2,1,0:T(8,128)(2,1)S(1)}, bf16[2,64,2048]{2,1,0:T(8,128)(2,1)S(1)}, u32[]{:S(2)}, u32[]{:S(2)}) collective-permute-start(bf16[2,64,2048]{2,1,0:T(8,128)(2,1)S(1)} %copy-done.4), channel_id=1, source_target_pairs={{0,6},{2,0},{4,2},{6,4},{1,7},{3,1},{5,3},{7,5},{8,14},{10,8},{12,... | collective-permute-start | bytes 1572872 | tf_op jit(solution)/shard_map/ppermute | solution.py:41
  39.6 18.2 %collective-permute-start = (bf16[2,64,2048]{2,1,0:T(8,128)(2,1)S(1)}, bf16[2,64,2048]{2,1,0:T(8,128)(2,1)S(1)}, u32[]{:S(2)}, u32[]{:S(2)}) collective-permute-start(bf16[2,64,2048]{2,1,0:T(8,128)(2,1)S(1)} %copy-done.4), channel_id=1, source_target_pairs={{0,2},{2,4},{4,6},{6,0},{1,3},{3,5},{5,7},{7,1},{8,10},{10,12},{12... | collective-permute-start | bytes 1572872 | tf_op jit(solution)/shard_map/ppermute | solution.py:40
  51.4 18.1 %copy-start.2 = (bf16[2,64,2048]{2,1,0:T(8,128)(2,1)}, bf16[2,64,2048]{2,1,0:T(8,128)(2,1)S(1)}, u32[]{:S(2)}) copy-start(bf16[2,64,2048]{2,1,0:T(8,128)(2,1)S(1)} %collective-permute-done.1.x2) | copy-start | bytes 1572868
  52.2 11.3 %collective-permute-start.3 = (bf16[1,64,2048]{2,1,0:T(8,128)(2,1)}, bf16[1,64,2048]{2,1,0:T(8,128)(2,1)S(1)}, u32[]{:S(2)}, u32[]{:S(2)}) collective-permute-start(bf16[1,64,2048]{2,1,0:T(8,128)(2,1)} %slice.45), channel_id=1, source_target_pairs={{0,6},{2,0},{4,2},{6,4},{1,7},{3,1},{5,3},{7,5},{8,14},{10,8},{12,... | collective-permute-start | bytes 786440 | tf_op jit(solution)/shard_map/ppermute | solution.py:44
  57.8 11.7 %copy-start.3 = (bf16[2,64,2048]{2,1,0:T(8,128)(2,1)}, bf16[2,64,2048]{2,1,0:T(8,128)(2,1)S(1)}, u32[]{:S(2)}) copy-start(bf16[2,64,2048]{2,1,0:T(8,128)(2,1)S(1)} %collective-permute-done.x1) | copy-start | bytes 1572868
  58.6 11.0 %collective-permute-start.2 = (bf16[1,64,2048]{2,1,0:T(8,128)(2,1)}, bf16[1,64,2048]{2,1,0:T(8,128)(2,1)}, u32[]{:S(2)}, u32[]{:S(2)}) collective-permute-start(bf16[1,64,2048]{2,1,0:T(8,128)(2,1)} %slice.44), channel_id=1, source_target_pairs={{0,2},{2,4},{4,6},{6,0},{1,3},{3,5},{5,7},{7,1},{8,10},{10,12},{12... | collective-permute-start | bytes 786440 | tf_op jit(solution)/shard_map/ppermute | solution.py:43
  63.4 6.1 %copy-start.6 = (bf16[1,64,2048]{2,1,0:T(8,128)(2,1)}, bf16[1,64,2048]{2,1,0:T(8,128)(2,1)S(1)}, u32[]{:S(2)}) copy-start(bf16[1,64,2048]{2,1,0:T(8,128)(2,1)S(1)} %collective-permute-done.3.x4) | copy-start | bytes 786436
  72.2 8.6 %copy-start.11 = (bf16[128,512]{1,0:T(8,128)(2,1)S(1)}, bf16[128,512]{1,0:T(8,128)(2,1)}, u32[]{:S(2)}) copy-start(bf16[128,512]{1,0:T(8,128)(2,1)} %param.21) | copy-start | bytes 393220
  72.2 8.6 %copy-start.12 = (bf16[128,512]{1,0:T(8,128)(2,1)S(1)}, bf16[128,512]{1,0:T(8,128)(2,1)}, u32[]{:S(2)}) copy-start(bf16[128,512]{1,0:T(8,128)(2,1)} %param.20) | copy-start | bytes 393220
  76.7 12.6 %all-to-all-start.1 = ((bf16[4,2,2,2,64,128]{5,4,3,2,1,0:T(8,128)(2,1)}), bf16[4,2,2,2,64,128]{5,4,3,2,1,0:T(8,128)(2,1)}, u32[]{:S(2)}, u32[]{:S(2)}) async-start(bf16[4,2,2,2,64,128]{5,4,3,2,1,0:T(8,128)(2,1)} %project.3), calls=%async_computation.1 | async-start | bytes 1048576 | tf_op jit(solution)/shard_map/all_to_all | solution.py:309
  80.9 23.9 %collective-permute-start.19 = (bf16[256,512]{1,0:T(8,128)(2,1)S(1)}, bf16[256,512]{1,0:T(8,128)(2,1)S(1)}, u32[]{:S(2)}, u32[]{:S(2)}) collective-permute-start(bf16[256,512]{1,0:T(8,128)(2,1)S(1)} %pad_maximum_fusion), channel_id=1, source_target_pairs={{0,24},{8,0},{16,8},{24,16},{1,25},{9,1},{17,9},{25,17},{2,26},{10... | collective-permute-start | bytes 786440 | tf_op jit(solution)/shard_map/ppermute | solution.py:41
  84.0 23.9 %collective-permute-start.18 = (bf16[256,512]{1,0:T(8,128)(2,1)S(1)}, bf16[256,512]{1,0:T(8,128)(2,1)S(1)}, u32[]{:S(2)}, u32[]{:S(2)}) collective-permute-start(bf16[256,512]{1,0:T(8,128)(2,1)S(1)} %pad_maximum_fusion), channel_id=1, source_target_pairs={{0,8},{8,16},{16,24},{24,0},{1,9},{9,17},{17,25},{25,1},{2,10},{10... | collective-permute-start | bytes 786440 | tf_op jit(solution)/shard_map/ppermute | solution.py:40
  89.3 81.5 %all-to-all-start.2 = ((bf16[16,2,64,128]{3,2,1,0:T(8,128)(2,1)}), bf16[16,2,64,128]{3,2,1,0:T(8,128)(2,1)}, u32[]{:S(2)}, u32[]{:S(2)}) async-start(bf16[16,2,64,128]{3,2,1,0:T(8,128)(2,1)} %bitcast.10), calls=%async_computation.2 | async-start | bytes 1048576 | tf_op jit(solution)/shard_map/all_to_all | solution.py:310
  104.8 13.3 %collective-permute-start.21 = (bf16[128,512]{1,0:T(8,128)(2,1)S(1)}, bf16[128,512]{1,0:T(8,128)(2,1)S(1)}, u32[]{:S(2)}, u32[]{:S(2)}) collective-permute-start(bf16[128,512]{1,0:T(8,128)(2,1)S(1)} %slice.52), channel_id=1, source_target_pairs={{0,24},{8,0},{16,8},{24,16},{1,25},{9,1},{17,9},{25,17},{2,26},{10... | collective-permute-start | bytes 393224 | tf_op jit(solution)/shard_map/ppermute | solution.py:44
  107.9 10.2 %collective-permute-start.20 = (bf16[128,512]{1,0:T(8,128)(2,1)S(1)}, bf16[128,512]{1,0:T(8,128)(2,1)S(1)}, u32[]{:S(2)}, u32[]{:S(2)}) collective-permute-start(bf16[128,512]{1,0:T(8,128)(2,1)S(1)} %slice.51), channel_id=1, source_target_pairs={{0,8},{8,16},{16,24},{24,0},{1,9},{9,17},{17,25},{25,1},{2,10},{10... | collective-permute-start | bytes 393224 | tf_op jit(solution)/shard_map/ppermute | solution.py:43
  114.9 10.1 %collective-permute-start.5 = (bf16[2,1,2,2,64,128]{5,4,3,2,1,0:T(8,128)(2,1)}, bf16[2,1,2,2,64,128]{5,4,3,2,1,0:T(8,128)(2,1)S(1)}, u32[]{:S(2)}, u32[]{:S(2)}) collective-permute-start(bf16[2,1,2,2,64,128]{5,4,3,2,1,0:T(8,128)(2,1)} %get-tuple-element.14), channel_id=1, source_target_pairs={{0,6},{2,0},{4,2},{6,4},{1,7},{3,1},{5,3},{7,5},{8,14},{10,8},{12,... | collective-permute-start | bytes 393224 | tf_op jit(solution)/shard_map/ppermute | solution.py:319
  118.1 99.2 %copy-start.5 = (bf16[4,256,512]{2,1,0:T(8,128)(2,1)}, bf16[4,256,512]{2,1,0:T(8,128)(2,1)S(1)}, u32[]{:S(2)}) copy-start(bf16[4,256,512]{2,1,0:T(8,128)(2,1)S(1)} %fusion.refs_0_) | copy-start | bytes 3145732
  118.1 8.3 %collective-permute-start.6 = (bf16[2,1,2,2,64,128]{5,4,3,2,1,0:T(8,128)(2,1)}, bf16[2,1,2,2,64,128]{5,4,3,2,1,0:T(8,128)(2,1)S(1)}, u32[]{:S(2)}, u32[]{:S(2)}) collective-permute-start(bf16[2,1,2,2,64,128]{5,4,3,2,1,0:T(8,128)(2,1)} %get-tuple-element.15), channel_id=1, source_target_pairs={{0,2},{2,4},{4,6},{6,0},{1,3},{3,5},{5,7},{7,1},{8,10},{10,12},{12... | collective-permute-start | bytes 393224 | tf_op jit(solution)/shard_map/ppermute | solution.py:319
  120.8 8.6 %collective-permute-start.7 = (bf16[2,1,2,2,64,128]{5,4,3,2,1,0:T(8,128)(2,1)}, bf16[2,1,2,2,64,128]{5,4,3,2,1,0:T(8,128)(2,1)S(1)}, u32[]{:S(2)}, u32[]{:S(2)}) collective-permute-start(bf16[2,1,2,2,64,128]{5,4,3,2,1,0:T(8,128)(2,1)} %get-tuple-element.16), channel_id=1, source_target_pairs={{0,4},{2,6},{4,0},{6,2},{1,5},{3,7},{5,1},{7,3},{8,12},{10,14},{12... | collective-permute-start | bytes 393224 | tf_op jit(solution)/shard_map/ppermute | solution.py:319
  129.4 75.5 %collective-permute-start.23 = (bf16[4,256,512]{2,1,0:T(8,128)(2,1)S(1)}, bf16[4,256,512]{2,1,0:T(8,128)(2,1)S(1)}, u32[]{:S(2)}, u32[]{:S(2)}) collective-permute-start(bf16[4,256,512]{2,1,0:T(8,128)(2,1)S(1)} %fusion.refs_0_), channel_id=1, source_target_pairs={{0,6},{2,0},{4,2},{6,4},{1,7},{3,1},{5,3},{7,5},{8,14},{10,8},{12,... | collective-permute-start | bytes 3145736 | tf_op jit(solution)/shard_map/ppermute | solution.py:41
  134.2 72.6 %collective-permute-start.22 = (bf16[4,256,512]{2,1,0:T(8,128)(2,1)S(1)}, bf16[4,256,512]{2,1,0:T(8,128)(2,1)S(1)}, u32[]{:S(2)}, u32[]{:S(2)}) collective-permute-start(bf16[4,256,512]{2,1,0:T(8,128)(2,1)S(1)} %fusion.refs_0_), channel_id=1, source_target_pairs={{0,2},{2,4},{4,6},{6,0},{1,3},{3,5},{5,7},{7,1},{8,10},{10,12},{12... | collective-permute-start | bytes 3145736 | tf_op jit(solution)/shard_map/ppermute | solution.py:40
  136.9 79.5 %copy-start.9 = (bf16[4,2,2,64,128]{4,3,2,1,0:T(8,128)(2,1)}, bf16[4,2,2,64,128]{4,3,2,1,0:T(8,128)(2,1)S(1)}, u32[]{:S(2)}) copy-start(bf16[4,2,2,64,128]{4,3,2,1,0:T(8,128)(2,1)S(1)} %get-tuple-element.22.in_ref) | copy-start | bytes 786436
  170.8 21.1 %collective-permute-start.10 = (bf16[16,2,64,128]{3,2,1,0:T(8,128)(2,1)}, bf16[16,2,64,128]{3,2,1,0:T(8,128)(2,1)}, u32[]{:S(2)}, u32[]{:S(2)}) collective-permute-start(bf16[16,2,64,128]{3,2,1,0:T(8,128)(2,1)} %all-to-all-done.2.refs_0_), channel_id=1, source_target_pairs={{0,6},{2,0},{4,2},{6,4},{1,7},{3,1},{5,3},{7,5},{8,14},{10,8},{12,... | collective-permute-start | bytes 1572872 | tf_op jit(solution)/shard_map/ppermute | solution.py:41
  172.7 24.2 %collective-permute-start.9 = (bf16[16,2,64,128]{3,2,1,0:T(8,128)(2,1)}, bf16[16,2,64,128]{3,2,1,0:T(8,128)(2,1)}, u32[]{:S(2)}, u32[]{:S(2)}) collective-permute-start(bf16[16,2,64,128]{3,2,1,0:T(8,128)(2,1)} %all-to-all-done.2.refs_0_), channel_id=1, source_target_pairs={{0,2},{2,4},{4,6},{6,0},{1,3},{3,5},{5,7},{7,1},{8,10},{10,12},{12... | collective-permute-start | bytes 1572872 | tf_op jit(solution)/shard_map/ppermute | solution.py:40
  177.5 54.4 %all-to-all-start.3 = ((bf16[16,64,128]{2,1,0:T(8,128)(2,1)}), bf16[16,64,128]{2,1,0:T(8,128)(2,1)}, u32[]{:S(2)}, u32[]{:S(2)}) async-start(bf16[16,64,128]{2,1,0:T(8,128)(2,1)} %bitcast.31), calls=%async_computation.3 | async-start | bytes 524288 | tf_op jit(solution)/shard_map/all_to_all | solution.py:335
  189.9 11.2 %collective-permute-start.8 = (bf16[4,2,2,16,128]{4,3,2,1,0:T(8,128)(2,1)}, bf16[4,2,2,16,128]{4,3,2,1,0:T(8,128)(2,1)S(1)}, u32[]{:S(2)}, u32[]{:S(2)}) collective-permute-start(bf16[4,2,2,16,128]{4,3,2,1,0:T(8,128)(2,1)} %slice.47), channel_id=1, source_target_pairs={{0,1},{1,2},{2,3},{3,4},{4,5},{5,6},{6,7},{7,32},{32,33},{33,34},{... | collective-permute-start | bytes 196616 | tf_op jit(solution)/shard_map/ppermute | solution.py:338
  193.5 15.8 %collective-permute-start.12 = (bf16[8,2,64,128]{3,2,1,0:T(8,128)(2,1)}, bf16[8,2,64,128]{3,2,1,0:T(8,128)(2,1)}, u32[]{:S(2)}, u32[]{:S(2)}) collective-permute-start(bf16[8,2,64,128]{3,2,1,0:T(8,128)(2,1)} %slice.50), channel_id=1, source_target_pairs={{0,6},{2,0},{4,2},{6,4},{1,7},{3,1},{5,3},{7,5},{8,14},{10,8},{12,... | collective-permute-start | bytes 786440 | tf_op jit(solution)/shard_map/ppermute | solution.py:44
  198.6 12.7 %collective-permute-start.11 = (bf16[8,2,64,128]{3,2,1,0:T(8,128)(2,1)}, bf16[8,2,64,128]{3,2,1,0:T(8,128)(2,1)}, u32[]{:S(2)}, u32[]{:S(2)}) collective-permute-start(bf16[8,2,64,128]{3,2,1,0:T(8,128)(2,1)} %slice.49), channel_id=1, source_target_pairs={{0,2},{2,4},{4,6},{6,0},{1,3},{3,5},{5,7},{7,1},{8,10},{10,12},{12... | collective-permute-start | bytes 786440 | tf_op jit(solution)/shard_map/ppermute | solution.py:43
  201.1 51.1 %copy-start.13 = (bf16[4,2,2,16,128]{4,3,2,1,0:T(8,128)(2,1)}, bf16[4,2,2,16,128]{4,3,2,1,0:T(8,128)(2,1)S(1)}, u32[]{:S(2)}) copy-start(bf16[4,2,2,16,128]{4,3,2,1,0:T(8,128)(2,1)S(1)} %collective-permute-done.8.edge_ref) | copy-start | bytes 196612
  201.1 16.2 %collective-permute-start.13 = (bf16[16,2,64,128]{3,2,1,0:T(8,128)(2,1)}, bf16[16,2,64,128]{3,2,1,0:T(8,128)(2,1)}, u32[]{:S(2)}, u32[]{:S(2)}) collective-permute-start(bf16[16,2,64,128]{3,2,1,0:T(8,128)(2,1)} %all-to-all-done.2.refs_0_), channel_id=1, source_target_pairs={{0,1},{1,0},{2,3},{3,2},{4,5},{5,4},{6,7},{7,6},{8,9},{9,8},{10,11... | collective-permute-start | bytes 1572872 | tf_op jit(solution)/shard_map/ppermute | solution.py:34
  204.9 47.2 %copy-start.7 = (bf16[4,256,512]{2,1,0:T(8,128)(2,1)}, bf16[4,256,512]{2,1,0:T(8,128)(2,1)S(1)}, u32[]{:S(2)}) copy-start(bf16[4,256,512]{2,1,0:T(8,128)(2,1)S(1)} %collective-permute-done.23.refs_2_) | copy-start | bytes 3145732
  204.9 19.1 %collective-permute-start.15 = (bf16[16,2,64,128]{3,2,1,0:T(8,128)(2,1)}, bf16[16,2,64,128]{3,2,1,0:T(8,128)(2,1)}, u32[]{:S(2)}, u32[]{:S(2)}) collective-permute-start(bf16[16,2,64,128]{3,2,1,0:T(8,128)(2,1)} %collective-permute-done.10.refs_2_), channel_id=1, source_target_pairs={{0,1},{1,0},{2,3},{3,2},{4,5},{5,4},{6,7},{7,6},{8,9},{9,8},{10,11... | collective-permute-start | bytes 1572872 | tf_op jit(solution)/shard_map/ppermute | solution.py:34
  206.9 45.3 %copy-start.8 = (bf16[4,256,512]{2,1,0:T(8,128)(2,1)}, bf16[4,256,512]{2,1,0:T(8,128)(2,1)S(1)}, u32[]{:S(2)}) copy-start(bf16[4,256,512]{2,1,0:T(8,128)(2,1)S(1)} %collective-permute-done.22.refs_1_) | copy-start | bytes 3145732
  206.9 21.3 %collective-permute-start.14 = (bf16[16,2,64,128]{3,2,1,0:T(8,128)(2,1)}, bf16[16,2,64,128]{3,2,1,0:T(8,128)(2,1)}, u32[]{:S(2)}, u32[]{:S(2)}) collective-permute-start(bf16[16,2,64,128]{3,2,1,0:T(8,128)(2,1)} %collective-permute-done.9.refs_1_), channel_id=1, source_target_pairs={{0,1},{1,0},{2,3},{3,2},{4,5},{5,4},{6,7},{7,6},{8,9},{9,8},{10,11... | collective-permute-start | bytes 1572872 | tf_op jit(solution)/shard_map/ppermute | solution.py:34
  209.4 9.8 %collective-permute-start.17 = (bf16[8,2,64,128]{3,2,1,0:T(8,128)(2,1)}, bf16[8,2,64,128]{3,2,1,0:T(8,128)(2,1)}, u32[]{:S(2)}, u32[]{:S(2)}) collective-permute-start(bf16[8,2,64,128]{3,2,1,0:T(8,128)(2,1)} %collective-permute-done.12.refs_4_), channel_id=1, source_target_pairs={{0,1},{1,0},{2,3},{3,2},{4,5},{5,4},{6,7},{7,6},{8,9},{9,8},{10,11... | collective-permute-start | bytes 786440 | tf_op jit(solution)/shard_map/ppermute | solution.py:34
  211.3 14.7 %collective-permute-start.16 = (bf16[8,2,64,128]{3,2,1,0:T(8,128)(2,1)}, bf16[8,2,64,128]{3,2,1,0:T(8,128)(2,1)}, u32[]{:S(2)}, u32[]{:S(2)}) collective-permute-start(bf16[8,2,64,128]{3,2,1,0:T(8,128)(2,1)} %collective-permute-done.11.refs_3_), channel_id=1, source_target_pairs={{0,1},{1,0},{2,3},{3,2},{4,5},{5,4},{6,7},{7,6},{8,9},{9,8},{10,11... | collective-permute-start | bytes 786440 | tf_op jit(solution)/shard_map/ppermute | solution.py:34
  217.3 53.8 %collective-permute-start.26 = (bf16[4,256,512]{2,1,0:T(8,128)(2,1)S(1)}, bf16[4,256,512]{2,1,0:T(8,128)(2,1)}, u32[]{:S(2)}, u32[]{:S(2)}) collective-permute-start(bf16[4,256,512]{2,1,0:T(8,128)(2,1)S(1)} %fusion.refs_0_), channel_id=1, source_target_pairs={{0,1},{1,0},{2,3},{3,2},{4,5},{5,4},{6,7},{7,6},{8,9},{9,8},{10,11... | collective-permute-start | bytes 3145736 | tf_op jit(solution)/shard_map/ppermute | solution.py:34
  219.2 45.4 %collective-permute-start.25 = (bf16[2,256,512]{2,1,0:T(8,128)(2,1)}, bf16[2,256,512]{2,1,0:T(8,128)(2,1)}, u32[]{:S(2)}, u32[]{:S(2)}) collective-permute-start(bf16[2,256,512]{2,1,0:T(8,128)(2,1)} %slice.54), channel_id=1, source_target_pairs={{0,6},{2,0},{4,2},{6,4},{1,7},{3,1},{5,3},{7,5},{8,14},{10,8},{12,... | collective-permute-start | bytes 1572872 | tf_op jit(solution)/shard_map/ppermute | solution.py:44
  224.1 42.4 %collective-permute-start.24 = (bf16[2,256,512]{2,1,0:T(8,128)(2,1)}, bf16[2,256,512]{2,1,0:T(8,128)(2,1)}, u32[]{:S(2)}, u32[]{:S(2)}) collective-permute-start(bf16[2,256,512]{2,1,0:T(8,128)(2,1)} %slice.53), channel_id=1, source_target_pairs={{0,2},{2,4},{4,6},{6,0},{1,3},{3,5},{5,7},{7,1},{8,10},{10,12},{12... | collective-permute-start | bytes 1572872 | tf_op jit(solution)/shard_map/ppermute | solution.py:43
  226.0 45.1 %collective-permute-start.28 = (bf16[4,256,512]{2,1,0:T(8,128)(2,1)S(1)}, bf16[4,256,512]{2,1,0:T(8,128)(2,1)}, u32[]{:S(2)}, u32[]{:S(2)}) collective-permute-start(bf16[4,256,512]{2,1,0:T(8,128)(2,1)S(1)} %collective-permute-done.23.refs_2_), channel_id=1, source_target_pairs={{0,1},{1,0},{2,3},{3,2},{4,5},{5,4},{6,7},{7,6},{8,9},{9,8},{10,11... | collective-permute-start | bytes 3145736 | tf_op jit(solution)/shard_map/ppermute | solution.py:34
  228.2 43.0 %collective-permute-start.27 = (bf16[4,256,512]{2,1,0:T(8,128)(2,1)S(1)}, bf16[4,256,512]{2,1,0:T(8,128)(2,1)}, u32[]{:S(2)}, u32[]{:S(2)}) collective-permute-start(bf16[4,256,512]{2,1,0:T(8,128)(2,1)S(1)} %collective-permute-done.22.refs_1_), channel_id=1, source_target_pairs={{0,1},{1,0},{2,3},{3,2},{4,5},{5,4},{6,7},{7,6},{8,9},{9,8},{10,11... | collective-permute-start | bytes 3145736 | tf_op jit(solution)/shard_map/ppermute | solution.py:34
  252.2 30.7 %all-to-all-start.4 = ((bf16[16,64,128]{2,1,0:T(8,128)(2,1)}), bf16[16,64,128]{2,1,0:T(8,128)(2,1)S(1)}, u32[]{:S(2)}, u32[]{:S(2)}) async-start(bf16[16,64,128]{2,1,0:T(8,128)(2,1)} %attend.1), calls=%async_computation.4 | async-start | bytes 524288 | tf_op jit(solution)/shard_map/all_to_all | solution.py:362
  264.6 6.5 %collective-permute-start.30 = (bf16[2,256,512]{2,1,0:T(8,128)(2,1)}, bf16[2,256,512]{2,1,0:T(8,128)(2,1)}, u32[]{:S(2)}, u32[]{:S(2)}) collective-permute-start(bf16[2,256,512]{2,1,0:T(8,128)(2,1)} %collective-permute-done.25.refs_4_), channel_id=1, source_target_pairs={{0,1},{1,0},{2,3},{3,2},{4,5},{5,4},{6,7},{7,6},{8,9},{9,8},{10,11... | collective-permute-start | bytes 1572872 | tf_op jit(solution)/shard_map/ppermute | solution.py:34
  266.5 4.6 %collective-permute-start.29 = (bf16[2,256,512]{2,1,0:T(8,128)(2,1)}, bf16[2,256,512]{2,1,0:T(8,128)(2,1)}, u32[]{:S(2)}, u32[]{:S(2)}) collective-permute-start(bf16[2,256,512]{2,1,0:T(8,128)(2,1)} %collective-permute-done.24.refs_3_), channel_id=1, source_target_pairs={{0,1},{1,0},{2,3},{3,2},{4,5},{5,4},{6,7},{7,6},{8,9},{9,8},{10,11... | collective-permute-start | bytes 1572872 | tf_op jit(solution)/shard_map/ppermute | solution.py:34
  (1 other events, 0.7 us)

commit v2 on v1

--- a/solution.py
+++ b/solution.py
@@ -11,6 +11,7 @@
 SP_TP = ("sp", "tp_0", "tp_1")
 EPS = 1e-06
 MASKED = -1e30
+GATE_ROWS = 16
 LOG2E = 1.4426950408889634
 F32 = jnp.float32
 BF16 = jnp.bfloat16
@@ -34,15 +35,22 @@
     return lax.ppermute(x, "tp_1", [(0, 1), (1, 0)])
 
 
+UP = [(i, (i + 1) % 4) for i in range(4)]
+DOWN = [(i, (i - 1) % 4) for i in range(4)]
+
+
+def hops(x, axis):
+    return lax.ppermute(x, axis, UP), lax.ppermute(x, axis, DOWN)
+
+
+def relays(before, after, axis):
+    half = before.shape[0] // 2
+    return lax.ppermute(before[:half], axis, UP), lax.ppermute(after[half:], axis, DOWN)
+
+
 def ring_of_four(x, axis):
-    up = [(i, (i + 1) % 4) for i in range(4)]
-    down = [(i, (i - 1) % 4) for i in range(4)]
-    before = lax.ppermute(x, axis, up)
-    after = lax.ppermute(x, axis, down)
-    half = x.shape[0] // 2
-    far_low = lax.ppermute(before[:half], axis, up)
-    far_high = lax.ppermute(after[half:], axis, down)
-    return x, before, after, far_low, far_high
+    near = hops(x, axis)
+    return (x, *near, *relays(*near, axis))
 
 
 def rms(x):
@@ -71,7 +79,7 @@
 
 
 def project(places, norm, rows_of, own, other, half, factors, split):
-    seqs, rows, depth = rows_of[0].shape
+    seqs, rows, _ = rows_of[0].shape
     kinds = len(factors)
 
     def body(p_ref, norm_ref, x0, x1, x2, x3, x4, own_ref, other_ref, *outs):
@@ -79,8 +87,27 @@
             [x0[0], x0[1], x1[0], x1[1], x2[0], x2[1], x3[0], x4[0]], axis=0
         )
         r = norm_ref[...]
+        lane = lax.broadcasted_iota(jnp.int32, (GATE_ROWS, HD), 1)
+        first_half = (lane < rows) == (p_ref[0] == 0)
         for ref, head in ((own_ref, p_ref[0]), (other_ref, 1 - p_ref[0])):
-            y = jnp.dot(x, ref[...], preferred_element_type=F32) * r
+            w = jnp.concatenate(
+                [ref[b, : ref.shape[1] - GATE_ROWS, cols] for b in range(ref.shape[0])], axis=0
+            )
+            y = jnp.dot(x, w, preferred_element_type=F32) * r
+            if not split:
+                for a in range(4):
+                    to = p_ref[1 + a]
+                    g = ref[
+                        p_ref[5],
+                        ref.shape[1] - GATE_ROWS :,
+                        pl.ds(pl.multiple_of(to * 2 * rows, 2 * rows), 2 * rows),
+                    ].astype(F32)
+                    turned = pltpu.roll(g, rows, 1)
+                    twice = jnp.where(first_half, g, turned).astype(BF16)
+                    for i in range(seqs):
+                        outs[0][to, i, head, 2 * rows :] = (
+                            twice if i == 0 else jnp.roll(twice, -i * 8, 0)
+                        )
             for kind, factor in enumerate(factors):
                 part = y[:, kind * HD : (kind + 1) * HD]
                 if factor != 1.0:
@@ -92,17 +119,18 @@
                         if split:
                             outs[a][kind, 0, i, head] = part[at : at + rows]
                         else:
-                            outs[0][p_ref[1 + a], i, head, kind] = part[at : at + rows]
-
-    w_spec = pl.BlockSpec((depth, kinds * HD), lambda *_: (0, half))
+                            outs[0][p_ref[1 + a], i, head, kind * rows : (kind + 1) * rows] = part[
+                                at : at + rows
+                            ]
+
+    cols = slice(half * kinds * HD, (half + 1) * kinds * HD)
     if split:
         shapes = [(kinds, 1, seqs, 2, rows, HD)] * 4
     else:
-        shapes = [(4, seqs, 2, kinds, rows, HD)]
+        shapes = [(4, seqs, 2, kinds * rows + GATE_ROWS, HD)]
     outs = pl.pallas_call(
         body,
-        grid=(1,),
-        in_specs=[whole(pltpu.SMEM)] + [whole()] * 6 + [w_spec, w_spec],
+        in_specs=[whole(pltpu.SMEM)] + [whole()] * 8,
         out_specs=[whole()] * len(shapes),
         out_shape=[jax.ShapeDtypeStruct(sh, BF16) for sh in shapes],
         compiler_params=params(),
@@ -111,7 +139,7 @@
     return outs
 
 
-def attend(q, own, other, gates, key_place, query_place):
+def attend(q, own, other, key_place, query_place):
     blocks, rows, _ = q.shape
     span = 8 * rows
     group = 4
@@ -119,20 +147,28 @@
     count = blocks // group
 
     def body(q_ref, *refs):
-        kvs, (gate_ref, kp_ref, qp_ref, out_ref, acc_ref, top_ref) = refs[:10], refs[10:]
+        kvs, (kp_ref, qp_ref, out_ref, acc_ref, top_ref) = refs[:7], refs[7:]
         ones = jnp.ones((span, HD), BF16)
-
-        def pieces(s, kind, late):
-            out = []
-            for side in (kvs[:5], kvs[5:]):
-                out += [side[0][s, kind], side[1][s, kind], side[2][s, kind]]
-                out.append(side[4][s - blocks // 2, kind] if late else side[3][s, kind])
-            return jnp.concatenate(out, axis=0)
+        left = lax.broadcasted_iota(jnp.int32, (1, HD), 1) < rows
+
+        def blocks_of(s, late, at):
+            far = kvs[4][s - blocks // 2, at] if late else kvs[3][s, at]
+            return [kvs[0][s, at], kvs[1][s, at], kvs[2][s, at], far, kvs[5][s, at]] + [
+                kvs[6][s + n * blocks, at] for n in range(3)
+            ]
+
+        def gates(s, late):
+            parts = blocks_of(s, late, slice(2 * rows, 2 * rows + GATE_ROWS))
+            parts = [jnp.sum(part.astype(F32)[:3], axis=0, keepdims=True) for part in parts]
+            return LOG2E * jnp.concatenate(
+                [jnp.where(left, parts[n], parts[n + 1]) for n in range(0, 8, 2)], axis=1
+            )
 
         def step(s, first_group, fresh, late):
-            k = pieces(s, 0, late)
-            v = jnp.concatenate([pieces(s, 1, late), ones], axis=1)
-            gate = gate_ref[s]
+            k = jnp.concatenate(blocks_of(s, late, slice(0, rows)), axis=0)
+            v = jnp.concatenate(blocks_of(s, late, slice(rows, 2 * rows)), axis=0)
+            v = jnp.concatenate([v, ones], axis=1)
+            gate = gates(s, late)
             for g in range(first_group, count):
                 at = pl.ds(g * tall, tall)
                 qt = q_ref[g * group : (g + 1) * group].reshape(tall, HD)
@@ -171,7 +207,7 @@
 
     return pl.pallas_call(
         body,
-        in_specs=[whole()] * 14,
+        in_specs=[whole()] * 10,
         out_specs=whole(),
         out_shape=jax.ShapeDtypeStruct(q.shape, BF16),
         scratch_shapes=[
@@ -180,7 +216,7 @@
         ],
         compiler_params=params(),
         name="attend",
-    )(q, *own, *other, gates, key_place, query_place)
+    )(q, *own, *other, key_place, query_place)
 
 
 def pool(first, rows_in, border, mix, scale):
@@ -291,10 +327,10 @@
     c = lax.axis_index("tp_1")
     planes = lax.axis_size("sp")
     chunks = lax.axis_size("tp_0")
-    seqs, rows, depth = tokens.shape
+    seqs, rows, _ = tokens.shape
     block = rows * chunks * 2
     seen = [x, (x + 3) % 4, (x + 1) % 4, (x + 2) % 4]
-    places = jnp.stack([c] + seen).astype(jnp.int32)
+    places = jnp.stack([c] + seen + [y]).astype(jnp.int32)
 
     deep = w_key.shape[0]
     gain = lax.dynamic_slice_in_dim(norm_gain, y * deep, deep, 0)
@@ -302,14 +338,18 @@
     norm = factors_of(all_rows)
     weights = jnp.concatenate([w_key, w_value, w_query, w_pool_in], axis=1)
     weights = (weights.astype(F32) * gain[:, None]).astype(BF16)
-    own_w = spread(weights, "fs").reshape(depth, -1)
+    here = lax.dynamic_slice_in_dim(gate_cache[:, 0], z * block, block, 1)
+    high = lax.reduce_precision(here, 8, 7)
+    rest = here - high
+    middle = lax.reduce_precision(rest, 8, 7)
+    parts = jnp.stack([high, middle, rest - middle], axis=1).astype(BF16)
+    parts = jnp.pad(parts, ((0, 0), (0, 5), (0, 0))).reshape(GATE_ROWS, block)
+    own_w = spread(jnp.concatenate([weights, parts], axis=0), "fs")
     other_w = sibling(own_w)
 
     (kv,) = project(places, norm, all_rows, own_w, other_w, 0, (1.0, 1.0), False)
     kv_here = lax.all_to_all(kv, "tp_0", 0, 0, tiled=True)
-    kv = lax.all_to_all(
-        kv_here.reshape(planes, 2, rows, HD), "sp", 0, 0, tiled=True
-    )
+    kv = lax.all_to_all(kv_here.reshape(planes, 2 * rows + GATE_ROWS, HD), "sp", 0, 0, tiled=True)
     qp = project(
         places, norm, all_rows, own_w, other_w, 1, (HD**-0.5 * LOG2E, 1.0), True
     )
@@ -321,17 +361,7 @@
     came = [x, (x + 1) % 4, (x + 3) % 4, (x + 2) % 4]
     qp = placed(got, came, 1)
 
-    pair_seq = (z // 2) % 2
-    pair_head = 2 * (z // 4) + z % 2
-    gate_rows = lax.dynamic_index_in_dim(gate_cache[:, 0], pair_seq, 0, keepdims=False)
-    gate_all = lax.all_gather(after(gate_rows, kv_here), TP, axis=0, tiled=False)
-    gate = lax.dynamic_index_in_dim(gate_all, pair_head, 0, keepdims=False) * LOG2E
-    gate = gate.reshape(planes, chunks, 2, rows).transpose(0, 2, 1, 3)
-    gate = jnp.where(c == 0, gate, gate[:, ::-1])
-    gate = jnp.concatenate([lax.dynamic_slice_in_dim(gate, at, 1, 2) for at in seen], axis=2)
-    gate = gate.reshape(planes, 1, block)
-
-    q = after(qp[0].reshape(planes, rows, HD), kv, gate)
+    q = after(qp[0].reshape(planes, rows, HD), kv)
     q = lax.all_to_all(q, "sp", 0, 0, tiled=True)
     pool_in = qp[1]
     total = planes * chunks * 2
@@ -342,14 +372,13 @@
     pooled = pool(first, pool_in, border, pool_mix, pool_scale.reshape(-1, HD))
 
     kv_own = ring_of_four(kv, "tp_0")
-    kv_other = [sibling(piece) for piece in kv_own]
+    kv_other = [sibling(kv), sibling(jnp.concatenate(kv_own[1:], axis=0))]
 
     out_w = jnp.concatenate([w_out_pool, w_out_attn], axis=0)
     o = ring_of_four(after(out_w, own_w), "fs")
     o = [o[0], o[1], o[2], jnp.concatenate(o[3:], axis=0)]
     o = placed([w[None] for w in o], [y, (y + 3) % 4, (y + 1) % 4, (y + 2) % 4], 0)
-    out_own = ring_of_four(after(o, kv_here), "tp_0")
-    out_other = [sibling(piece) for piece in out_own]
+    out_near = hops(after(o, kv_here), "tp_0")
 
     at = jnp.arange(rows, dtype=jnp.int32)
     key_place = jnp.concatenate(
@@ -358,7 +387,10 @@
     query_place = (
         jnp.arange(planes, dtype=jnp.int32)[:, None] * block + (2 * x + c) * rows + at[None]
     ).reshape(-1, 1)
-    attn = attend(q, kv_own, kv_other, gate, key_place, query_place)
+    attn = attend(q, kv_own, kv_other, key_place, query_place)
+    out_near = lax.optimization_barrier((*out_near, attn))[:2]
+    out_own = (o, *out_near, *relays(*out_near, "tp_0"))
+    out_other = [sibling(piece) for piece in (after(o, attn), *out_own[1:])]
     attn = lax.all_to_all(attn, "sp", 0, 0, tiled=True)
     attn = attn.reshape(chunks, seqs, 2, rows, HD)
     return finish(places, pooled, attn, out_own, out_other)

time: 291 us -> 290 us (level)
  the two profiles are of different devices: /device:TPU:32 before, /device:TPU:24 now
where the time goes in v2:
time: 290 us; the launch traced here: 289 us
  starting transfers between devices  92.6 us (32%)
  blocking collectives  91.2 us (31%)
  waiting for transfers between devices  46.5 us (16%)
  Pallas kernels  41.5 us (14%)
  local copies, waits for them, and re-layouts  11.2 us (4%)
  other arithmetic  4.75 us (2%)
    all_to_all x1, blocking collectives, on_device(): lax.all_to_all(kv_here.reshape(planes, 2 * rows + GATE_ROWS, HD), 'sp', 0...  47.6 us
    all_to_all x1, blocking collectives, spread(): lax.all_to_all(jnp.broadcast_to(x[None], (n,) + x.shape), axis, 0, 0, til...  29.6 us
    ppermute x8, starting transfers between devices, hops(): return (lax.ppermute(x, axis, UP), lax.ppermute(x, axis, DOWN))  28.2 us
    pallas_call x1, Pallas kernels, attend(): pl.pallas_call(body, in_specs=[whole()] * 10, out_specs=whole(), out_shap...  20.5 us
    ppermute x4, starting transfers between devices, relays(): lax.ppermute(after[half:], axis, DOWN)  17 us
    ppermute x8, starting transfers between devices, sibling(): return lax.ppermute(x, 'tp_1', [(0, 1), (1, 0)])  16.3 us
    all_to_all x1, blocking collectives, on_device(): kv_here = lax.all_to_all(kv, 'tp_0', 0, 0, tiled=True)  13.9 us
    ppermute x8, waiting for transfers between devices, hops(): return (lax.ppermute(x, axis, UP), lax.ppermute(x, axis, DOWN))  13.3 us
  transfers between devices with their start and end apart: 30, of which 9 were waited for; matrix products, arithmetic and copies ran while one was open for 4% of the time, Pallas kernels for 11%

profile of v2, /device:TPU:24, one launch (start us, length us, event | category | flops | bytes accessed | tf_op | source)
XLA Modules:
  0.0 288.6 jit_solution(12694746566412688111)
XLA Ops:
  3.0 29.6 %all_to_all.25.own_ref = bf16[4,528,512]{2,1,0:T(8,128)(2,1)S(1)} all-to-all(bf16[4,528,512]{2,1,0:T(8,128)(2,1)S(1)} %broadcast_in_dim.28), channel_id=1, replica_groups=mesh['sp'=16,'fs'=4,'tp_0'=4,'tp_1'=2] {'fs'}, dimensions={0} | all-to-all | bytes 4325376 | tf_op jit(solution)/shard_map/all_to_all | solution.py:31
  32.6 1.9 collective-permute-start.4
  34.5 3.4 %collective-permute-start = (bf16[2,64,2048]{2,1,0:T(8,128)(2,1)S(1)}, bf16[2,64,2048]{2,1,0:T(8,128)(2,1)S(1)}, u32[]{:S(2)}, u32[]{:S(2)}) collective-permute-start(bf16[2,64,2048]{2,1,0:T(8,128)(2,1)S(1)} %copy-done.3), channel_id=1, source_target_pairs={{0,2},{2,4},{4,6},{6,0},{1,3},{3,5},{5,7},{7,1},{8,10},{10,12},{12... | collective-permute-start | bytes 1572872 | tf_op jit(solution)/shard_map/ppermute | solution.py:43
  37.9 3.7 %collective-permute-start.1 = (bf16[2,64,2048]{2,1,0:T(8,128)(2,1)S(1)}, bf16[2,64,2048]{2,1,0:T(8,128)(2,1)S(1)}, u32[]{:S(2)}, u32[]{:S(2)}) collective-permute-start(bf16[2,64,2048]{2,1,0:T(8,128)(2,1)S(1)} %copy-done.3), channel_id=1, source_target_pairs={{0,6},{2,0},{4,2},{6,4},{1,7},{3,1},{5,3},{7,5},{8,14},{10,8},{12,... | collective-permute-start | bytes 1572872 | tf_op jit(solution)/shard_map/ppermute | solution.py:43
  41.6 10.4 %collective-permute-done.x1 = bf16[2,64,2048]{2,1,0:T(8,128)(2,1)S(1)} collective-permute-done((bf16[2,64,2048]{2,1,0:T(8,128)(2,1)S(1)}, bf16[2,64,2048]{2,1,0:T(8,128)(2,1)S(1)}, u32[]{:S(2)}, u32[]{:S(2)}) %collective-permute-start) | collective-permute-done | bytes 524320 | tf_op jit(solution)/shard_map/ppermute | solution.py:43
  52.7 2.2 collective-permute-start.2
  55.7 4.9 %collective-permute-start.3 = (bf16[1,64,2048]{2,1,0:T(8,128)(2,1)}, bf16[1,64,2048]{2,1,0:T(8,128)(2,1)}, u32[]{:S(2)}, u32[]{:S(2)}) collective-permute-start(bf16[1,64,2048]{2,1,0:T(8,128)(2,1)} %slice.45), channel_id=1, source_target_pairs={{0,6},{2,0},{4,2},{6,4},{1,7},{3,1},{5,3},{7,5},{8,14},{10,8},{12,... | collective-permute-start | bytes 786440 | tf_op jit(solution)/shard_map/ppermute | solution.py:48
  61.2 2.7 collective-permute-done.2.x3
  63.9 2.1 collective-permute-done.3.x4
  66.0 2.7 factors.1.norm_ref
  68.7 5.1 %project.3 = bf16[4,2,2,144,128]{4,3,2,1,0:T(8,128)(2,1)} custom-call(s32[6]{0:T(128)} %stack.34.p_ref, f32[512,1]{1,0:T(8,128)} %factors.1.norm_ref, bf16[2,64,2048]{2,1,0:T(8,128)(2,1)} %x0.5, bf16[2,64,2048]{2,1,0:T(8,128)(2,1)} %copy-done.1, bf16[2,64,2048]{2,1,0:T(8,128)(2,1)} %copy-done.2, bf16[1,64,2048]{2,1,0:T(8,128)(2,1)} %copy-done.7, ...), custom_call_target="tpu_custom_call" | custom-call | tf_op jit(solution)/shard_map/project/pallas_call | solution.py:131
  73.8 13.9 %all_to_all.26 = bf16[4,2,2,144,128]{4,3,2,1,0:T(8,128)(2,1)S(1)} all-to-all(bf16[4,2,2,144,128]{4,3,2,1,0:T(8,128)(2,1)} %project.3), channel_id=1, replica_groups=mesh['sp'=16,'fs'=4,'tp_0'=4,'tp_1'=2] {'tp_0'}, dimensions={0} | all-to-all | bytes 1179648 | tf_op jit(solution)/shard_map/all_to_all | solution.py:351
  87.8 47.6 %all_to_all.27.refs_0_ = bf16[16,144,128]{2,1,0:T(8,128)(2,1)S(1)} all-to-all(bf16[16,144,128]{2,1,0:T(8,128)(2,1)S(1)} %bitcast.26), channel_id=1, replica_groups=mesh['sp'=16,'fs'=4,'tp_0'=4,'tp_1'=2] {'sp'}, dimensions={0} | all-to-all | bytes 1179648 | tf_op jit(solution)/shard_map/all_to_all | solution.py:352
  135.4 2.5 collective-permute-start.9
  137.9 4.6 %collective-permute-start.10 = (bf16[16,144,128]{2,1,0:T(8,128)(2,1)S(1)}, bf16[16,144,128]{2,1,0:T(8,128)(2,1)S(1)}, u32[]{:S(2)}, u32[]{:S(2)}) collective-permute-start(bf16[16,144,128]{2,1,0:T(8,128)(2,1)S(1)} %all_to_all.27.refs_0_), channel_id=1, source_target_pairs={{0,6},{2,0},{4,2},{6,4},{1,7},{3,1},{5,3},{7,5},{8,14},{10,8},{12,... | collective-permute-start | bytes 1769480 | tf_op jit(solution)/shard_map/ppermute | solution.py:43
  142.5 2.3 collective-permute-start.16
  144.8 4.8 %collective-permute-start.15 = (bf16[256,512]{1,0:T(8,128)(2,1)S(1)}, bf16[256,512]{1,0:T(8,128)(2,1)}, u32[]{:S(2)}, u32[]{:S(2)}) collective-permute-start(bf16[256,512]{1,0:T(8,128)(2,1)S(1)} %pad_maximum_fusion.2), channel_id=1, source_target_pairs={{0,8},{8,16},{16,24},{24,0},{1,9},{9,17},{17,25},{25,1},{2,10},{10... | collective-permute-start | bytes 786440 | tf_op jit(solution)/shard_map/ppermute | solution.py:43
  149.8 2.9 %collective-permute-done.16 = bf16[256,512]{1,0:T(8,128)(2,1)S(1)} collective-permute-done((bf16[256,512]{1,0:T(8,128)(2,1)S(1)}, bf16[256,512]{1,0:T(8,128)(2,1)S(1)}, u32[]{:S(2)}, u32[]{:S(2)}) %collective-permute-start.16) | collective-permute-done | bytes 262176 | tf_op jit(solution)/shard_map/ppermute | solution.py:43
  152.7 1.9 collective-permute-start.18
  155.6 5.1 %collective-permute-start.17 = (bf16[128,512]{1,0:T(8,128)(2,1)S(1)}, bf16[128,512]{1,0:T(8,128)(2,1)S(1)}, u32[]{:S(2)}, u32[]{:S(2)}) collective-permute-start(bf16[128,512]{1,0:T(8,128)(2,1)S(1)} %slice.51), channel_id=1, source_target_pairs={{0,8},{8,16},{16,24},{24,0},{1,9},{9,17},{17,25},{25,1},{2,10},{10... | collective-permute-start | bytes 393224 | tf_op jit(solution)/shard_map/ppermute | solution.py:48
  160.8 1.9 collective-permute-start.11
  162.7 5.1 %collective-permute-start.12 = (bf16[8,144,128]{2,1,0:T(8,128)(2,1)S(1)}, bf16[8,144,128]{2,1,0:T(8,128)(2,1)S(1)}, u32[]{:S(2)}, u32[]{:S(2)}) collective-permute-start(bf16[8,144,128]{2,1,0:T(8,128)(2,1)S(1)} %slice.50), channel_id=1, source_target_pairs={{0,6},{2,0},{4,2},{6,4},{1,7},{3,1},{5,3},{7,5},{8,14},{10,8},{12,... | collective-permute-start | bytes 884744 | tf_op jit(solution)/shard_map/ppermute | solution.py:48
  168.9 5.0 %project.2 = (bf16[2,1,2,2,64,128]{5,4,3,2,1,0:T(8,128)(2,1)}, bf16[2,1,2,2,64,128]{5,4,3,2,1,0:T(8,128)(2,1)}, bf16[2,1,2,2,64,128]{5,4,3,2,1,0:T(8,128)(2,1)}, bf16[2,1,2,2,64,128]{5,4,3,2,1,0:T(8,128)(2,1)}) custom-call(s32[6]{0:T(128)} %stack.34.p_ref, f32[512,1]{1,0:T(8,128)} %factors.1.norm_ref, bf16[2,64,2048]{2,1,0:T(8,128)(2,1)} %x0.5, ...), custom_call_target="tpu_custom_call" | custom-call | tf_op jit(solution)/shard_map/project/pallas_call | solution.py:131
  173.9 2.1 collective-permute-start.5
  177.5 1.9 collective-permute-start.14
  179.5 3.9 %collective-permute-start.6 = (bf16[2,1,2,2,64,128]{5,4,3,2,1,0:T(8,128)(2,1)S(1)}, bf16[2,1,2,2,64,128]{5,4,3,2,1,0:T(8,128)(2,1)S(1)}, u32[]{:S(2)}, u32[]{:S(2)}) collective-permute-start(bf16[2,1,2,2,64,128]{5,4,3,2,1,0:T(8,128)(2,1)S(1)} %copy-done.20), channel_id=1, source_target_pairs={{0,2},{2,4},{4,6},{6,0},{1,3},{3,5},{5,7},{7,1},{8,10},{10,12},{12... | collective-permute-start | bytes 393224 | tf_op jit(solution)/shard_map/ppermute | solution.py:359
  183.4 1.9 collective-permute-start.7
  185.6 2.9 %collective-permute-done.6 = bf16[2,1,2,2,64,128]{5,4,3,2,1,0:T(8,128)(2,1)S(1)} collective-permute-done((bf16[2,1,2,2,64,128]{5,4,3,2,1,0:T(8,128)(2,1)S(1)}, bf16[2,1,2,2,64,128]{5,4,3,2,1,0:T(8,128)(2,1)S(1)}, u32[]{:S(2)}, u32[]{:S(2)}) %collective-permute-start.6) | collective-permute-done | bytes 131104 | tf_op jit(solution)/shard_map/ppermute | solution.py:359
  188.5 3.9 %collective-permute-done.7 = bf16[2,1,2,2,64,128]{5,4,3,2,1,0:T(8,128)(2,1)S(1)} collective-permute-done((bf16[2,1,2,2,64,128]{5,4,3,2,1,0:T(8,128)(2,1)S(1)}, bf16[2,1,2,2,64,128]{5,4,3,2,1,0:T(8,128)(2,1)S(1)}, u32[]{:S(2)}, u32[]{:S(2)}) %collective-permute-start.7) | collective-permute-done | bytes 131104 | tf_op jit(solution)/shard_map/ppermute | solution.py:359
  192.5 2.2 collective-permute-start.19
  194.7 4.9 %collective-permute-start.20 = (bf16[4,256,512]{2,1,0:T(8,128)(2,1)S(1)}, bf16[4,256,512]{2,1,0:T(8,128)(2,1)S(1)}, u32[]{:S(2)}, u32[]{:S(2)}) collective-permute-start(bf16[4,256,512]{2,1,0:T(8,128)(2,1)S(1)} %fusion.refs_0_), channel_id=1, source_target_pairs={{0,6},{2,0},{4,2},{6,4},{1,7},{3,1},{5,3},{7,5},{8,14},{10,8},{12,... | collective-permute-start | bytes 3145736 | tf_op jit(solution)/shard_map/ppermute | solution.py:43
  200.3 4.2 %all-to-all-start.3 = ((bf16[16,64,128]{2,1,0:T(8,128)(2,1)}), bf16[16,64,128]{2,1,0:T(8,128)(2,1)}, u32[]{:S(2)}, u32[]{:S(2)}) async-start(bf16[16,64,128]{2,1,0:T(8,128)(2,1)} %bitcast.28), calls=%async_computation.3 | async-start | bytes 524288 | tf_op jit(solution)/shard_map/all_to_all | solution.py:365
  204.5 1.9 collective-permute-start.13
  208.4 2.4 collective-permute-start.8
  212.7 9.7 %all-to-all-done.3.q_ref = bf16[16,64,128]{2,1,0:T(8,128)(2,1)} async-done(((bf16[16,64,128]{2,1,0:T(8,128)(2,1)}), bf16[16,64,128]{2,1,0:T(8,128)(2,1)}, u32[]{:S(2)}, u32[]{:S(2)}) %all-to-all-start.3) | async-done | bytes 262176 | tf_op jit(solution)/shard_map/all_to_all | solution.py:365
  222.5 20.5 %attend.1 = bf16[16,64,128]{2,1,0:T(8,128)(2,1)} custom-call(bf16[16,64,128]{2,1,0:T(8,128)(2,1)} %all-to-all-done.3.q_ref, bf16[16,144,128]{2,1,0:T(8,128)(2,1)} %copy-done.10, bf16[16,144,128]{2,1,0:T(8,128)(2,1)} %copy-done.5, bf16[16,144,128]{2,1,0:T(8,128)(2,1)} %copy-done.6, bf16[8,144,128]{2,1,0:T(8,128)(2,1)} %copy-done.12, ...), custom_call_target="tpu_custom_call" | custom-call | tf_op jit(solution)/shard_map/attend/pallas_call | solution.py:208
  243.9 1.9 collective-permute-start.24
  246.6 2.4 collective-permute-start.25
  249.1 1.9 collective-permute-start.23
  251.0 1.9 collective-permute-start.21
  252.9 5.1 %collective-permute-start.22 = (bf16[2,256,512]{2,1,0:T(8,128)(2,1)}, bf16[2,256,512]{2,1,0:T(8,128)(2,1)}, u32[]{:S(2)}, u32[]{:S(2)}) collective-permute-start(bf16[2,256,512]{2,1,0:T(8,128)(2,1)} %slice.43), channel_id=1, source_target_pairs={{0,6},{2,0},{4,2},{6,4},{1,7},{3,1},{5,3},{7,5},{8,14},{10,8},{12,... | collective-permute-start | bytes 1572872 | tf_op jit(solution)/shard_map/ppermute | solution.py:48
  258.1 5.4 %all-to-all-start.4 = ((bf16[16,64,128]{2,1,0:T(8,128)(2,1)}), bf16[16,64,128]{2,1,0:T(8,128)(2,1)S(1)}, u32[]{:S(2)}, u32[]{:S(2)}) async-start(bf16[16,64,128]{2,1,0:T(8,128)(2,1)} %attend.1), calls=%async_computation.4 | async-start | bytes 524288 | tf_op jit(solution)/shard_map/all_to_all | solution.py:394
  263.5 5.2 %collective-permute-done.21.refs_3_ = bf16[2,256,512]{2,1,0:T(8,128)(2,1)} collective-permute-done((bf16[2,256,512]{2,1,0:T(8,128)(2,1)}, bf16[2,256,512]{2,1,0:T(8,128)(2,1)}, u32[]{:S(2)}, u32[]{:S(2)}) %collective-permute-start.21) | collective-permute-done | bytes 524320 | tf_op jit(solution)/shard_map/ppermute | solution.py:48
  268.7 1.9 collective-permute-start.26
  270.7 2.4 collective-permute-start.27
  273.1 2.1 pool.1.pool_ref
  275.2 6.6 %all-to-all-done.4 = bf16[16,64,128]{2,1,0:T(8,128)(2,1)S(1)} async-done(((bf16[16,64,128]{2,1,0:T(8,128)(2,1)}), bf16[16,64,128]{2,1,0:T(8,128)(2,1)S(1)}, u32[]{:S(2)}, u32[]{:S(2)}) %all-to-all-start.4) | async-done | bytes 262176 | tf_op jit(solution)/shard_map/all_to_all | solution.py:394
  282.6 6.0 %finish.1 = bf16[2,64,2048]{2,1,0:T(8,128)(2,1)} custom-call(s32[6]{0:T(128)} %stack.34.p_ref, bf16[4,2,2,64,128]{4,3,2,1,0:T(8,128)(2,1)} %pool.1.pool_ref, bf16[4,2,2,64,128]{4,3,2,1,0:T(8,128)(2,1)} %bitcast.27, bf16[4,256,512]{2,1,0:T(8,128)(2,1)} %copy-done.4, bf16[4,256,512]{2,1,0:T(8,128)(2,1)} %copy-done.8, bf16[4,256,512]{2,1,0:T(8,128)(2,1)} %copy-done.9, ...), custom_call_target="tpu_custom_call" | custom-call | tf_op jit(solution)/shard_map/finish/pallas_call | solution.py:287
  (100 shorter events, 16.0 us)
Async XLA Ops:
  3.0 31.5 %copy-start.3 = (bf16[2,64,2048]{2,1,0:T(8,128)(2,1)S(1)}, bf16[2,64,2048]{2,1,0:T(8,128)(2,1)}, u32[]{:S(2)}) copy-start(bf16[2,64,2048]{2,1,0:T(8,128)(2,1)} %x0.5) | copy-start | bytes 1572868
  32.6 36.1 %copy-start = (bf16[4,528,512]{2,1,0:T(8,128)(2,1)}, bf16[4,528,512]{2,1,0:T(8,128)(2,1)S(1)}, u32[]{:S(2)}) copy-start(bf16[4,528,512]{2,1,0:T(8,128)(2,1)S(1)} %all_to_all.25.own_ref) | copy-start | bytes 6488068
  32.6 36.1 %collective-permute-start.4 = (bf16[4,528,512]{2,1,0:T(8,128)(2,1)S(1)}, bf16[4,528,512]{2,1,0:T(8,128)(2,1)}, u32[]{:S(2)}, u32[]{:S(2)}) collective-permute-start(bf16[4,528,512]{2,1,0:T(8,128)(2,1)S(1)} %all_to_all.25.own_ref), channel_id=1, source_target_pairs={{0,1},{1,0},{2,3},{3,2},{4,5},{5,4},{6,7},{7,6},{8,9},{9,8},{10,11... | collective-permute-start | bytes 6488072 | tf_op jit(solution)/shard_map/ppermute | solution.py:35
  34.5 17.4 %collective-permute-start = (bf16[2,64,2048]{2,1,0:T(8,128)(2,1)S(1)}, bf16[2,64,2048]{2,1,0:T(8,128)(2,1)S(1)}, u32[]{:S(2)}, u32[]{:S(2)}) collective-permute-start(bf16[2,64,2048]{2,1,0:T(8,128)(2,1)S(1)} %copy-done.3), channel_id=1, source_target_pairs={{0,2},{2,4},{4,6},{6,0},{1,3},{3,5},{5,7},{7,1},{8,10},{10,12},{12... | collective-permute-start | bytes 1572872 | tf_op jit(solution)/shard_map/ppermute | solution.py:43
  37.9 17.0 %collective-permute-start.1 = (bf16[2,64,2048]{2,1,0:T(8,128)(2,1)S(1)}, bf16[2,64,2048]{2,1,0:T(8,128)(2,1)S(1)}, u32[]{:S(2)}, u32[]{:S(2)}) collective-permute-start(bf16[2,64,2048]{2,1,0:T(8,128)(2,1)S(1)} %copy-done.3), channel_id=1, source_target_pairs={{0,6},{2,0},{4,2},{6,4},{1,7},{3,1},{5,3},{7,5},{8,14},{10,8},{12,... | collective-permute-start | bytes 1572872 | tf_op jit(solution)/shard_map/ppermute | solution.py:43
  51.9 14.0 %copy-start.1 = (bf16[2,64,2048]{2,1,0:T(8,128)(2,1)}, bf16[2,64,2048]{2,1,0:T(8,128)(2,1)S(1)}, u32[]{:S(2)}) copy-start(bf16[2,64,2048]{2,1,0:T(8,128)(2,1)S(1)} %collective-permute-done.x1) | copy-start | bytes 1572868
  52.7 11.2 %collective-permute-start.2 = (bf16[1,64,2048]{2,1,0:T(8,128)(2,1)}, bf16[1,64,2048]{2,1,0:T(8,128)(2,1)S(1)}, u32[]{:S(2)}, u32[]{:S(2)}) collective-permute-start(bf16[1,64,2048]{2,1,0:T(8,128)(2,1)} %slice.44), channel_id=1, source_target_pairs={{0,2},{2,4},{4,6},{6,0},{1,3},{3,5},{5,7},{7,1},{8,10},{10,12},{12... | collective-permute-start | bytes 786440 | tf_op jit(solution)/shard_map/ppermute | solution.py:48
  54.9 11.0 %copy-start.2 = (bf16[2,64,2048]{2,1,0:T(8,128)(2,1)}, bf16[2,64,2048]{2,1,0:T(8,128)(2,1)S(1)}, u32[]{:S(2)}) copy-start(bf16[2,64,2048]{2,1,0:T(8,128)(2,1)S(1)} %collective-permute-done.1.x2) | copy-start | bytes 1572868
  55.7 10.2 %collective-permute-start.3 = (bf16[1,64,2048]{2,1,0:T(8,128)(2,1)}, bf16[1,64,2048]{2,1,0:T(8,128)(2,1)}, u32[]{:S(2)}, u32[]{:S(2)}) collective-permute-start(bf16[1,64,2048]{2,1,0:T(8,128)(2,1)} %slice.45), channel_id=1, source_target_pairs={{0,6},{2,0},{4,2},{6,4},{1,7},{3,1},{5,3},{7,5},{8,14},{10,8},{12,... | collective-permute-start | bytes 786440 | tf_op jit(solution)/shard_map/ppermute | solution.py:48
  63.9 2.1 copy-start.7
  73.8 68.7 %copy-start.16 = (bf16[128,512]{1,0:T(8,128)(2,1)S(1)}, bf16[128,512]{1,0:T(8,128)(2,1)}, u32[]{:S(2)}) copy-start(bf16[128,512]{1,0:T(8,128)(2,1)} %param.21) | copy-start | bytes 393220
  73.8 68.7 %copy-start.17 = (bf16[128,512]{1,0:T(8,128)(2,1)S(1)}, bf16[128,512]{1,0:T(8,128)(2,1)}, u32[]{:S(2)}) copy-start(bf16[128,512]{1,0:T(8,128)(2,1)} %param.20) | copy-start | bytes 393220
  135.4 27.3 %copy-start.10 = (bf16[16,144,128]{2,1,0:T(8,128)(2,1)}, bf16[16,144,128]{2,1,0:T(8,128)(2,1)S(1)}, u32[]{:S(2)}) copy-start(bf16[16,144,128]{2,1,0:T(8,128)(2,1)S(1)} %all_to_all.27.refs_0_) | copy-start | bytes 1769476
  135.4 25.3 %collective-permute-start.9 = (bf16[16,144,128]{2,1,0:T(8,128)(2,1)S(1)}, bf16[16,144,128]{2,1,0:T(8,128)(2,1)S(1)}, u32[]{:S(2)}, u32[]{:S(2)}) collective-permute-start(bf16[16,144,128]{2,1,0:T(8,128)(2,1)S(1)} %all_to_all.27.refs_0_), channel_id=1, source_target_pairs={{0,2},{2,4},{4,6},{6,0},{1,3},{3,5},{5,7},{7,1},{8,10},{10,12},{12... | collective-permute-start | bytes 1769480 | tf_op jit(solution)/shard_map/ppermute | solution.py:43
  137.9 24.8 %collective-permute-start.10 = (bf16[16,144,128]{2,1,0:T(8,128)(2,1)S(1)}, bf16[16,144,128]{2,1,0:T(8,128)(2,1)S(1)}, u32[]{:S(2)}, u32[]{:S(2)}) collective-permute-start(bf16[16,144,128]{2,1,0:T(8,128)(2,1)S(1)} %all_to_all.27.refs_0_), channel_id=1, source_target_pairs={{0,6},{2,0},{4,2},{6,4},{1,7},{3,1},{5,3},{7,5},{8,14},{10,8},{12,... | collective-permute-start | bytes 1769480 | tf_op jit(solution)/shard_map/ppermute | solution.py:43
  142.5 10.2 %collective-permute-start.16 = (bf16[256,512]{1,0:T(8,128)(2,1)S(1)}, bf16[256,512]{1,0:T(8,128)(2,1)S(1)}, u32[]{:S(2)}, u32[]{:S(2)}) collective-permute-start(bf16[256,512]{1,0:T(8,128)(2,1)S(1)} %pad_maximum_fusion.2), channel_id=1, source_target_pairs={{0,24},{8,0},{16,8},{24,16},{1,25},{9,1},{17,9},{25,17},{2,26},{10... | collective-permute-start | bytes 786440 | tf_op jit(solution)/shard_map/ppermute | solution.py:43
  144.8 9.8 %collective-permute-start.15 = (bf16[256,512]{1,0:T(8,128)(2,1)S(1)}, bf16[256,512]{1,0:T(8,128)(2,1)}, u32[]{:S(2)}, u32[]{:S(2)}) collective-permute-start(bf16[256,512]{1,0:T(8,128)(2,1)S(1)} %pad_maximum_fusion.2), channel_id=1, source_target_pairs={{0,8},{8,16},{16,24},{24,0},{1,9},{9,17},{17,25},{25,1},{2,10},{10... | collective-permute-start | bytes 786440 | tf_op jit(solution)/shard_map/ppermute | solution.py:43
  152.7 26.7 %collective-permute-start.18 = (bf16[128,512]{1,0:T(8,128)(2,1)S(1)}, bf16[128,512]{1,0:T(8,128)(2,1)S(1)}, u32[]{:S(2)}, u32[]{:S(2)}) collective-permute-start(bf16[128,512]{1,0:T(8,128)(2,1)S(1)} %slice.52), channel_id=1, source_target_pairs={{0,24},{8,0},{16,8},{24,16},{1,25},{9,1},{17,9},{25,17},{2,26},{10... | collective-permute-start | bytes 393224 | tf_op jit(solution)/shard_map/ppermute | solution.py:48
  155.6 23.9 %collective-permute-start.17 = (bf16[128,512]{1,0:T(8,128)(2,1)S(1)}, bf16[128,512]{1,0:T(8,128)(2,1)S(1)}, u32[]{:S(2)}, u32[]{:S(2)}) collective-permute-start(bf16[128,512]{1,0:T(8,128)(2,1)S(1)} %slice.51), channel_id=1, source_target_pairs={{0,8},{8,16},{16,24},{24,0},{1,9},{9,17},{17,25},{25,1},{2,10},{10... | collective-permute-start | bytes 393224 | tf_op jit(solution)/shard_map/ppermute | solution.py:48
  160.7 15.3 %copy-start.5 = (bf16[16,144,128]{2,1,0:T(8,128)(2,1)}, bf16[16,144,128]{2,1,0:T(8,128)(2,1)S(1)}, u32[]{:S(2)}) copy-start(bf16[16,144,128]{2,1,0:T(8,128)(2,1)S(1)} %collective-permute-done.9.refs_1_) | copy-start | bytes 1769476
  160.8 15.2 %collective-permute-start.11 = (bf16[8,144,128]{2,1,0:T(8,128)(2,1)S(1)}, bf16[8,144,128]{2,1,0:T(8,128)(2,1)S(1)}, u32[]{:S(2)}, u32[]{:S(2)}) collective-permute-start(bf16[8,144,128]{2,1,0:T(8,128)(2,1)S(1)} %slice.49), channel_id=1, source_target_pairs={{0,2},{2,4},{4,6},{6,0},{1,3},{3,5},{5,7},{7,1},{8,10},{10,12},{12... | collective-permute-start | bytes 884744 | tf_op jit(solution)/shard_map/ppermute | solution.py:48
  162.7 13.3 %copy-start.6 = (bf16[16,144,128]{2,1,0:T(8,128)(2,1)}, bf16[16,144,128]{2,1,0:T(8,128)(2,1)S(1)}, u32[]{:S(2)}) copy-start(bf16[16,144,128]{2,1,0:T(8,128)(2,1)S(1)} %collective-permute-done.10.refs_2_) | copy-start | bytes 1769476
  162.7 13.3 %collective-permute-start.12 = (bf16[8,144,128]{2,1,0:T(8,128)(2,1)S(1)}, bf16[8,144,128]{2,1,0:T(8,128)(2,1)S(1)}, u32[]{:S(2)}, u32[]{:S(2)}) collective-permute-start(bf16[8,144,128]{2,1,0:T(8,128)(2,1)S(1)} %slice.50), channel_id=1, source_target_pairs={{0,6},{2,0},{4,2},{6,4},{1,7},{3,1},{5,3},{7,5},{8,14},{10,8},{12,... | collective-permute-start | bytes 884744 | tf_op jit(solution)/shard_map/ppermute | solution.py:48
  173.9 5.6 %copy-start.20 = (bf16[2,1,2,2,64,128]{5,4,3,2,1,0:T(8,128)(2,1)S(1)}, bf16[2,1,2,2,64,128]{5,4,3,2,1,0:T(8,128)(2,1)}, u32[]{:S(2)}) copy-start(bf16[2,1,2,2,64,128]{5,4,3,2,1,0:T(8,128)(2,1)} %get-tuple-element.17) | copy-start | bytes 393220
  173.9 9.5 %copy-start.19 = (bf16[2,1,2,2,64,128]{5,4,3,2,1,0:T(8,128)(2,1)S(1)}, bf16[2,1,2,2,64,128]{5,4,3,2,1,0:T(8,128)(2,1)}, u32[]{:S(2)}) copy-start(bf16[2,1,2,2,64,128]{5,4,3,2,1,0:T(8,128)(2,1)} %get-tuple-element.18) | copy-start | bytes 393220
  173.9 11.6 %copy-start.15 = (bf16[2,1,2,2,64,128]{5,4,3,2,1,0:T(8,128)(2,1)S(1)}, bf16[2,1,2,2,64,128]{5,4,3,2,1,0:T(8,128)(2,1)}, u32[]{:S(2)}) copy-start(bf16[2,1,2,2,64,128]{5,4,3,2,1,0:T(8,128)(2,1)} %get-tuple-element.15) | copy-start | bytes 393220
  173.9 11.6 %collective-permute-start.5 = (bf16[2,1,2,2,64,128]{5,4,3,2,1,0:T(8,128)(2,1)}, bf16[2,1,2,2,64,128]{5,4,3,2,1,0:T(8,128)(2,1)S(1)}, u32[]{:S(2)}, u32[]{:S(2)}) collective-permute-start(bf16[2,1,2,2,64,128]{5,4,3,2,1,0:T(8,128)(2,1)} %get-tuple-element.16), channel_id=1, source_target_pairs={{0,6},{2,0},{4,2},{6,4},{1,7},{3,1},{5,3},{7,5},{8,14},{10,8},{12,... | collective-permute-start | bytes 393224 | tf_op jit(solution)/shard_map/ppermute | solution.py:359
  177.5 44.9 %collective-permute-start.14 = (bf16[48,144,128]{2,1,0:T(8,128)(2,1)}, bf16[48,144,128]{2,1,0:T(8,128)(2,1)}, u32[]{:S(2)}, u32[]{:S(2)}) collective-permute-start(bf16[48,144,128]{2,1,0:T(8,128)(2,1)} %pad_maximum_fusion), channel_id=1, source_target_pairs={{0,1},{1,0},{2,3},{3,2},{4,5},{5,4},{6,7},{7,6},{8,9},{9,8},{10,11... | collective-permute-start | bytes 5308424 | tf_op jit(solution)/shard_map/ppermute | solution.py:35
  179.5 69.6 %copy-start.4 = (bf16[4,256,512]{2,1,0:T(8,128)(2,1)}, bf16[4,256,512]{2,1,0:T(8,128)(2,1)S(1)}, u32[]{:S(2)}) copy-start(bf16[4,256,512]{2,1,0:T(8,128)(2,1)S(1)} %fusion.refs_0_) | copy-start | bytes 3145732
  179.5 9.0 %collective-permute-start.6 = (bf16[2,1,2,2,64,128]{5,4,3,2,1,0:T(8,128)(2,1)S(1)}, bf16[2,1,2,2,64,128]{5,4,3,2,1,0:T(8,128)(2,1)S(1)}, u32[]{:S(2)}, u32[]{:S(2)}) collective-permute-start(bf16[2,1,2,2,64,128]{5,4,3,2,1,0:T(8,128)(2,1)S(1)} %copy-done.20), channel_id=1, source_target_pairs={{0,2},{2,4},{4,6},{6,0},{1,3},{3,5},{5,7},{7,1},{8,10},{10,12},{12... | collective-permute-start | bytes 393224 | tf_op jit(solution)/shard_map/ppermute | solution.py:359
  183.4 9.0 %collective-permute-start.7 = (bf16[2,1,2,2,64,128]{5,4,3,2,1,0:T(8,128)(2,1)S(1)}, bf16[2,1,2,2,64,128]{5,4,3,2,1,0:T(8,128)(2,1)S(1)}, u32[]{:S(2)}, u32[]{:S(2)}) collective-permute-start(bf16[2,1,2,2,64,128]{5,4,3,2,1,0:T(8,128)(2,1)S(1)} %copy-done.19), channel_id=1, source_target_pairs={{0,4},{2,6},{4,0},{6,2},{1,5},{3,7},{5,1},{7,3},{8,12},{10,14},{12... | collective-permute-start | bytes 393224 | tf_op jit(solution)/shard_map/ppermute | solution.py:359
  192.5 50.5 %collective-permute-start.19 = (bf16[4,256,512]{2,1,0:T(8,128)(2,1)S(1)}, bf16[4,256,512]{2,1,0:T(8,128)(2,1)S(1)}, u32[]{:S(2)}, u32[]{:S(2)}) collective-permute-start(bf16[4,256,512]{2,1,0:T(8,128)(2,1)S(1)} %fusion.refs_0_), channel_id=1, source_target_pairs={{0,2},{2,4},{4,6},{6,0},{1,3},{3,5},{5,7},{7,1},{8,10},{10,12},{12... | collective-permute-start | bytes 3145736 | tf_op jit(solution)/shard_map/ppermute | solution.py:43
  194.7 48.3 %collective-permute-start.20 = (bf16[4,256,512]{2,1,0:T(8,128)(2,1)S(1)}, bf16[4,256,512]{2,1,0:T(8,128)(2,1)S(1)}, u32[]{:S(2)}, u32[]{:S(2)}) collective-permute-start(bf16[4,256,512]{2,1,0:T(8,128)(2,1)S(1)} %fusion.refs_0_), channel_id=1, source_target_pairs={{0,6},{2,0},{4,2},{6,4},{1,7},{3,1},{5,3},{7,5},{8,14},{10,8},{12,... | collective-permute-start | bytes 3145736 | tf_op jit(solution)/shard_map/ppermute | solution.py:43
  200.3 42.6 %copy-start.11 = (bf16[4,2,2,64,128]{4,3,2,1,0:T(8,128)(2,1)}, bf16[4,2,2,64,128]{4,3,2,1,0:T(8,128)(2,1)S(1)}, u32[]{:S(2)}) copy-start(bf16[4,2,2,64,128]{4,3,2,1,0:T(8,128)(2,1)S(1)} %get-tuple-element.26.in_ref) | copy-start | bytes 786436
  200.3 22.1 %all-to-all-start.3 = ((bf16[16,64,128]{2,1,0:T(8,128)(2,1)}), bf16[16,64,128]{2,1,0:T(8,128)(2,1)}, u32[]{:S(2)}, u32[]{:S(2)}) async-start(bf16[16,64,128]{2,1,0:T(8,128)(2,1)} %bitcast.28), calls=%async_computation.3 | async-start | bytes 524288 | tf_op jit(solution)/shard_map/all_to_all | solution.py:365
  204.5 8.2 %collective-permute-start.13 = (bf16[16,144,128]{2,1,0:T(8,128)(2,1)}, bf16[16,144,128]{2,1,0:T(8,128)(2,1)}, u32[]{:S(2)}, u32[]{:S(2)}) collective-permute-start(bf16[16,144,128]{2,1,0:T(8,128)(2,1)} %copy-done.10), channel_id=1, source_target_pairs={{0,1},{1,0},{2,3},{3,2},{4,5},{5,4},{6,7},{7,6},{8,9},{9,8},{10,11... | collective-permute-start | bytes 1769480 | tf_op jit(solution)/shard_map/ppermute | solution.py:35
  208.4 44.5 %collective-permute-start.8 = (bf16[4,2,2,16,128]{4,3,2,1,0:T(8,128)(2,1)S(1)}, bf16[4,2,2,16,128]{4,3,2,1,0:T(8,128)(2,1)S(1)}, u32[]{:S(2)}, u32[]{:S(2)}) collective-permute-start(bf16[4,2,2,16,128]{4,3,2,1,0:T(8,128)(2,1)S(1)} %slice.47), channel_id=1, source_target_pairs={{0,1},{1,2},{2,3},{3,4},{4,5},{5,6},{6,7},{7,32},{32,33},{33,34},{... | collective-permute-start | bytes 196616 | tf_op jit(solution)/shard_map/ppermute | solution.py:368
  242.9 39.0 %copy-start.8 = (bf16[4,256,512]{2,1,0:T(8,128)(2,1)}, bf16[4,256,512]{2,1,0:T(8,128)(2,1)S(1)}, u32[]{:S(2)}) copy-start(bf16[4,256,512]{2,1,0:T(8,128)(2,1)S(1)} %collective-permute-done.19.refs_1_) | copy-start | bytes 3145732
  243.0 38.9 %copy-start.9 = (bf16[4,256,512]{2,1,0:T(8,128)(2,1)}, bf16[4,256,512]{2,1,0:T(8,128)(2,1)S(1)}, u32[]{:S(2)}) copy-start(bf16[4,256,512]{2,1,0:T(8,128)(2,1)S(1)} %collective-permute-done.20.refs_2_) | copy-start | bytes 3145732
  243.9 38.0 %collective-permute-start.24 = (bf16[4,256,512]{2,1,0:T(8,128)(2,1)S(1)}, bf16[4,256,512]{2,1,0:T(8,128)(2,1)}, u32[]{:S(2)}, u32[]{:S(2)}) collective-permute-start(bf16[4,256,512]{2,1,0:T(8,128)(2,1)S(1)} %collective-permute-done.19.refs_1_), channel_id=1, source_target_pairs={{0,1},{1,0},{2,3},{3,2},{4,5},{5,4},{6,7},{7,6},{8,9},{9,8},{10,11... | collective-permute-start | bytes 3145736 | tf_op jit(solution)/shard_map/ppermute | solution.py:35
  246.6 35.2 %collective-permute-start.25 = (bf16[4,256,512]{2,1,0:T(8,128)(2,1)S(1)}, bf16[4,256,512]{2,1,0:T(8,128)(2,1)}, u32[]{:S(2)}, u32[]{:S(2)}) collective-permute-start(bf16[4,256,512]{2,1,0:T(8,128)(2,1)S(1)} %collective-permute-done.20.refs_2_), channel_id=1, source_target_pairs={{0,1},{1,0},{2,3},{3,2},{4,5},{5,4},{6,7},{7,6},{8,9},{9,8},{10,11... | collective-permute-start | bytes 3145736 | tf_op jit(solution)/shard_map/ppermute | solution.py:35
  249.1 32.8 %collective-permute-start.23 = (bf16[4,256,512]{2,1,0:T(8,128)(2,1)S(1)}, bf16[4,256,512]{2,1,0:T(8,128)(2,1)}, u32[]{:S(2)}, u32[]{:S(2)}) collective-permute-start(bf16[4,256,512]{2,1,0:T(8,128)(2,1)S(1)} %fusion.refs_0_), channel_id=1, source_target_pairs={{0,1},{1,0},{2,3},{3,2},{4,5},{5,4},{6,7},{7,6},{8,9},{9,8},{10,11... | collective-permute-start | bytes 3145736 | tf_op jit(solution)/shard_map/ppermute | solution.py:35
  251.0 17.7 %collective-permute-start.21 = (bf16[2,256,512]{2,1,0:T(8,128)(2,1)}, bf16[2,256,512]{2,1,0:T(8,128)(2,1)}, u32[]{:S(2)}, u32[]{:S(2)}) collective-permute-start(bf16[2,256,512]{2,1,0:T(8,128)(2,1)} %slice.42), channel_id=1, source_target_pairs={{0,2},{2,4},{4,6},{6,0},{1,3},{3,5},{5,7},{7,1},{8,10},{10,12},{12... | collective-permute-start | bytes 1572872 | tf_op jit(solution)/shard_map/ppermute | solution.py:48
  252.9 20.2 %copy-start.18 = (bf16[4,2,2,16,128]{4,3,2,1,0:T(8,128)(2,1)}, bf16[4,2,2,16,128]{4,3,2,1,0:T(8,128)(2,1)S(1)}, u32[]{:S(2)}) copy-start(bf16[4,2,2,16,128]{4,3,2,1,0:T(8,128)(2,1)S(1)} %collective-permute-done.8.edge_ref) | copy-start | bytes 196612
  252.9 17.7 %collective-permute-start.22 = (bf16[2,256,512]{2,1,0:T(8,128)(2,1)}, bf16[2,256,512]{2,1,0:T(8,128)(2,1)}, u32[]{:S(2)}, u32[]{:S(2)}) collective-permute-start(bf16[2,256,512]{2,1,0:T(8,128)(2,1)} %slice.43), channel_id=1, source_target_pairs={{0,6},{2,0},{4,2},{6,4},{1,7},{3,1},{5,3},{7,5},{8,14},{10,8},{12,... | collective-permute-start | bytes 1572872 | tf_op jit(solution)/shard_map/ppermute | solution.py:48
  258.1 23.8 %all-to-all-start.4 = ((bf16[16,64,128]{2,1,0:T(8,128)(2,1)}), bf16[16,64,128]{2,1,0:T(8,128)(2,1)S(1)}, u32[]{:S(2)}, u32[]{:S(2)}) async-start(bf16[16,64,128]{2,1,0:T(8,128)(2,1)} %attend.1), calls=%async_computation.4 | async-start | bytes 524288 | tf_op jit(solution)/shard_map/all_to_all | solution.py:394
  268.7 13.1 %collective-permute-start.26 = (bf16[2,256,512]{2,1,0:T(8,128)(2,1)}, bf16[2,256,512]{2,1,0:T(8,128)(2,1)}, u32[]{:S(2)}, u32[]{:S(2)}) collective-permute-start(bf16[2,256,512]{2,1,0:T(8,128)(2,1)} %collective-permute-done.21.refs_3_), channel_id=1, source_target_pairs={{0,1},{1,0},{2,3},{3,2},{4,5},{5,4},{6,7},{7,6},{8,9},{9,8},{10,11... | collective-permute-start | bytes 1572872 | tf_op jit(solution)/shard_map/ppermute | solution.py:35
  270.7 11.2 %collective-permute-start.27 = (bf16[2,256,512]{2,1,0:T(8,128)(2,1)}, bf16[2,256,512]{2,1,0:T(8,128)(2,1)}, u32[]{:S(2)}, u32[]{:S(2)}) collective-permute-start(bf16[2,256,512]{2,1,0:T(8,128)(2,1)} %collective-permute-done.22.refs_4_), channel_id=1, source_target_pairs={{0,1},{1,0},{2,3},{3,2},{4,5},{5,4},{6,7},{7,6},{8,9},{9,8},{10,11... | collective-permute-start | bytes 1572872 | tf_op jit(solution)/shard_map/ppermute | solution.py:35
  (3 other events, 3.7 us)

commit v3 on v2

--- a/solution.py
+++ b/solution.py
@@ -26,11 +26,6 @@
     return pl.BlockSpec(memory_space=memory)
 
 
-def spread(x, axis):
-    n = lax.axis_size(axis)
-    return lax.all_to_all(jnp.broadcast_to(x[None], (n,) + x.shape), axis, 0, 0, tiled=True)
-
-
 def sibling(x):
     return lax.ppermute(x, "tp_1", [(0, 1), (1, 0)])
 
@@ -82,24 +77,39 @@
     seqs, rows, _ = rows_of[0].shape
     kinds = len(factors)
 
-    def body(p_ref, norm_ref, x0, x1, x2, x3, x4, own_ref, other_ref, *outs):
-        x = jnp.concatenate(
-            [x0[0], x0[1], x1[0], x1[1], x2[0], x2[1], x3[0], x4[0]], axis=0
-        )
+    def body(p_ref, norm_ref, *refs):
+        xs, own_refs, other_refs, outs = refs[:5], refs[5:10], refs[10:12], refs[12:]
+        deep = own_refs[0].shape[0] - GATE_ROWS
+        tall = deep + GATE_ROWS
         r = norm_ref[...]
         lane = lax.broadcasted_iota(jnp.int32, (GATE_ROWS, HD), 1)
         first_half = (lane < rows) == (p_ref[0] == 0)
-        for ref, head in ((own_ref, p_ref[0]), (other_ref, 1 - p_ref[0])):
-            w = jnp.concatenate(
-                [ref[b, : ref.shape[1] - GATE_ROWS, cols] for b in range(ref.shape[0])], axis=0
+        slabs = []
+        for b in range(4):
+            at = pl.ds(pl.multiple_of(p_ref[5 + b] * deep, deep), deep)
+            slabs.append(
+                jnp.concatenate(
+                    [ref[i, :, at] for ref in xs for i in range(ref.shape[0])], axis=0
+                )
             )
-            y = jnp.dot(x, w, preferred_element_type=F32) * r
+        own = [ref[:deep, cols] for ref in own_refs[:3]]
+        far = jnp.concatenate([ref[:, cols] for ref in own_refs[3:]], axis=0)
+        own.append(far[:deep])
+        other = [other_refs[0][:deep, cols]]
+        other += [other_refs[1][n * tall : n * tall + deep, cols] for n in range(3)]
+        for ref, ws, head in (
+            (own_refs[0], own, p_ref[0]),
+            (other_refs[0], other, 1 - p_ref[0]),
+        ):
+            y = jnp.dot(slabs[0], ws[0], preferred_element_type=F32)
+            for b in range(1, 4):
+                y = y + jnp.dot(slabs[b], ws[b], preferred_element_type=F32)
+            y = y * r
             if not split:
                 for a in range(4):
                     to = p_ref[1 + a]
                     g = ref[
-                        p_ref[5],
-                        ref.shape[1] - GATE_ROWS :,
+                        deep:,
                         pl.ds(pl.multiple_of(to * 2 * rows, 2 * rows), 2 * rows),
                     ].astype(F32)
                     turned = pltpu.roll(g, rows, 1)
@@ -130,12 +140,12 @@
         shapes = [(4, seqs, 2, kinds * rows + GATE_ROWS, HD)]
     outs = pl.pallas_call(
         body,
-        in_specs=[whole(pltpu.SMEM)] + [whole()] * 8,
+        in_specs=[whole(pltpu.SMEM)] + [whole()] * 13,
         out_specs=[whole()] * len(shapes),
         out_shape=[jax.ShapeDtypeStruct(sh, BF16) for sh in shapes],
         compiler_params=params(),
         name="project",
-    )(places, norm, *rows_of, own, other)
+    )(places, norm, *rows_of, *own, *other)
     return outs
 
 
@@ -256,27 +266,31 @@
     )(first, rows_in, border, mix, scale)
 
 
-def finish(places, pooled, attn, own, other):
+def finish(places, pooled, attn, pooled_pair, attn_pair, w):
     nx, seqs, _, rows, _ = pooled.shape
-    ny, deep, wide = own[0].shape
-
-    def body(p_ref, pool_ref, attn_ref, *refs):
-        out_ref = refs[10]
+    ny, deep, wide = w[0].shape
+    own = seqs * rows
+
+    def body(p_ref, pool_ref, attn_ref, pool_pair_ref, attn_pair_ref, *refs):
+        out_ref, pair_ref = refs[5:]
         late = pl.program_id(0) >= ny // 2
-        total = jnp.zeros((seqs * rows, wide), F32)
-        for side, c in ((refs[:5], p_ref[0]), (refs[5:10], 1 - p_ref[0])):
-            for a in range(nx):
-                x = p_ref[1 + a]
-                left = jnp.concatenate(
-                    [
-                        jnp.concatenate([pool_ref[x, i, c] for i in range(seqs)], axis=0),
-                        jnp.concatenate([attn_ref[x, i, c] for i in range(seqs)], axis=0),
-                    ],
-                    axis=1,
-                )
-                right = side[a][0] if a < 3 else jnp.where(late, side[4][0], side[3][0])
-                total = total + jnp.dot(left, right, preferred_element_type=F32)
-        out_ref[...] = total.astype(BF16).reshape(seqs, rows, wide)
+        c = p_ref[0]
+        total = jnp.zeros((2 * own, wide), F32)
+        for a in range(nx):
+            x = p_ref[1 + a]
+            left = jnp.concatenate(
+                [
+                    jnp.concatenate(
+                        [ref[x, i, c] for ref in two for i in range(seqs)], axis=0
+                    )
+                    for two in ((pool_ref, pool_pair_ref), (attn_ref, attn_pair_ref))
+                ],
+                axis=1,
+            )
+            right = refs[a][0] if a < 3 else jnp.where(late, refs[4][0], refs[3][0])
+            total = total + jnp.dot(left, right, preferred_element_type=F32)
+        out_ref[...] = total[:own].reshape(seqs, rows, wide)
+        pair_ref[...] = total[own:].astype(BF16).reshape(seqs, rows, wide)
 
     half = ny // 2
     shape = (1, deep, wide)
@@ -284,15 +298,17 @@
         pl.BlockSpec(shape, lambda j: (jnp.minimum(j, half - 1), 0, 0)),
         pl.BlockSpec(shape, lambda j: (jnp.maximum(j - half, 0), 0, 0)),
     ]
+    out_spec = pl.BlockSpec((seqs, rows, wide), lambda j: (0, 0, j))
+    out = (seqs, rows, ny * wide)
     return pl.pallas_call(
         body,
         grid=(ny,),
-        in_specs=[whole(pltpu.SMEM), whole(), whole()] + specs + specs,
-        out_specs=pl.BlockSpec((seqs, rows, wide), lambda j: (0, 0, j)),
-        out_shape=jax.ShapeDtypeStruct((seqs, rows, ny * wide), BF16),
+        in_specs=[whole(pltpu.SMEM)] + [whole()] * 4 + specs,
+        out_specs=[out_spec, out_spec],
+        out_shape=[jax.ShapeDtypeStruct(out, F32), jax.ShapeDtypeStruct(out, BF16)],
         compiler_params=params(),
         name="finish",
-    )(places, pooled, attn, *own, *other)
+    )(places, pooled, attn, pooled_pair, attn_pair, *w)
 
 
 def after(x, *others):
@@ -330,7 +346,8 @@
     seqs, rows, _ = tokens.shape
     block = rows * chunks * 2
     seen = [x, (x + 3) % 4, (x + 1) % 4, (x + 2) % 4]
-    places = jnp.stack([c] + seen + [y]).astype(jnp.int32)
+    deeps = [y, (y + 3) % 4, (y + 1) % 4, (y + 2) % 4]
+    places = jnp.stack([c] + seen + deeps).astype(jnp.int32)
 
     deep = w_key.shape[0]
     gain = lax.dynamic_slice_in_dim(norm_gain, y * deep, deep, 0)
@@ -344,8 +361,9 @@
     middle = lax.reduce_precision(rest, 8, 7)
     parts = jnp.stack([high, middle, rest - middle], axis=1).astype(BF16)
     parts = jnp.pad(parts, ((0, 0), (0, 5), (0, 0))).reshape(GATE_ROWS, block)
-    own_w = spread(jnp.concatenate([weights, parts], axis=0), "fs")
-    other_w = sibling(own_w)
+    own_w = ring_of_four(jnp.concatenate([weights, parts], axis=0), "fs")
+    other_w = sibling(own_w[0])
+    other_w = (other_w, sibling(jnp.concatenate(own_w[1:], axis=0)))
 
     (kv,) = project(places, norm, all_rows, own_w, other_w, 0, (1.0, 1.0), False)
     kv_here = lax.all_to_all(kv, "tp_0", 0, 0, tiled=True)
@@ -370,14 +388,16 @@
     )
     first = (z * block + (2 * x + c) * rows).reshape(1).astype(jnp.int32)
     pooled = pool(first, pool_in, border, pool_mix, pool_scale.reshape(-1, HD))
+    pooled_pair = sibling(pooled)
 
     kv_own = ring_of_four(kv, "tp_0")
-    kv_other = [sibling(kv), sibling(jnp.concatenate(kv_own[1:], axis=0))]
+    kv_other = sibling(kv)
+    kv_other = (kv_other, sibling(jnp.concatenate(kv_own[1:], axis=0)))
 
     out_w = jnp.concatenate([w_out_pool, w_out_attn], axis=0)
-    o = ring_of_four(after(out_w, own_w), "fs")
+    o = ring_of_four(after(out_w, own_w[1]), "fs")
     o = [o[0], o[1], o[2], jnp.concatenate(o[3:], axis=0)]
-    o = placed([w[None] for w in o], [y, (y + 3) % 4, (y + 1) % 4, (y + 2) % 4], 0)
+    o = placed([w[None] for w in o], deeps, 0)
     out_near = hops(after(o, kv_here), "tp_0")
 
     at = jnp.arange(rows, dtype=jnp.int32)
@@ -390,10 +410,12 @@
     attn = attend(q, kv_own, kv_other, key_place, query_place)
     out_near = lax.optimization_barrier((*out_near, attn))[:2]
     out_own = (o, *out_near, *relays(*out_near, "tp_0"))
-    out_other = [sibling(piece) for piece in (after(o, attn), *out_own[1:])]
     attn = lax.all_to_all(attn, "sp", 0, 0, tiled=True)
     attn = attn.reshape(chunks, seqs, 2, rows, HD)
-    return finish(places, pooled, attn, out_own, out_other)
+    mine, theirs = finish(
+        places, pooled, attn, pooled_pair, sibling(attn), out_own
+    )
+    return (mine + sibling(theirs).astype(F32)).astype(BF16)
 
 
 def solution(mesh):

time: 290 us -> 294 us (1.014)
  the two profiles are of different devices: /device:TPU:24 before, /device:TPU:33 now
where the time goes in v3:
time: 294 us; the launch traced here: 292 us
  starting transfers between devices  121 us (41%)
  blocking collectives  60.1 us (20%)
  waiting for transfers between devices  46.5 us (16%)
  Pallas kernels  40.8 us (14%)
  local copies, waits for them, and re-layouts  15.6 us (5%)
  other arithmetic  7.05 us (2%)
    all_to_all x1, blocking collectives, on_device(): lax.all_to_all(kv_here.reshape(planes, 2 * rows + GATE_ROWS, HD), 'sp', 0...  47.5 us
    ppermute x10, starting transfers between devices, hops(): return (lax.ppermute(x, axis, UP), lax.ppermute(x, axis, DOWN))  33.5 us
    ppermute x7, starting transfers between devices, sibling(): return lax.ppermute(x, 'tp_1', [(0, 1), (1, 0)])  28.4 us
    ppermute x10, waiting for transfers between devices, hops(): return (lax.ppermute(x, axis, UP), lax.ppermute(x, axis, DOWN))  26.1 us
    ppermute x5, starting transfers between devices, relays(): lax.ppermute(after[half:], axis, DOWN)  21.9 us
    pallas_call x1, Pallas kernels, attend(): pl.pallas_call(body, in_specs=[whole()] * 10, out_specs=whole(), out_shap...  20.5 us
    all_to_all x1, blocking collectives, on_device(): kv_here = lax.all_to_all(kv, 'tp_0', 0, 0, tiled=True)  12.6 us
    all_to_all x1, starting transfers between devices, on_device(): attn = lax.all_to_all(attn, 'sp', 0, 0, tiled=True)  11.5 us
  transfers between devices with their start and end apart: 33, of which 11 were waited for; matrix products, arithmetic and copies ran while one was open for 4% of the time, Pallas kernels for 10%

profile of v3, /device:TPU:33, one launch (start us, length us, event | category | flops | bytes accessed | tf_op | source)
XLA Modules:
  0.0 291.9 jit_solution(13264570509468159198)
XLA Ops:
  2.8 3.2 %collective-permute-start.4 = (bf16[528,512]{1,0:T(8,128)(2,1)S(1)}, bf16[528,512]{1,0:T(8,128)(2,1)S(1)}, u32[]{:S(2)}, u32[]{:S(2)}) collective-permute-start(bf16[528,512]{1,0:T(8,128)(2,1)S(1)} %pad_maximum_fusion.2.refs_5_), channel_id=1, source_target_pairs={{0,8},{8,16},{16,24},{24,0},{1,9},{9,17},{17,25},{25,1},{2,10},{10... | collective-permute-start | bytes 1622024 | tf_op jit(solution)/shard_map/ppermute | solution.py:38
  6.0 3.4 %collective-permute-start.5 = (bf16[528,512]{1,0:T(8,128)(2,1)S(1)}, bf16[528,512]{1,0:T(8,128)(2,1)S(1)}, u32[]{:S(2)}, u32[]{:S(2)}) collective-permute-start(bf16[528,512]{1,0:T(8,128)(2,1)S(1)} %pad_maximum_fusion.2.refs_5_), channel_id=1, source_target_pairs={{0,24},{8,0},{16,8},{24,16},{1,25},{9,1},{17,9},{25,17},{2,26},{10... | collective-permute-start | bytes 1622024 | tf_op jit(solution)/shard_map/ppermute | solution.py:38
  9.4 9.8 %collective-permute-done.4.refs_6_ = bf16[528,512]{1,0:T(8,128)(2,1)S(1)} collective-permute-done((bf16[528,512]{1,0:T(8,128)(2,1)S(1)}, bf16[528,512]{1,0:T(8,128)(2,1)S(1)}, u32[]{:S(2)}, u32[]{:S(2)}) %collective-permute-start.4) | collective-permute-done | bytes 540704 | tf_op jit(solution)/shard_map/ppermute | solution.py:38
  19.3 2.1 collective-permute-start.6
  21.4 4.6 %collective-permute-start.7 = (bf16[264,512]{1,0:T(8,128)(2,1)S(1)}, bf16[264,512]{1,0:T(8,128)(2,1)S(1)}, u32[]{:S(2)}, u32[]{:S(2)}) collective-permute-start(bf16[264,512]{1,0:T(8,128)(2,1)S(1)} %slice.55), channel_id=1, source_target_pairs={{0,24},{8,0},{16,8},{24,16},{1,25},{9,1},{17,9},{25,17},{2,26},{10... | collective-permute-start | bytes 811016 | tf_op jit(solution)/shard_map/ppermute | solution.py:43
  25.9 3.1 %collective-permute-done.6.refs_8_ = bf16[264,512]{1,0:T(8,128)(2,1)S(1)} collective-permute-done((bf16[264,512]{1,0:T(8,128)(2,1)S(1)}, bf16[264,512]{1,0:T(8,128)(2,1)S(1)}, u32[]{:S(2)}, u32[]{:S(2)}) %collective-permute-start.6) | collective-permute-done | bytes 270368 | tf_op jit(solution)/shard_map/ppermute | solution.py:43
  32.0 4.5 %collective-permute-start.9 = (bf16[1584,512]{1,0:T(8,128)(2,1)}, bf16[1584,512]{1,0:T(8,128)(2,1)S(1)}, u32[]{:S(2)}, u32[]{:S(2)}) collective-permute-start(bf16[1584,512]{1,0:T(8,128)(2,1)} %pad_maximum_fusion.1), channel_id=1, source_target_pairs={{0,1},{1,0},{2,3},{3,2},{4,5},{5,4},{6,7},{7,6},{8,9},{9,8},{10,11... | collective-permute-start | bytes 4866056 | tf_op jit(solution)/shard_map/ppermute | solution.py:30
  36.6 3.1 %collective-permute-start = (bf16[2,64,2048]{2,1,0:T(8,128)(2,1)S(1)}, bf16[2,64,2048]{2,1,0:T(8,128)(2,1)S(1)}, u32[]{:S(2)}, u32[]{:S(2)}) collective-permute-start(bf16[2,64,2048]{2,1,0:T(8,128)(2,1)S(1)} %copy-done.6), channel_id=1, source_target_pairs={{0,2},{2,4},{4,6},{6,0},{1,3},{3,5},{5,7},{7,1},{8,10},{10,12},{12... | collective-permute-start | bytes 1572872 | tf_op jit(solution)/shard_map/ppermute | solution.py:38
  39.7 3.4 %collective-permute-start.1 = (bf16[2,64,2048]{2,1,0:T(8,128)(2,1)S(1)}, bf16[2,64,2048]{2,1,0:T(8,128)(2,1)S(1)}, u32[]{:S(2)}, u32[]{:S(2)}) collective-permute-start(bf16[2,64,2048]{2,1,0:T(8,128)(2,1)S(1)} %copy-done.6), channel_id=1, source_target_pairs={{0,6},{2,0},{4,2},{6,4},{1,7},{3,1},{5,3},{7,5},{8,14},{10,8},{12,... | collective-permute-start | bytes 1572872 | tf_op jit(solution)/shard_map/ppermute | solution.py:38
  43.1 2.5 collective-permute-start.8
  45.6 7.6 %collective-permute-done.x1.refs_1_ = bf16[2,64,2048]{2,1,0:T(8,128)(2,1)S(1)} collective-permute-done((bf16[2,64,2048]{2,1,0:T(8,128)(2,1)S(1)}, bf16[2,64,2048]{2,1,0:T(8,128)(2,1)S(1)}, u32[]{:S(2)}, u32[]{:S(2)}) %collective-permute-start) | collective-permute-done | bytes 524320 | tf_op jit(solution)/shard_map/ppermute | solution.py:38
  56.6 4.6 %collective-permute-start.3 = (bf16[1,64,2048]{2,1,0:T(8,128)(2,1)}, bf16[1,64,2048]{2,1,0:T(8,128)(2,1)S(1)}, u32[]{:S(2)}, u32[]{:S(2)}) collective-permute-start(bf16[1,64,2048]{2,1,0:T(8,128)(2,1)} %slice.53), channel_id=1, source_target_pairs={{0,6},{2,0},{4,2},{6,4},{1,7},{3,1},{5,3},{7,5},{8,14},{10,8},{12,... | collective-permute-start | bytes 786440 | tf_op jit(solution)/shard_map/ppermute | solution.py:43
  61.9 2.4 collective-permute-done.2.x3.refs_3_
  66.7 2.7 factors.1.norm_ref
  70.6 5.1 %project.3 = bf16[4,2,2,144,128]{4,3,2,1,0:T(8,128)(2,1)} custom-call(s32[9]{0:T(128)} %stack.46.p_ref, f32[512,1]{1,0:T(8,128)} %factors.1.norm_ref, bf16[2,64,2048]{2,1,0:T(8,128)(2,1)} %refs_0_.3, bf16[2,64,2048]{2,1,0:T(8,128)(2,1)} %copy-done.3, bf16[2,64,2048]{2,1,0:T(8,128)(2,1)} %copy-done.4, bf16[1,64,2048]{2,1,0:T(8,128)(2,1)} %collective-permute-done.2.x3.refs_3_, ...), custom_call_target="tpu_custom_call" | custom-call | tf_op jit(solution)/shard_map/project/pallas_call | solution.py:141
  75.7 12.6 %all_to_all.20 = bf16[4,2,2,144,128]{4,3,2,1,0:T(8,128)(2,1)S(1)} all-to-all(bf16[4,2,2,144,128]{4,3,2,1,0:T(8,128)(2,1)} %project.3), channel_id=1, replica_groups=mesh['sp'=16,'fs'=4,'tp_0'=4,'tp_1'=2] {'tp_0'}, dimensions={0} | all-to-all | bytes 1179648 | tf_op jit(solution)/shard_map/all_to_all | solution.py:369
  88.3 47.5 %all_to_all.21.refs_0_ = bf16[16,144,128]{2,1,0:T(8,128)(2,1)S(1)} all-to-all(bf16[16,144,128]{2,1,0:T(8,128)(2,1)S(1)} %bitcast.29), channel_id=1, replica_groups=mesh['sp'=16,'fs'=4,'tp_0'=4,'tp_1'=2] {'sp'}, dimensions={0} | all-to-all | bytes 1179648 | tf_op jit(solution)/shard_map/all_to_all | solution.py:370
  135.8 2.2 collective-permute-start.14
  138.0 4.3 %collective-permute-start.15 = (bf16[16,144,128]{2,1,0:T(8,128)(2,1)S(1)}, bf16[16,144,128]{2,1,0:T(8,128)(2,1)S(1)}, u32[]{:S(2)}, u32[]{:S(2)}) collective-permute-start(bf16[16,144,128]{2,1,0:T(8,128)(2,1)S(1)} %all_to_all.21.refs_0_), channel_id=1, source_target_pairs={{0,6},{2,0},{4,2},{6,4},{1,7},{3,1},{5,3},{7,5},{8,14},{10,8},{12,... | collective-permute-start | bytes 1769480 | tf_op jit(solution)/shard_map/ppermute | solution.py:38
  142.3 8.7 %collective-permute-done.14.refs_1_ = bf16[16,144,128]{2,1,0:T(8,128)(2,1)S(1)} collective-permute-done((bf16[16,144,128]{2,1,0:T(8,128)(2,1)S(1)}, bf16[16,144,128]{2,1,0:T(8,128)(2,1)S(1)}, u32[]{:S(2)}, u32[]{:S(2)}) %collective-permute-start.14) | collective-permute-done | bytes 589856 | tf_op jit(solution)/shard_map/ppermute | solution.py:38
  151.0 1.9 collective-permute-start.16
  152.9 4.6 %collective-permute-start.17 = (bf16[8,144,128]{2,1,0:T(8,128)(2,1)S(1)}, bf16[8,144,128]{2,1,0:T(8,128)(2,1)S(1)}, u32[]{:S(2)}, u32[]{:S(2)}) collective-permute-start(bf16[8,144,128]{2,1,0:T(8,128)(2,1)S(1)} %slice.60), channel_id=1, source_target_pairs={{0,6},{2,0},{4,2},{6,4},{1,7},{3,1},{5,3},{7,5},{8,14},{10,8},{12,... | collective-permute-start | bytes 884744 | tf_op jit(solution)/shard_map/ppermute | solution.py:43
  158.9 2.7 collective-permute-start.22
  161.6 4.6 %collective-permute-start.23 = (bf16[256,512]{1,0:T(8,128)(2,1)S(1)}, bf16[256,512]{1,0:T(8,128)(2,1)}, u32[]{:S(2)}, u32[]{:S(2)}) collective-permute-start(bf16[256,512]{1,0:T(8,128)(2,1)S(1)} %pad_maximum_fusion.3), channel_id=1, source_target_pairs={{0,24},{8,0},{16,8},{24,16},{1,25},{9,1},{17,9},{25,17},{2,26},{10... | collective-permute-start | bytes 786440 | tf_op jit(solution)/shard_map/ppermute | solution.py:38
  166.2 5.0 %project.2 = (bf16[2,1,2,2,64,128]{5,4,3,2,1,0:T(8,128)(2,1)}, bf16[2,1,2,2,64,128]{5,4,3,2,1,0:T(8,128)(2,1)}, bf16[2,1,2,2,64,128]{5,4,3,2,1,0:T(8,128)(2,1)}, bf16[2,1,2,2,64,128]{5,4,3,2,1,0:T(8,128)(2,1)}) custom-call(s32[9]{0:T(128)} %stack.46.p_ref, f32[512,1]{1,0:T(8,128)} %factors.1.norm_ref, bf16[2,64,2048]{2,1,0:T(8,128)(2,1)} %refs_0_.3, ...), custom_call_target="tpu_custom_call" | custom-call | tf_op jit(solution)/shard_map/project/pallas_call | solution.py:141
  173.1 3.5 %collective-permute-start.11 = (bf16[2,1,2,2,64,128]{5,4,3,2,1,0:T(8,128)(2,1)}, bf16[2,1,2,2,64,128]{5,4,3,2,1,0:T(8,128)(2,1)S(1)}, u32[]{:S(2)}, u32[]{:S(2)}) collective-permute-start(bf16[2,1,2,2,64,128]{5,4,3,2,1,0:T(8,128)(2,1)} %get-tuple-element.18), channel_id=1, source_target_pairs={{0,2},{2,4},{4,6},{6,0},{1,3},{3,5},{5,7},{7,1},{8,10},{10,12},{12... | collective-permute-start | bytes 393224 | tf_op jit(solution)/shard_map/ppermute | solution.py:377
  178.1 7.0 %collective-permute-start.19 = (bf16[48,144,128]{2,1,0:T(8,128)(2,1)}, bf16[48,144,128]{2,1,0:T(8,128)(2,1)}, u32[]{:S(2)}, u32[]{:S(2)}) collective-permute-start(bf16[48,144,128]{2,1,0:T(8,128)(2,1)} %pad_maximum_fusion), channel_id=1, source_target_pairs={{0,1},{1,0},{2,3},{3,2},{4,5},{5,4},{6,7},{7,6},{8,9},{9,8},{10,11... | collective-permute-start | bytes 5308424 | tf_op jit(solution)/shard_map/ppermute | solution.py:30
  185.3 1.9 collective-permute-start.12
  187.3 6.4 %collective-permute-done.12 = bf16[2,1,2,2,64,128]{5,4,3,2,1,0:T(8,128)(2,1)S(1)} collective-permute-done((bf16[2,1,2,2,64,128]{5,4,3,2,1,0:T(8,128)(2,1)S(1)}, bf16[2,1,2,2,64,128]{5,4,3,2,1,0:T(8,128)(2,1)S(1)}, u32[]{:S(2)}, u32[]{:S(2)}) %collective-permute-start.12) | collective-permute-done | bytes 131104 | tf_op jit(solution)/shard_map/ppermute | solution.py:377
  194.5 4.5 %all-to-all-start.2 = ((bf16[16,64,128]{2,1,0:T(8,128)(2,1)}), bf16[16,64,128]{2,1,0:T(8,128)(2,1)S(1)}, u32[]{:S(2)}, u32[]{:S(2)}) async-start(bf16[16,64,128]{2,1,0:T(8,128)(2,1)} %bitcast.13), calls=%async_computation.2 | async-start | bytes 524288 | tf_op jit(solution)/shard_map/all_to_all | solution.py:383
  200.0 3.6 %collective-permute-start.25 = (bf16[128,512]{1,0:T(8,128)(2,1)S(1)}, bf16[128,512]{1,0:T(8,128)(2,1)S(1)}, u32[]{:S(2)}, u32[]{:S(2)}) collective-permute-start(bf16[128,512]{1,0:T(8,128)(2,1)S(1)} %slice.62), channel_id=1, source_target_pairs={{0,24},{8,0},{16,8},{24,16},{1,25},{9,1},{17,9},{25,17},{2,26},{10... | collective-permute-start | bytes 393224 | tf_op jit(solution)/shard_map/ppermute | solution.py:43
  204.6 1.9 collective-permute-start.24
  207.5 3.6 %collective-permute-start.18 = (bf16[16,144,128]{2,1,0:T(8,128)(2,1)S(1)}, bf16[16,144,128]{2,1,0:T(8,128)(2,1)}, u32[]{:S(2)}, u32[]{:S(2)}) collective-permute-start(bf16[16,144,128]{2,1,0:T(8,128)(2,1)S(1)} %all_to_all.21.refs_0_), channel_id=1, source_target_pairs={{0,1},{1,0},{2,3},{3,2},{4,5},{5,4},{6,7},{7,6},{8,9},{9,8},{10,11... | collective-permute-start | bytes 1769480 | tf_op jit(solution)/shard_map/ppermute | solution.py:30
  212.2 1.9 collective-permute-start.26
  214.1 4.8 %collective-permute-start.27 = (bf16[4,256,512]{2,1,0:T(8,128)(2,1)S(1)}, bf16[4,256,512]{2,1,0:T(8,128)(2,1)}, u32[]{:S(2)}, u32[]{:S(2)}) collective-permute-start(bf16[4,256,512]{2,1,0:T(8,128)(2,1)S(1)} %fusion.refs_0_), channel_id=1, source_target_pairs={{0,6},{2,0},{4,2},{6,4},{1,7},{3,1},{5,3},{7,5},{8,14},{10,8},{12,... | collective-permute-start | bytes 3145736 | tf_op jit(solution)/shard_map/ppermute | solution.py:38
  220.3 20.5 %attend.1 = bf16[16,64,128]{2,1,0:T(8,128)(2,1)} custom-call(bf16[16,64,128]{2,1,0:T(8,128)(2,1)} %copy-done.18, bf16[16,144,128]{2,1,0:T(8,128)(2,1)} %copy-done.13, bf16[16,144,128]{2,1,0:T(8,128)(2,1)} %copy-done.8, bf16[16,144,128]{2,1,0:T(8,128)(2,1)} %copy-done.9, bf16[8,144,128]{2,1,0:T(8,128)(2,1)} %copy-done.16, bf16[8,144,128]{2,1,0:T(8,128)(2,1)} %copy-done.17, ...), custom_call_target="tpu_custom_call" | custom-call | tf_op jit(solution)/shard_map/attend/pallas_call | solution.py:218
  240.8 11.5 %all-to-all-start.3 = ((bf16[16,64,128]{2,1,0:T(8,128)(2,1)}), bf16[16,64,128]{2,1,0:T(8,128)(2,1)S(1)}, u32[]{:S(2)}, u32[]{:S(2)}) async-start(bf16[16,64,128]{2,1,0:T(8,128)(2,1)} %attend.1), calls=%async_computation.3 | async-start | bytes 524288 | tf_op jit(solution)/shard_map/all_to_all | solution.py:413
  252.3 1.9 collective-permute-start.28
  255.3 4.6 %collective-permute-start.29 = (bf16[2,256,512]{2,1,0:T(8,128)(2,1)S(1)}, bf16[2,256,512]{2,1,0:T(8,128)(2,1)}, u32[]{:S(2)}, u32[]{:S(2)}) collective-permute-start(bf16[2,256,512]{2,1,0:T(8,128)(2,1)S(1)} %slice.51), channel_id=1, source_target_pairs={{0,6},{2,0},{4,2},{6,4},{1,7},{3,1},{5,3},{7,5},{8,14},{10,8},{12,... | collective-permute-start | bytes 1572872 | tf_op jit(solution)/shard_map/ppermute | solution.py:43
  259.9 4.2 %collective-permute-start.13 = (bf16[4,2,2,16,128]{4,3,2,1,0:T(8,128)(2,1)S(1)}, bf16[4,2,2,16,128]{4,3,2,1,0:T(8,128)(2,1)S(1)}, u32[]{:S(2)}, u32[]{:S(2)}) collective-permute-start(bf16[4,2,2,16,128]{4,3,2,1,0:T(8,128)(2,1)S(1)} %slice.57), channel_id=1, source_target_pairs={{0,1},{1,2},{2,3},{3,4},{4,5},{5,6},{6,7},{7,32},{32,33},{33,34},{... | collective-permute-start | bytes 196616 | tf_op jit(solution)/shard_map/ppermute | solution.py:386
  264.2 2.3 collective-permute-done.13.edge_ref
  267.1 2.1 pool.1.pool_ref
  269.3 6.9 %collective-permute-start.20 = (bf16[4,2,2,64,128]{4,3,2,1,0:T(8,128)(2,1)}, bf16[4,2,2,64,128]{4,3,2,1,0:T(8,128)(2,1)S(1)}, u32[]{:S(2)}, u32[]{:S(2)}) collective-permute-start(bf16[4,2,2,64,128]{4,3,2,1,0:T(8,128)(2,1)} %pool.1.pool_ref), channel_id=1, source_target_pairs={{0,1},{1,0},{2,3},{3,2},{4,5},{5,4},{6,7},{7,6},{8,9},{9,8},{10,11... | collective-permute-start | bytes 786440 | tf_op jit(solution)/shard_map/ppermute | solution.py:30
  276.2 1.9 collective-permute-start.21
  280.4 5.4 %finish.1 = (f32[2,64,2048]{2,1,0:T(8,128)}, bf16[2,64,2048]{2,1,0:T(8,128)(2,1)}) custom-call(s32[9]{0:T(128)} %stack.46.p_ref, bf16[4,2,2,64,128]{4,3,2,1,0:T(8,128)(2,1)} %pool.1.pool_ref, bf16[4,2,2,64,128]{4,3,2,1,0:T(8,128)(2,1)} %bitcast.31, bf16[4,2,2,64,128]{4,3,2,1,0:T(8,128)(2,1)} %copy-done.21, bf16[4,2,2,64,128]{4,3,2,1,0:T(8,128)(2,1)} %copy-done.22, ...), custom_call_target="tpu_custom_call" | custom-call | tf_op jit(solution)/shard_map/finish/pallas_call | solution.py:303
  285.8 2.0 collective-permute-start.30
  287.8 2.0 collective-permute-done.30
  289.8 2.1 add_convert_fusion
  (122 shorter events, 28.5 us)
Async XLA Ops:
  2.8 40.3 %copy-start.5 = (bf16[528,512]{1,0:T(8,128)(2,1)}, bf16[528,512]{1,0:T(8,128)(2,1)S(1)}, u32[]{:S(2)}) copy-start(bf16[528,512]{1,0:T(8,128)(2,1)S(1)} %pad_maximum_fusion.2.refs_5_) | copy-start | bytes 1622020
  2.8 16.4 %collective-permute-start.4 = (bf16[528,512]{1,0:T(8,128)(2,1)S(1)}, bf16[528,512]{1,0:T(8,128)(2,1)S(1)}, u32[]{:S(2)}, u32[]{:S(2)}) collective-permute-start(bf16[528,512]{1,0:T(8,128)(2,1)S(1)} %pad_maximum_fusion.2.refs_5_), channel_id=1, source_target_pairs={{0,8},{8,16},{16,24},{24,0},{1,9},{9,17},{17,25},{25,1},{2,10},{10... | collective-permute-start | bytes 1622024 | tf_op jit(solution)/shard_map/ppermute | solution.py:38
  6.0 15.3 %collective-permute-start.5 = (bf16[528,512]{1,0:T(8,128)(2,1)S(1)}, bf16[528,512]{1,0:T(8,128)(2,1)S(1)}, u32[]{:S(2)}, u32[]{:S(2)}) collective-permute-start(bf16[528,512]{1,0:T(8,128)(2,1)S(1)} %pad_maximum_fusion.2.refs_5_), channel_id=1, source_target_pairs={{0,24},{8,0},{16,8},{24,16},{1,25},{9,1},{17,9},{25,17},{2,26},{10... | collective-permute-start | bytes 1622024 | tf_op jit(solution)/shard_map/ppermute | solution.py:38
  19.2 12.8 %copy-start = (bf16[528,512]{1,0:T(8,128)(2,1)}, bf16[528,512]{1,0:T(8,128)(2,1)S(1)}, u32[]{:S(2)}) copy-start(bf16[528,512]{1,0:T(8,128)(2,1)S(1)} %collective-permute-done.4.refs_6_) | copy-start | bytes 1622020
  19.2 17.3 %copy-start.6 = (bf16[2,64,2048]{2,1,0:T(8,128)(2,1)S(1)}, bf16[2,64,2048]{2,1,0:T(8,128)(2,1)}, u32[]{:S(2)}) copy-start(bf16[2,64,2048]{2,1,0:T(8,128)(2,1)} %refs_0_.3) | copy-start | bytes 1572868
  19.3 9.8 %collective-permute-start.6 = (bf16[264,512]{1,0:T(8,128)(2,1)S(1)}, bf16[264,512]{1,0:T(8,128)(2,1)S(1)}, u32[]{:S(2)}, u32[]{:S(2)}) collective-permute-start(bf16[264,512]{1,0:T(8,128)(2,1)S(1)} %slice.54), channel_id=1, source_target_pairs={{0,8},{8,16},{16,24},{24,0},{1,9},{9,17},{17,25},{25,1},{2,10},{10... | collective-permute-start | bytes 811016 | tf_op jit(solution)/shard_map/ppermute | solution.py:43
  21.4 8.7 %collective-permute-start.7 = (bf16[264,512]{1,0:T(8,128)(2,1)S(1)}, bf16[264,512]{1,0:T(8,128)(2,1)S(1)}, u32[]{:S(2)}, u32[]{:S(2)}) collective-permute-start(bf16[264,512]{1,0:T(8,128)(2,1)S(1)} %slice.55), channel_id=1, source_target_pairs={{0,24},{8,0},{16,8},{24,16},{1,25},{9,1},{17,9},{25,17},{2,26},{10... | collective-permute-start | bytes 811016 | tf_op jit(solution)/shard_map/ppermute | solution.py:43
  29.1 24.8 %copy-start.10 = (bf16[264,512]{1,0:T(8,128)(2,1)}, bf16[264,512]{1,0:T(8,128)(2,1)S(1)}, u32[]{:S(2)}) copy-start(bf16[264,512]{1,0:T(8,128)(2,1)S(1)} %collective-permute-done.6.refs_8_) | copy-start | bytes 811012
  32.0 37.3 %collective-permute-start.9 = (bf16[1584,512]{1,0:T(8,128)(2,1)}, bf16[1584,512]{1,0:T(8,128)(2,1)S(1)}, u32[]{:S(2)}, u32[]{:S(2)}) collective-permute-start(bf16[1584,512]{1,0:T(8,128)(2,1)} %pad_maximum_fusion.1), channel_id=1, source_target_pairs={{0,1},{1,0},{2,3},{3,2},{4,5},{5,4},{6,7},{7,6},{8,9},{9,8},{10,11... | collective-permute-start | bytes 4866056 | tf_op jit(solution)/shard_map/ppermute | solution.py:30
  36.6 16.6 %collective-permute-start = (bf16[2,64,2048]{2,1,0:T(8,128)(2,1)S(1)}, bf16[2,64,2048]{2,1,0:T(8,128)(2,1)S(1)}, u32[]{:S(2)}, u32[]{:S(2)}) collective-permute-start(bf16[2,64,2048]{2,1,0:T(8,128)(2,1)S(1)} %copy-done.6), channel_id=1, source_target_pairs={{0,2},{2,4},{4,6},{6,0},{1,3},{3,5},{5,7},{7,1},{8,10},{10,12},{12... | collective-permute-start | bytes 1572872 | tf_op jit(solution)/shard_map/ppermute | solution.py:38
  39.7 16.1 %collective-permute-start.1 = (bf16[2,64,2048]{2,1,0:T(8,128)(2,1)S(1)}, bf16[2,64,2048]{2,1,0:T(8,128)(2,1)S(1)}, u32[]{:S(2)}, u32[]{:S(2)}) collective-permute-start(bf16[2,64,2048]{2,1,0:T(8,128)(2,1)S(1)} %copy-done.6), channel_id=1, source_target_pairs={{0,6},{2,0},{4,2},{6,4},{1,7},{3,1},{5,3},{7,5},{8,14},{10,8},{12,... | collective-permute-start | bytes 1572872 | tf_op jit(solution)/shard_map/ppermute | solution.py:38
  43.1 26.3 %collective-permute-start.8 = (bf16[528,512]{1,0:T(8,128)(2,1)S(1)}, bf16[528,512]{1,0:T(8,128)(2,1)}, u32[]{:S(2)}, u32[]{:S(2)}) collective-permute-start(bf16[528,512]{1,0:T(8,128)(2,1)S(1)} %pad_maximum_fusion.2.refs_5_), channel_id=1, source_target_pairs={{0,1},{1,0},{2,3},{3,2},{4,5},{5,4},{6,7},{7,6},{8,9},{9,8},{10,11... | collective-permute-start | bytes 1622024 | tf_op jit(solution)/shard_map/ppermute | solution.py:30
  53.1 12.9 %copy-start.3 = (bf16[2,64,2048]{2,1,0:T(8,128)(2,1)}, bf16[2,64,2048]{2,1,0:T(8,128)(2,1)S(1)}, u32[]{:S(2)}) copy-start(bf16[2,64,2048]{2,1,0:T(8,128)(2,1)S(1)} %collective-permute-done.x1.refs_1_) | copy-start | bytes 1572868
  53.9 10.4 %collective-permute-start.2 = (bf16[1,64,2048]{2,1,0:T(8,128)(2,1)}, bf16[1,64,2048]{2,1,0:T(8,128)(2,1)}, u32[]{:S(2)}, u32[]{:S(2)}) collective-permute-start(bf16[1,64,2048]{2,1,0:T(8,128)(2,1)} %slice.52), channel_id=1, source_target_pairs={{0,2},{2,4},{4,6},{6,0},{1,3},{3,5},{5,7},{7,1},{8,10},{10,12},{12... | collective-permute-start | bytes 786440 | tf_op jit(solution)/shard_map/ppermute | solution.py:43
  56.6 9.4 %collective-permute-start.3 = (bf16[1,64,2048]{2,1,0:T(8,128)(2,1)}, bf16[1,64,2048]{2,1,0:T(8,128)(2,1)S(1)}, u32[]{:S(2)}, u32[]{:S(2)}) collective-permute-start(bf16[1,64,2048]{2,1,0:T(8,128)(2,1)} %slice.53), channel_id=1, source_target_pairs={{0,6},{2,0},{4,2},{6,4},{1,7},{3,1},{5,3},{7,5},{8,14},{10,8},{12,... | collective-permute-start | bytes 786440 | tf_op jit(solution)/shard_map/ppermute | solution.py:43
  88.2 70.7 %copy-start.24 = (bf16[128,512]{1,0:T(8,128)(2,1)S(1)}, bf16[128,512]{1,0:T(8,128)(2,1)}, u32[]{:S(2)}) copy-start(bf16[128,512]{1,0:T(8,128)(2,1)} %param.21) | copy-start | bytes 393220
  88.3 70.7 %copy-start.25 = (bf16[128,512]{1,0:T(8,128)(2,1)S(1)}, bf16[128,512]{1,0:T(8,128)(2,1)}, u32[]{:S(2)}) copy-start(bf16[128,512]{1,0:T(8,128)(2,1)} %param.20) | copy-start | bytes 393220
  135.8 71.8 %copy-start.13 = (bf16[16,144,128]{2,1,0:T(8,128)(2,1)}, bf16[16,144,128]{2,1,0:T(8,128)(2,1)S(1)}, u32[]{:S(2)}) copy-start(bf16[16,144,128]{2,1,0:T(8,128)(2,1)S(1)} %all_to_all.21.refs_0_) | copy-start | bytes 1769476
  135.8 15.2 %collective-permute-start.14 = (bf16[16,144,128]{2,1,0:T(8,128)(2,1)S(1)}, bf16[16,144,128]{2,1,0:T(8,128)(2,1)S(1)}, u32[]{:S(2)}, u32[]{:S(2)}) collective-permute-start(bf16[16,144,128]{2,1,0:T(8,128)(2,1)S(1)} %all_to_all.21.refs_0_), channel_id=1, source_target_pairs={{0,2},{2,4},{4,6},{6,0},{1,3},{3,5},{5,7},{7,1},{8,10},{10,12},{12... | collective-permute-start | bytes 1769480 | tf_op jit(solution)/shard_map/ppermute | solution.py:38
  138.0 14.9 %collective-permute-start.15 = (bf16[16,144,128]{2,1,0:T(8,128)(2,1)S(1)}, bf16[16,144,128]{2,1,0:T(8,128)(2,1)S(1)}, u32[]{:S(2)}, u32[]{:S(2)}) collective-permute-start(bf16[16,144,128]{2,1,0:T(8,128)(2,1)S(1)} %all_to_all.21.refs_0_), channel_id=1, source_target_pairs={{0,6},{2,0},{4,2},{6,4},{1,7},{3,1},{5,3},{7,5},{8,14},{10,8},{12,... | collective-permute-start | bytes 1769480 | tf_op jit(solution)/shard_map/ppermute | solution.py:38
  150.9 25.7 %copy-start.8 = (bf16[16,144,128]{2,1,0:T(8,128)(2,1)}, bf16[16,144,128]{2,1,0:T(8,128)(2,1)S(1)}, u32[]{:S(2)}) copy-start(bf16[16,144,128]{2,1,0:T(8,128)(2,1)S(1)} %collective-permute-done.14.refs_1_) | copy-start | bytes 1769476
  151.0 22.1 %collective-permute-start.16 = (bf16[8,144,128]{2,1,0:T(8,128)(2,1)S(1)}, bf16[8,144,128]{2,1,0:T(8,128)(2,1)S(1)}, u32[]{:S(2)}, u32[]{:S(2)}) collective-permute-start(bf16[8,144,128]{2,1,0:T(8,128)(2,1)S(1)} %slice.59), channel_id=1, source_target_pairs={{0,2},{2,4},{4,6},{6,0},{1,3},{3,5},{5,7},{7,1},{8,10},{10,12},{12... | collective-permute-start | bytes 884744 | tf_op jit(solution)/shard_map/ppermute | solution.py:43
  152.9 23.7 %copy-start.9 = (bf16[16,144,128]{2,1,0:T(8,128)(2,1)}, bf16[16,144,128]{2,1,0:T(8,128)(2,1)S(1)}, u32[]{:S(2)}) copy-start(bf16[16,144,128]{2,1,0:T(8,128)(2,1)S(1)} %collective-permute-done.15.refs_2_) | copy-start | bytes 1769476
  152.9 23.7 %collective-permute-start.17 = (bf16[8,144,128]{2,1,0:T(8,128)(2,1)S(1)}, bf16[8,144,128]{2,1,0:T(8,128)(2,1)S(1)}, u32[]{:S(2)}, u32[]{:S(2)}) collective-permute-start(bf16[8,144,128]{2,1,0:T(8,128)(2,1)S(1)} %slice.60), channel_id=1, source_target_pairs={{0,6},{2,0},{4,2},{6,4},{1,7},{3,1},{5,3},{7,5},{8,14},{10,8},{12,... | collective-permute-start | bytes 884744 | tf_op jit(solution)/shard_map/ppermute | solution.py:43
  158.9 44.7 %collective-permute-start.22 = (bf16[256,512]{1,0:T(8,128)(2,1)S(1)}, bf16[256,512]{1,0:T(8,128)(2,1)}, u32[]{:S(2)}, u32[]{:S(2)}) collective-permute-start(bf16[256,512]{1,0:T(8,128)(2,1)S(1)} %pad_maximum_fusion.3), channel_id=1, source_target_pairs={{0,8},{8,16},{16,24},{24,0},{1,9},{9,17},{17,25},{25,1},{2,10},{10... | collective-permute-start | bytes 786440 | tf_op jit(solution)/shard_map/ppermute | solution.py:38
  161.6 37.5 %collective-permute-start.23 = (bf16[256,512]{1,0:T(8,128)(2,1)S(1)}, bf16[256,512]{1,0:T(8,128)(2,1)}, u32[]{:S(2)}, u32[]{:S(2)}) collective-permute-start(bf16[256,512]{1,0:T(8,128)(2,1)S(1)} %pad_maximum_fusion.3), channel_id=1, source_target_pairs={{0,24},{8,0},{16,8},{24,16},{1,25},{9,1},{17,9},{25,17},{2,26},{10... | collective-permute-start | bytes 786440 | tf_op jit(solution)/shard_map/ppermute | solution.py:38
  171.1 14.1 %collective-permute-start.10 = (bf16[2,1,2,2,64,128]{5,4,3,2,1,0:T(8,128)(2,1)}, bf16[2,1,2,2,64,128]{5,4,3,2,1,0:T(8,128)(2,1)S(1)}, u32[]{:S(2)}, u32[]{:S(2)}) collective-permute-start(bf16[2,1,2,2,64,128]{5,4,3,2,1,0:T(8,128)(2,1)} %get-tuple-element.17), channel_id=1, source_target_pairs={{0,6},{2,0},{4,2},{6,4},{1,7},{3,1},{5,3},{7,5},{8,14},{10,8},{12,... | collective-permute-start | bytes 393224 | tf_op jit(solution)/shard_map/ppermute | solution.py:377
  173.1 12.1 %copy-start.23 = (bf16[2,1,2,2,64,128]{5,4,3,2,1,0:T(8,128)(2,1)S(1)}, bf16[2,1,2,2,64,128]{5,4,3,2,1,0:T(8,128)(2,1)}, u32[]{:S(2)}) copy-start(bf16[2,1,2,2,64,128]{5,4,3,2,1,0:T(8,128)(2,1)} %get-tuple-element.16) | copy-start | bytes 393220
  173.1 12.1 %copy-start.27 = (bf16[2,1,2,2,64,128]{5,4,3,2,1,0:T(8,128)(2,1)S(1)}, bf16[2,1,2,2,64,128]{5,4,3,2,1,0:T(8,128)(2,1)}, u32[]{:S(2)}) copy-start(bf16[2,1,2,2,64,128]{5,4,3,2,1,0:T(8,128)(2,1)} %get-tuple-element.19) | copy-start | bytes 393220
  173.1 14.1 %collective-permute-start.11 = (bf16[2,1,2,2,64,128]{5,4,3,2,1,0:T(8,128)(2,1)}, bf16[2,1,2,2,64,128]{5,4,3,2,1,0:T(8,128)(2,1)S(1)}, u32[]{:S(2)}, u32[]{:S(2)}) collective-permute-start(bf16[2,1,2,2,64,128]{5,4,3,2,1,0:T(8,128)(2,1)} %get-tuple-element.18), channel_id=1, source_target_pairs={{0,2},{2,4},{4,6},{6,0},{1,3},{3,5},{5,7},{7,1},{8,10},{10,12},{12... | collective-permute-start | bytes 393224 | tf_op jit(solution)/shard_map/ppermute | solution.py:377
  178.1 41.5 %collective-permute-start.19 = (bf16[48,144,128]{2,1,0:T(8,128)(2,1)}, bf16[48,144,128]{2,1,0:T(8,128)(2,1)}, u32[]{:S(2)}, u32[]{:S(2)}) collective-permute-start(bf16[48,144,128]{2,1,0:T(8,128)(2,1)} %pad_maximum_fusion), channel_id=1, source_target_pairs={{0,1},{1,0},{2,3},{3,2},{4,5},{5,4},{6,7},{7,6},{8,9},{9,8},{10,11... | collective-permute-start | bytes 5308424 | tf_op jit(solution)/shard_map/ppermute | solution.py:30
  185.3 8.4 %collective-permute-start.12 = (bf16[2,1,2,2,64,128]{5,4,3,2,1,0:T(8,128)(2,1)S(1)}, bf16[2,1,2,2,64,128]{5,4,3,2,1,0:T(8,128)(2,1)S(1)}, u32[]{:S(2)}, u32[]{:S(2)}) collective-permute-start(bf16[2,1,2,2,64,128]{5,4,3,2,1,0:T(8,128)(2,1)S(1)} %copy-done.27), channel_id=1, source_target_pairs={{0,4},{2,6},{4,0},{6,2},{1,5},{3,7},{5,1},{7,3},{8,12},{10,14},{12... | collective-permute-start | bytes 393224 | tf_op jit(solution)/shard_map/ppermute | solution.py:377
  194.5 65.4 %copy-start.15 = (bf16[4,2,2,64,128]{4,3,2,1,0:T(8,128)(2,1)}, bf16[4,2,2,64,128]{4,3,2,1,0:T(8,128)(2,1)S(1)}, u32[]{:S(2)}) copy-start(bf16[4,2,2,64,128]{4,3,2,1,0:T(8,128)(2,1)S(1)} %get-tuple-element.28.in_ref) | copy-start | bytes 786436
  194.5 25.1 %all-to-all-start.2 = ((bf16[16,64,128]{2,1,0:T(8,128)(2,1)}), bf16[16,64,128]{2,1,0:T(8,128)(2,1)S(1)}, u32[]{:S(2)}, u32[]{:S(2)}) async-start(bf16[16,64,128]{2,1,0:T(8,128)(2,1)} %bitcast.13), calls=%async_computation.2 | async-start | bytes 524288 | tf_op jit(solution)/shard_map/all_to_all | solution.py:383
  200.0 12.1 %collective-permute-start.25 = (bf16[128,512]{1,0:T(8,128)(2,1)S(1)}, bf16[128,512]{1,0:T(8,128)(2,1)S(1)}, u32[]{:S(2)}, u32[]{:S(2)}) collective-permute-start(bf16[128,512]{1,0:T(8,128)(2,1)S(1)} %slice.62), channel_id=1, source_target_pairs={{0,24},{8,0},{16,8},{24,16},{1,25},{9,1},{17,9},{25,17},{2,26},{10... | collective-permute-start | bytes 393224 | tf_op jit(solution)/shard_map/ppermute | solution.py:43
  204.6 7.5 %collective-permute-start.24 = (bf16[128,512]{1,0:T(8,128)(2,1)S(1)}, bf16[128,512]{1,0:T(8,128)(2,1)S(1)}, u32[]{:S(2)}, u32[]{:S(2)}) collective-permute-start(bf16[128,512]{1,0:T(8,128)(2,1)S(1)} %slice.61), channel_id=1, source_target_pairs={{0,8},{8,16},{16,24},{24,0},{1,9},{9,17},{17,25},{25,1},{2,10},{10... | collective-permute-start | bytes 393224 | tf_op jit(solution)/shard_map/ppermute | solution.py:43
  207.5 12.0 %collective-permute-start.18 = (bf16[16,144,128]{2,1,0:T(8,128)(2,1)S(1)}, bf16[16,144,128]{2,1,0:T(8,128)(2,1)}, u32[]{:S(2)}, u32[]{:S(2)}) collective-permute-start(bf16[16,144,128]{2,1,0:T(8,128)(2,1)S(1)} %all_to_all.21.refs_0_), channel_id=1, source_target_pairs={{0,1},{1,0},{2,3},{3,2},{4,5},{5,4},{6,7},{7,6},{8,9},{9,8},{10,11... | collective-permute-start | bytes 1769480 | tf_op jit(solution)/shard_map/ppermute | solution.py:30
  212.2 28.6 %copy-start.7 = (bf16[4,256,512]{2,1,0:T(8,128)(2,1)}, bf16[4,256,512]{2,1,0:T(8,128)(2,1)S(1)}, u32[]{:S(2)}) copy-start(bf16[4,256,512]{2,1,0:T(8,128)(2,1)S(1)} %fusion.refs_0_) | copy-start | bytes 3145732
  212.2 40.1 %collective-permute-start.26 = (bf16[4,256,512]{2,1,0:T(8,128)(2,1)S(1)}, bf16[4,256,512]{2,1,0:T(8,128)(2,1)S(1)}, u32[]{:S(2)}, u32[]{:S(2)}) collective-permute-start(bf16[4,256,512]{2,1,0:T(8,128)(2,1)S(1)} %fusion.refs_0_), channel_id=1, source_target_pairs={{0,2},{2,4},{4,6},{6,0},{1,3},{3,5},{5,7},{7,1},{8,10},{10,12},{12... | collective-permute-start | bytes 3145736 | tf_op jit(solution)/shard_map/ppermute | solution.py:38
  214.1 38.1 %collective-permute-start.27 = (bf16[4,256,512]{2,1,0:T(8,128)(2,1)S(1)}, bf16[4,256,512]{2,1,0:T(8,128)(2,1)}, u32[]{:S(2)}, u32[]{:S(2)}) collective-permute-start(bf16[4,256,512]{2,1,0:T(8,128)(2,1)S(1)} %fusion.refs_0_), channel_id=1, source_target_pairs={{0,6},{2,0},{4,2},{6,4},{1,7},{3,1},{5,3},{7,5},{8,14},{10,8},{12,... | collective-permute-start | bytes 3145736 | tf_op jit(solution)/shard_map/ppermute | solution.py:38
  240.8 35.4 %all-to-all-start.3 = ((bf16[16,64,128]{2,1,0:T(8,128)(2,1)}), bf16[16,64,128]{2,1,0:T(8,128)(2,1)S(1)}, u32[]{:S(2)}, u32[]{:S(2)}) async-start(bf16[16,64,128]{2,1,0:T(8,128)(2,1)} %attend.1), calls=%async_computation.3 | async-start | bytes 524288 | tf_op jit(solution)/shard_map/all_to_all | solution.py:413
  252.3 27.4 %copy-start.14 = (bf16[4,256,512]{2,1,0:T(8,128)(2,1)}, bf16[4,256,512]{2,1,0:T(8,128)(2,1)S(1)}, u32[]{:S(2)}) copy-start(bf16[4,256,512]{2,1,0:T(8,128)(2,1)S(1)} %collective-permute-done.26.refs_1_) | copy-start | bytes 3145732
  252.3 25.9 %collective-permute-start.28 = (bf16[2,256,512]{2,1,0:T(8,128)(2,1)S(1)}, bf16[2,256,512]{2,1,0:T(8,128)(2,1)S(1)}, u32[]{:S(2)}, u32[]{:S(2)}) collective-permute-start(bf16[2,256,512]{2,1,0:T(8,128)(2,1)S(1)} %slice.50), channel_id=1, source_target_pairs={{0,2},{2,4},{4,6},{6,0},{1,3},{3,5},{5,7},{7,1},{8,10},{10,12},{12... | collective-permute-start | bytes 1572872 | tf_op jit(solution)/shard_map/ppermute | solution.py:43
  255.3 22.9 %collective-permute-start.29 = (bf16[2,256,512]{2,1,0:T(8,128)(2,1)S(1)}, bf16[2,256,512]{2,1,0:T(8,128)(2,1)}, u32[]{:S(2)}, u32[]{:S(2)}) collective-permute-start(bf16[2,256,512]{2,1,0:T(8,128)(2,1)S(1)} %slice.51), channel_id=1, source_target_pairs={{0,6},{2,0},{4,2},{6,4},{1,7},{3,1},{5,3},{7,5},{8,14},{10,8},{12,... | collective-permute-start | bytes 1572872 | tf_op jit(solution)/shard_map/ppermute | solution.py:43
  259.9 6.6 %collective-permute-start.13 = (bf16[4,2,2,16,128]{4,3,2,1,0:T(8,128)(2,1)S(1)}, bf16[4,2,2,16,128]{4,3,2,1,0:T(8,128)(2,1)S(1)}, u32[]{:S(2)}, u32[]{:S(2)}) collective-permute-start(bf16[4,2,2,16,128]{4,3,2,1,0:T(8,128)(2,1)S(1)} %slice.57), channel_id=1, source_target_pairs={{0,1},{1,2},{2,3},{3,4},{4,5},{5,6},{6,7},{7,32},{32,33},{33,34},{... | collective-permute-start | bytes 196616 | tf_op jit(solution)/shard_map/ppermute | solution.py:386
  269.3 8.9 %collective-permute-start.20 = (bf16[4,2,2,64,128]{4,3,2,1,0:T(8,128)(2,1)}, bf16[4,2,2,64,128]{4,3,2,1,0:T(8,128)(2,1)S(1)}, u32[]{:S(2)}, u32[]{:S(2)}) collective-permute-start(bf16[4,2,2,64,128]{4,3,2,1,0:T(8,128)(2,1)} %pool.1.pool_ref), channel_id=1, source_target_pairs={{0,1},{1,0},{2,3},{3,2},{4,5},{5,4},{6,7},{7,6},{8,9},{9,8},{10,11... | collective-permute-start | bytes 786440 | tf_op jit(solution)/shard_map/ppermute | solution.py:30
  276.2 3.4 %collective-permute-start.21 = (bf16[4,2,2,64,128]{4,3,2,1,0:T(8,128)(2,1)S(1)}, bf16[4,2,2,64,128]{4,3,2,1,0:T(8,128)(2,1)S(1)}, u32[]{:S(2)}, u32[]{:S(2)}) collective-permute-start(bf16[4,2,2,64,128]{4,3,2,1,0:T(8,128)(2,1)S(1)} %bitcast.30), channel_id=1, source_target_pairs={{0,1},{1,0},{2,3},{3,2},{4,5},{5,4},{6,7},{7,6},{8,9},{9,8},{10,11... | collective-permute-start | bytes 786440 | tf_op jit(solution)/shard_map/ppermute | solution.py:30
  285.8 4.0 %collective-permute-start.30 = (bf16[2,64,2048]{2,1,0:T(8,128)(2,1)}, bf16[2,64,2048]{2,1,0:T(8,128)(2,1)S(1)}, u32[]{:S(2)}, u32[]{:S(2)}) collective-permute-start(bf16[2,64,2048]{2,1,0:T(8,128)(2,1)} %get-tuple-element.26), channel_id=1, source_target_pairs={{0,1},{1,0},{2,3},{3,2},{4,5},{5,4},{6,7},{7,6},{8,9},{9,8},{10,11... | collective-permute-start | bytes 1572872 | tf_op jit(solution)/shard_map/ppermute | solution.py:30
  (13 other events, 38.5 us)

commit v4 on v3

--- a/solution.py
+++ b/solution.py
@@ -12,6 +12,7 @@
 EPS = 1e-06
 MASKED = -1e30
 GATE_ROWS = 16
+WIDE = 4
 LOG2E = 1.4426950408889634
 F32 = jnp.float32
 BF16 = jnp.bfloat16
@@ -48,6 +49,11 @@
     return (x, *near, *relays(*near, axis))
 
 
+def ring_in_three(x, axis):
+    near = hops(x, axis)
+    return (x, *near, lax.ppermute(near[0], axis, UP))
+
+
 def rms(x):
     wide = x.astype(F32)
     return lax.rsqrt(jnp.mean(wide * wide, axis=-1, keepdims=True) + EPS)
@@ -56,16 +62,16 @@
 def factors_of(rows_of):
     seqs, rows, _ = rows_of[0].shape
 
-    def body(x0, x1, x2, x3, x4, out_ref):
+    def body(x0, x1, x2, x3, out_ref):
         at = 0
-        for ref in (x0, x1, x2, x3, x4):
+        for ref in (x0, x1, x2, x3):
             for i in range(ref.shape[0]):
                 out_ref[at : at + rows] = rms(ref[i])
                 at += rows
 
     return pl.pallas_call(
         body,
-        in_specs=[whole()] * 5,
+        in_specs=[whole()] * 4,
         out_specs=whole(),
         out_shape=jax.ShapeDtypeStruct((4 * seqs * rows, 1), F32),
         compiler_params=params(),
@@ -78,7 +84,7 @@
     kinds = len(factors)
 
     def body(p_ref, norm_ref, *refs):
-        xs, own_refs, other_refs, outs = refs[:5], refs[5:10], refs[10:12], refs[12:]
+        xs, own_refs, other_refs, outs = refs[:4], refs[4:8], refs[8:10], refs[10:]
         deep = own_refs[0].shape[0] - GATE_ROWS
         tall = deep + GATE_ROWS
         r = norm_ref[...]
@@ -92,9 +98,7 @@
                     [ref[i, :, at] for ref in xs for i in range(ref.shape[0])], axis=0
                 )
             )
-        own = [ref[:deep, cols] for ref in own_refs[:3]]
-        far = jnp.concatenate([ref[:, cols] for ref in own_refs[3:]], axis=0)
-        own.append(far[:deep])
+        own = [ref[:deep, cols] for ref in own_refs]
         other = [other_refs[0][:deep, cols]]
         other += [other_refs[1][n * tall : n * tall + deep, cols] for n in range(3)]
         for ref, ws, head in (
@@ -140,7 +144,7 @@
         shapes = [(4, seqs, 2, kinds * rows + GATE_ROWS, HD)]
     outs = pl.pallas_call(
         body,
-        in_specs=[whole(pltpu.SMEM)] + [whole()] * 13,
+        in_specs=[whole(pltpu.SMEM)] + [whole()] * 11,
         out_specs=[whole()] * len(shapes),
         out_shape=[jax.ShapeDtypeStruct(sh, BF16) for sh in shapes],
         compiler_params=params(),
@@ -149,17 +153,32 @@
     return outs
 
 
-def attend(q, own, other, key_place, query_place):
+def attend(places, q, own, other):
     blocks, rows, _ = q.shape
     span = 8 * rows
     group = 4
     tall = group * rows
     count = blocks // group
-
-    def body(q_ref, *refs):
-        kvs, (kp_ref, qp_ref, out_ref, acc_ref, top_ref) = refs[:7], refs[7:]
-        ones = jnp.ones((span, HD), BF16)
-        left = lax.broadcasted_iota(jnp.int32, (1, HD), 1) < rows
+    wide = WIDE
+
+    def body(p_ref, q_ref, *refs):
+        kvs, (out_ref, acc_ref, top_ref) = refs[:7], refs[7:]
+        ones = jnp.ones((wide * span, HD), BF16)
+        lane = lax.broadcasted_iota(jnp.int32, (1, HD), 1)
+        left = lane < rows
+        c = p_ref[0]
+        bases = [(2 * p_ref[1 + n] + c) * rows for n in range(4)]
+        bases += [(2 * p_ref[1 + n] + 1 - c) * rows for n in range(4)]
+        key_at = jnp.concatenate(
+            [
+                jnp.where(left, lane + bases[n], lane - rows + bases[n + 1])
+                for n in range(0, 8, 2)
+            ],
+            axis=1,
+        )
+        key_at = jnp.concatenate([key_at + n * span for n in range(wide)], axis=1)
+        row = lax.broadcasted_iota(jnp.int32, (tall, 1), 0)
+        query_at = (row // rows) * span + row % rows + bases[0]
 
         def blocks_of(s, late, at):
             far = kvs[4][s - blocks // 2, at] if late else kvs[3][s, at]
@@ -167,16 +186,19 @@
                 kvs[6][s + n * blocks, at] for n in range(3)
             ]
 
+        def several(s, late, at):
+            return [p for n in range(wide) for p in blocks_of(s + n, late, at)]
+
         def gates(s, late):
-            parts = blocks_of(s, late, slice(2 * rows, 2 * rows + GATE_ROWS))
+            parts = several(s, late, slice(2 * rows, 2 * rows + GATE_ROWS))
             parts = [jnp.sum(part.astype(F32)[:3], axis=0, keepdims=True) for part in parts]
             return LOG2E * jnp.concatenate(
-                [jnp.where(left, parts[n], parts[n + 1]) for n in range(0, 8, 2)], axis=1
+                [jnp.where(left, parts[n], parts[n + 1]) for n in range(0, 8 * wide, 2)], axis=1
             )
 
         def step(s, first_group, fresh, late):
-            k = jnp.concatenate(blocks_of(s, late, slice(0, rows)), axis=0)
-            v = jnp.concatenate(blocks_of(s, late, slice(rows, 2 * rows)), axis=0)
+            k = jnp.concatenate(several(s, late, slice(0, rows)), axis=0)
+            v = jnp.concatenate(several(s, late, slice(rows, 2 * rows)), axis=0)
             v = jnp.concatenate([v, ones], axis=1)
             gate = gates(s, late)
             for g in range(first_group, count):
@@ -187,7 +209,7 @@
                 )
                 sc = sc - gate
                 if g == first_group:
-                    sc = jnp.where(kp_ref[...] + s * span <= qp_ref[at], sc, MASKED)
+                    sc = jnp.where(key_at + (s - g * group) * span <= query_at, sc, MASKED)
                 new = jnp.max(sc, axis=1, keepdims=True)
                 if fresh:
                     p = jnp.exp2(sc - new).astype(BF16)
@@ -204,11 +226,11 @@
         step(0, 0, True, False)
         for r in range(count):
 
-            def loop(s, carry, r=r):
-                step(s, r, False, 2 * r >= count)
+            def loop(n, carry, r=r):
+                step(n * wide, r, False, 2 * r >= count)
                 return carry
 
-            lax.fori_loop(max(1, r * group), (r + 1) * group, loop, 0)
+            lax.fori_loop(max(1, r * group // wide), (r + 1) * group // wide, loop, 0)
         for g in range(count):
             acc = acc_ref[g * tall : (g + 1) * tall]
             out_ref[g * group : (g + 1) * group] = (
@@ -217,7 +239,7 @@
 
     return pl.pallas_call(
         body,
-        in_specs=[whole()] * 10,
+        in_specs=[whole(pltpu.SMEM)] + [whole()] * 8,
         out_specs=whole(),
         out_shape=jax.ShapeDtypeStruct(q.shape, BF16),
         scratch_shapes=[
@@ -226,7 +248,7 @@
         ],
         compiler_params=params(),
         name="attend",
-    )(q, *own, *other, key_place, query_place)
+    )(places, q, *own, *other)
 
 
 def pool(first, rows_in, border, mix, scale):
@@ -351,7 +373,7 @@
 
     deep = w_key.shape[0]
     gain = lax.dynamic_slice_in_dim(norm_gain, y * deep, deep, 0)
-    all_rows = ring_of_four(tokens, "tp_0")
+    all_rows = ring_in_three(tokens, "tp_0")
     norm = factors_of(all_rows)
     weights = jnp.concatenate([w_key, w_value, w_query, w_pool_in], axis=1)
     weights = (weights.astype(F32) * gain[:, None]).astype(BF16)
@@ -361,7 +383,7 @@
     middle = lax.reduce_precision(rest, 8, 7)
     parts = jnp.stack([high, middle, rest - middle], axis=1).astype(BF16)
     parts = jnp.pad(parts, ((0, 0), (0, 5), (0, 0))).reshape(GATE_ROWS, block)
-    own_w = ring_of_four(jnp.concatenate([weights, parts], axis=0), "fs")
+    own_w = ring_in_three(jnp.concatenate([weights, parts], axis=0), "fs")
     other_w = sibling(own_w[0])
     other_w = (other_w, sibling(jnp.concatenate(own_w[1:], axis=0)))
 
@@ -395,19 +417,11 @@
     kv_other = (kv_other, sibling(jnp.concatenate(kv_own[1:], axis=0)))
 
     out_w = jnp.concatenate([w_out_pool, w_out_attn], axis=0)
-    o = ring_of_four(after(out_w, own_w[1]), "fs")
-    o = [o[0], o[1], o[2], jnp.concatenate(o[3:], axis=0)]
+    o = ring_in_three(after(out_w, own_w[1]), "fs")
     o = placed([w[None] for w in o], deeps, 0)
     out_near = hops(after(o, kv_here), "tp_0")
 
-    at = jnp.arange(rows, dtype=jnp.int32)
-    key_place = jnp.concatenate(
-        [((2 * s + cc) * rows + at) for cc in (c, 1 - c) for s in seen]
-    ).reshape(1, -1).astype(jnp.int32)
-    query_place = (
-        jnp.arange(planes, dtype=jnp.int32)[:, None] * block + (2 * x + c) * rows + at[None]
-    ).reshape(-1, 1)
-    attn = attend(q, kv_own, kv_other, key_place, query_place)
+    attn = attend(places, q, kv_own, kv_other)
     out_near = lax.optimization_barrier((*out_near, attn))[:2]
     out_own = (o, *out_near, *relays(*out_near, "tp_0"))
     attn = lax.all_to_all(attn, "sp", 0, 0, tiled=True)

time: 294 us -> 280 us (0.952)
  waiting for transfers between devices: 46.5 us -> 73 us
  starting transfers between devices: 121 us -> 99.2 us
  Pallas kernels: 40.8 us -> 30.6 us
  local copies, waits for them, and re-layouts: 15.6 us -> 8 us
    ppermute x0 -> x3, waiting for transfers between devices: none -> 25.6 us  [ring_in_three(): return (x, *near, lax.ppermute(near[0], axis, UP))]
    ppermute x5 -> x2, starting transfers between devices: 21.9 us -> 8.87 us  [relays(): lax.ppermute(after[half:], axis, DOWN)]
    pallas_call x4, Pallas kernels: 33.3 us -> 23.1 us  [the longest x1 10.3 us: attend(): pl.pallas_call(body, in_specs=[whole(pltpu.SMEM)] + [whole()] * 8, out_sp...]
    all_to_all x1, waiting for transfers between devices: 0.01 us -> 6.44 us  [on_device(): q = lax.all_to_all(q, 'sp', 0, 0, tiled=True)]
    ppermute x0 -> x3, starting transfers between devices: none -> 5.74 us  [ring_in_three(): return (x, *near, lax.ppermute(near[0], axis, UP))]
    ppermute x5 -> x2, starting transfers between devices: 9.72 us -> 4.12 us  [relays(): lax.ppermute(before[:half], axis, UP)]
    ppermute x5 -> x2, waiting for transfers between devices: 5.58 us -> 0.01 us  [relays(): lax.ppermute(before[:half], axis, UP)]
    all_to_all x1, starting transfers between devices: 11.5 us -> 6.24 us  [on_device(): attn = lax.all_to_all(attn, 'sp', 0, 0, tiled=True)]
  transfers between devices with their start and end apart: 33 -> 30, of which waited for: 11 -> 12; matrix products, arithmetic and copies ran while one was open for 4% -> 2% of each run, Pallas kernels for 10% -> 7%
where the time goes in v4:
time: 280 us; the launch traced here: 279 us
  starting transfers between devices  99.2 us (35%)
  waiting for transfers between devices  73 us (26%)
  blocking collectives  59.2 us (21%)
  Pallas kernels  30.6 us (11%)
  local copies, waits for them, and re-layouts  8 us (3%)
  other arithmetic  7.82 us (3%)
    all_to_all x1, blocking collectives, on_device(): lax.all_to_all(kv_here.reshape(planes, 2 * rows + GATE_ROWS, HD), 'sp', 0...  47.4 us
    ppermute x10, starting transfers between devices, hops(): return (lax.ppermute(x, axis, UP), lax.ppermute(x, axis, DOWN))  32.7 us
    ppermute x10, waiting for transfers between devices, hops(): return (lax.ppermute(x, axis, UP), lax.ppermute(x, axis, DOWN))  28.1 us
    ppermute x7, starting transfers between devices, sibling(): return lax.ppermute(x, 'tp_1', [(0, 1), (1, 0)])  26.4 us
    ppermute x3, waiting for transfers between devices, ring_in_three(): return (x, *near, lax.ppermute(near[0], axis, UP))  25.6 us
    all_to_all x1, blocking collectives, on_device(): kv_here = lax.all_to_all(kv, 'tp_0', 0, 0, tiled=True)  11.8 us
    pallas_call x1, Pallas kernels, attend(): pl.pallas_call(body, in_specs=[whole(pltpu.SMEM)] + [whole()] * 8, out_sp...  10.3 us
    pallas_call x2, Pallas kernels, project(): pl.pallas_call(body, in_specs=[whole(pltpu.SMEM)] + [whole()] * 11, out_s...  10 us
  transfers between devices with their start and end apart: 30, of which 12 were waited for; matrix products, arithmetic and copies ran while one was open for 2% of the time, Pallas kernels for 7%

profile of v4, /device:TPU:33, one launch (start us, length us, event | category | flops | bytes accessed | tf_op | source)
XLA Modules:
  0.0 278.6 jit_solution(15519805864938104092)
XLA Ops:
  3.6 3.2 %collective-permute-start.3 = (bf16[528,512]{1,0:T(8,128)(2,1)}, bf16[528,512]{1,0:T(8,128)(2,1)S(1)}, u32[]{:S(2)}, u32[]{:S(2)}) collective-permute-start(bf16[528,512]{1,0:T(8,128)(2,1)} %pad_maximum_fusion.2.refs_4_), channel_id=1, source_target_pairs={{0,8},{8,16},{16,24},{24,0},{1,9},{9,17},{17,25},{25,1},{2,10},{10... | collective-permute-start | bytes 1622024 | tf_op jit(solution)/shard_map/ppermute | solution.py:39
  6.8 3.4 %collective-permute-start.4 = (bf16[528,512]{1,0:T(8,128)(2,1)}, bf16[528,512]{1,0:T(8,128)(2,1)S(1)}, u32[]{:S(2)}, u32[]{:S(2)}) collective-permute-start(bf16[528,512]{1,0:T(8,128)(2,1)} %pad_maximum_fusion.2.refs_4_), channel_id=1, source_target_pairs={{0,24},{8,0},{16,8},{24,16},{1,25},{9,1},{17,9},{25,17},{2,26},{10... | collective-permute-start | bytes 1622024 | tf_op jit(solution)/shard_map/ppermute | solution.py:39
  10.2 10.0 %collective-permute-done.3.refs_5_ = bf16[528,512]{1,0:T(8,128)(2,1)S(1)} collective-permute-done((bf16[528,512]{1,0:T(8,128)(2,1)}, bf16[528,512]{1,0:T(8,128)(2,1)S(1)}, u32[]{:S(2)}, u32[]{:S(2)}) %collective-permute-start.3) | collective-permute-done | bytes 540704 | tf_op jit(solution)/shard_map/ppermute | solution.py:39
  22.1 13.5 %collective-permute-done.5.refs_7_ = bf16[528,512]{1,0:T(8,128)(2,1)S(1)} collective-permute-done((bf16[528,512]{1,0:T(8,128)(2,1)S(1)}, bf16[528,512]{1,0:T(8,128)(2,1)S(1)}, u32[]{:S(2)}, u32[]{:S(2)}) %collective-permute-start.5) | collective-permute-done | bytes 540704 | tf_op jit(solution)/shard_map/ppermute | solution.py:54
  37.0 4.2 %collective-permute-start.7 = (bf16[1584,512]{1,0:T(8,128)(2,1)}, bf16[1584,512]{1,0:T(8,128)(2,1)S(1)}, u32[]{:S(2)}, u32[]{:S(2)}) collective-permute-start(bf16[1584,512]{1,0:T(8,128)(2,1)} %pad_maximum_fusion.1), channel_id=1, source_target_pairs={{0,1},{1,0},{2,3},{3,2},{4,5},{5,4},{6,7},{7,6},{8,9},{9,8},{10,11... | collective-permute-start | bytes 4866056 | tf_op jit(solution)/shard_map/ppermute | solution.py:31
  41.3 3.1 %collective-permute-start = (bf16[2,64,2048]{2,1,0:T(8,128)(2,1)}, bf16[2,64,2048]{2,1,0:T(8,128)(2,1)}, u32[]{:S(2)}, u32[]{:S(2)}) collective-permute-start(bf16[2,64,2048]{2,1,0:T(8,128)(2,1)} %refs_0_.3), channel_id=1, source_target_pairs={{0,2},{2,4},{4,6},{6,0},{1,3},{3,5},{5,7},{7,1},{8,10},{10,12},{12... | collective-permute-start | bytes 1572872 | tf_op jit(solution)/shard_map/ppermute | solution.py:39
  44.4 2.2 collective-permute-start.6
  46.6 3.4 %collective-permute-start.1 = (bf16[2,64,2048]{2,1,0:T(8,128)(2,1)}, bf16[2,64,2048]{2,1,0:T(8,128)(2,1)}, u32[]{:S(2)}, u32[]{:S(2)}) collective-permute-start(bf16[2,64,2048]{2,1,0:T(8,128)(2,1)} %refs_0_.3), channel_id=1, source_target_pairs={{0,6},{2,0},{4,2},{6,4},{1,7},{3,1},{5,3},{7,5},{8,14},{10,8},{12,... | collective-permute-start | bytes 1572872 | tf_op jit(solution)/shard_map/ppermute | solution.py:39
  50.0 8.2 %collective-permute-done.x1.refs_1_ = bf16[2,64,2048]{2,1,0:T(8,128)(2,1)} collective-permute-done((bf16[2,64,2048]{2,1,0:T(8,128)(2,1)}, bf16[2,64,2048]{2,1,0:T(8,128)(2,1)}, u32[]{:S(2)}, u32[]{:S(2)}) %collective-permute-start) | collective-permute-done | bytes 524320 | tf_op jit(solution)/shard_map/ppermute | solution.py:39
  58.2 1.9 collective-permute-start.2
  62.1 12.1 %collective-permute-done.2.x3.refs_3_ = bf16[2,64,2048]{2,1,0:T(8,128)(2,1)} collective-permute-done((bf16[2,64,2048]{2,1,0:T(8,128)(2,1)}, bf16[2,64,2048]{2,1,0:T(8,128)(2,1)}, u32[]{:S(2)}, u32[]{:S(2)}) %collective-permute-start.2) | collective-permute-done | bytes 524320 | tf_op jit(solution)/shard_map/ppermute | solution.py:54
  74.2 2.7 factors.1.norm_ref
  78.1 5.1 %project.3 = bf16[4,2,2,144,128]{4,3,2,1,0:T(8,128)(2,1)} custom-call(s32[9]{0:T(128)} %stack.46.p_ref, f32[512,1]{1,0:T(8,128)} %factors.1.norm_ref, bf16[2,64,2048]{2,1,0:T(8,128)(2,1)} %refs_0_.3, bf16[2,64,2048]{2,1,0:T(8,128)(2,1)} %collective-permute-done.x1.refs_1_, bf16[2,64,2048]{2,1,0:T(8,128)(2,1)} %collective-permute-done.1.x2.refs_2_, ...), custom_call_target="tpu_custom_call" | custom-call | tf_op jit(solution)/shard_map/project/pallas_call | solution.py:145
  83.2 11.8 %all_to_all.20 = bf16[4,2,2,144,128]{4,3,2,1,0:T(8,128)(2,1)S(1)} all-to-all(bf16[4,2,2,144,128]{4,3,2,1,0:T(8,128)(2,1)} %project.3), channel_id=1, replica_groups=mesh['sp'=16,'fs'=4,'tp_0'=4,'tp_1'=2] {'tp_0'}, dimensions={0} | all-to-all | bytes 1179648 | tf_op jit(solution)/shard_map/all_to_all | solution.py:391
  95.1 47.4 %all_to_all.21.refs_0_ = bf16[16,144,128]{2,1,0:T(8,128)(2,1)S(1)} all-to-all(bf16[16,144,128]{2,1,0:T(8,128)(2,1)S(1)} %bitcast.26), channel_id=1, replica_groups=mesh['sp'=16,'fs'=4,'tp_0'=4,'tp_1'=2] {'sp'}, dimensions={0} | all-to-all | bytes 1179648 | tf_op jit(solution)/shard_map/all_to_all | solution.py:392
  142.4 2.2 collective-permute-start.12
  144.6 4.3 %collective-permute-start.13 = (bf16[16,144,128]{2,1,0:T(8,128)(2,1)S(1)}, bf16[16,144,128]{2,1,0:T(8,128)(2,1)S(1)}, u32[]{:S(2)}, u32[]{:S(2)}) collective-permute-start(bf16[16,144,128]{2,1,0:T(8,128)(2,1)S(1)} %all_to_all.21.refs_0_), channel_id=1, source_target_pairs={{0,6},{2,0},{4,2},{6,4},{1,7},{3,1},{5,3},{7,5},{8,14},{10,8},{12,... | collective-permute-start | bytes 1769480 | tf_op jit(solution)/shard_map/ppermute | solution.py:39
  148.9 8.7 %collective-permute-done.12.refs_1_ = bf16[16,144,128]{2,1,0:T(8,128)(2,1)S(1)} collective-permute-done((bf16[16,144,128]{2,1,0:T(8,128)(2,1)S(1)}, bf16[16,144,128]{2,1,0:T(8,128)(2,1)S(1)}, u32[]{:S(2)}, u32[]{:S(2)}) %collective-permute-start.12) | collective-permute-done | bytes 589856 | tf_op jit(solution)/shard_map/ppermute | solution.py:39
  157.6 1.9 collective-permute-start.14
  159.6 4.6 %collective-permute-start.15 = (bf16[8,144,128]{2,1,0:T(8,128)(2,1)S(1)}, bf16[8,144,128]{2,1,0:T(8,128)(2,1)S(1)}, u32[]{:S(2)}, u32[]{:S(2)}) collective-permute-start(bf16[8,144,128]{2,1,0:T(8,128)(2,1)S(1)} %slice.32), channel_id=1, source_target_pairs={{0,6},{2,0},{4,2},{6,4},{1,7},{3,1},{5,3},{7,5},{8,14},{10,8},{12,... | collective-permute-start | bytes 884744 | tf_op jit(solution)/shard_map/ppermute | solution.py:44
  164.3 1.9 collective-permute-start.20
  166.2 4.6 %collective-permute-start.21 = (bf16[256,512]{1,0:T(8,128)(2,1)S(1)}, bf16[256,512]{1,0:T(8,128)(2,1)}, u32[]{:S(2)}, u32[]{:S(2)}) collective-permute-start(bf16[256,512]{1,0:T(8,128)(2,1)S(1)} %pad_maximum_fusion.3), channel_id=1, source_target_pairs={{0,24},{8,0},{16,8},{24,16},{1,25},{9,1},{17,9},{25,17},{2,26},{10... | collective-permute-start | bytes 786440 | tf_op jit(solution)/shard_map/ppermute | solution.py:39
  170.8 4.9 %project.2 = (bf16[2,1,2,2,64,128]{5,4,3,2,1,0:T(8,128)(2,1)}, bf16[2,1,2,2,64,128]{5,4,3,2,1,0:T(8,128)(2,1)}, bf16[2,1,2,2,64,128]{5,4,3,2,1,0:T(8,128)(2,1)}, bf16[2,1,2,2,64,128]{5,4,3,2,1,0:T(8,128)(2,1)}) custom-call(s32[9]{0:T(128)} %stack.46.p_ref, f32[512,1]{1,0:T(8,128)} %factors.1.norm_ref, bf16[2,64,2048]{2,1,0:T(8,128)(2,1)} %refs_0_.3, ...), custom_call_target="tpu_custom_call" | custom-call | tf_op jit(solution)/shard_map/project/pallas_call | solution.py:145
  175.7 2.0 collective-permute-start.8
  179.3 6.8 %collective-permute-start.17 = (bf16[48,144,128]{2,1,0:T(8,128)(2,1)}, bf16[48,144,128]{2,1,0:T(8,128)(2,1)}, u32[]{:S(2)}, u32[]{:S(2)}) collective-permute-start(bf16[48,144,128]{2,1,0:T(8,128)(2,1)} %pad_maximum_fusion), channel_id=1, source_target_pairs={{0,1},{1,0},{2,3},{3,2},{4,5},{5,4},{6,7},{7,6},{8,9},{9,8},{10,11... | collective-permute-start | bytes 5308424 | tf_op jit(solution)/shard_map/ppermute | solution.py:31
  186.3 1.9 collective-permute-start.22
  188.2 3.6 %collective-permute-start.9 = (bf16[2,1,2,2,64,128]{5,4,3,2,1,0:T(8,128)(2,1)S(1)}, bf16[2,1,2,2,64,128]{5,4,3,2,1,0:T(8,128)(2,1)S(1)}, u32[]{:S(2)}, u32[]{:S(2)}) collective-permute-start(bf16[2,1,2,2,64,128]{5,4,3,2,1,0:T(8,128)(2,1)S(1)} %copy-done.22), channel_id=1, source_target_pairs={{0,2},{2,4},{4,6},{6,0},{1,3},{3,5},{5,7},{7,1},{8,10},{10,12},{12... | collective-permute-start | bytes 393224 | tf_op jit(solution)/shard_map/ppermute | solution.py:399
  192.1 1.9 collective-permute-start.10
  194.0 2.4 collective-permute-done.9
  196.4 3.8 %collective-permute-done.10 = bf16[2,1,2,2,64,128]{5,4,3,2,1,0:T(8,128)(2,1)S(1)} collective-permute-done((bf16[2,1,2,2,64,128]{5,4,3,2,1,0:T(8,128)(2,1)S(1)}, bf16[2,1,2,2,64,128]{5,4,3,2,1,0:T(8,128)(2,1)S(1)}, u32[]{:S(2)}, u32[]{:S(2)}) %collective-permute-start.10) | collective-permute-done | bytes 131104 | tf_op jit(solution)/shard_map/ppermute | solution.py:399
  201.0 4.8 %all-to-all-start.2 = ((bf16[16,64,128]{2,1,0:T(8,128)(2,1)}), bf16[16,64,128]{2,1,0:T(8,128)(2,1)S(1)}, u32[]{:S(2)}, u32[]{:S(2)}) async-start(bf16[16,64,128]{2,1,0:T(8,128)(2,1)} %bitcast.13), calls=%async_computation.2 | async-start | bytes 524288 | tf_op jit(solution)/shard_map/all_to_all | solution.py:405
  205.8 3.6 %collective-permute-start.16 = (bf16[16,144,128]{2,1,0:T(8,128)(2,1)S(1)}, bf16[16,144,128]{2,1,0:T(8,128)(2,1)}, u32[]{:S(2)}, u32[]{:S(2)}) collective-permute-start(bf16[16,144,128]{2,1,0:T(8,128)(2,1)S(1)} %all_to_all.21.refs_0_), channel_id=1, source_target_pairs={{0,1},{1,0},{2,3},{3,2},{4,5},{5,4},{6,7},{7,6},{8,9},{9,8},{10,11... | collective-permute-start | bytes 1769480 | tf_op jit(solution)/shard_map/ppermute | solution.py:31
  210.5 1.9 collective-permute-start.23
  212.4 4.8 %collective-permute-start.24 = (bf16[4,256,512]{2,1,0:T(8,128)(2,1)S(1)}, bf16[4,256,512]{2,1,0:T(8,128)(2,1)}, u32[]{:S(2)}, u32[]{:S(2)}) collective-permute-start(bf16[4,256,512]{2,1,0:T(8,128)(2,1)S(1)} %bitcast_dynamic-update-slice_fusion.refs_0_), channel_id=1, source_target_pairs={{0,6},{2,0},{4,2},{6,4},{1,7},{3,1},{5,3},{7,5},{8,14},{10,8},{12,... | collective-permute-start | bytes 3145736 | tf_op jit(solution)/shard_map/ppermute | solution.py:39
  217.2 6.4 %all-to-all-done.2.q_ref = bf16[16,64,128]{2,1,0:T(8,128)(2,1)S(1)} async-done(((bf16[16,64,128]{2,1,0:T(8,128)(2,1)}), bf16[16,64,128]{2,1,0:T(8,128)(2,1)S(1)}, u32[]{:S(2)}, u32[]{:S(2)}) %all-to-all-start.2) | async-done | bytes 262176 | tf_op jit(solution)/shard_map/all_to_all | solution.py:405
  224.3 10.3 %attend.1 = bf16[16,64,128]{2,1,0:T(8,128)(2,1)} custom-call(s32[9]{0:T(128)} %stack.46.p_ref, bf16[16,64,128]{2,1,0:T(8,128)(2,1)} %copy-done.13, bf16[16,144,128]{2,1,0:T(8,128)(2,1)} %copy-done.7, bf16[16,144,128]{2,1,0:T(8,128)(2,1)} %copy-done.5, bf16[16,144,128]{2,1,0:T(8,128)(2,1)} %copy-done.6, bf16[8,144,128]{2,1,0:T(8,128)(2,1)} %copy-done.10, ...), custom_call_target="tpu_custom_call" | custom-call | tf_op jit(solution)/shard_map/attend/pallas_call | solution.py:240
  234.7 6.2 %all-to-all-start.3 = ((bf16[16,64,128]{2,1,0:T(8,128)(2,1)}), bf16[16,64,128]{2,1,0:T(8,128)(2,1)S(1)}, u32[]{:S(2)}, u32[]{:S(2)}) async-start(bf16[16,64,128]{2,1,0:T(8,128)(2,1)} %attend.1), calls=%async_computation.3 | async-start | bytes 524288 | tf_op jit(solution)/shard_map/all_to_all | solution.py:427
  241.0 2.2 collective-permute-start.25
  244.3 4.3 %collective-permute-start.26 = (bf16[2,256,512]{2,1,0:T(8,128)(2,1)S(1)}, bf16[2,256,512]{2,1,0:T(8,128)(2,1)}, u32[]{:S(2)}, u32[]{:S(2)}) collective-permute-start(bf16[2,256,512]{2,1,0:T(8,128)(2,1)S(1)} %slice.27), channel_id=1, source_target_pairs={{0,6},{2,0},{4,2},{6,4},{1,7},{3,1},{5,3},{7,5},{8,14},{10,8},{12,... | collective-permute-start | bytes 1572872 | tf_op jit(solution)/shard_map/ppermute | solution.py:44
  248.6 2.7 collective-permute-start.11
  251.4 3.2 %collective-permute-done.11.edge_ref = bf16[4,2,2,16,128]{4,3,2,1,0:T(8,128)(2,1)S(1)} collective-permute-done((bf16[4,2,2,16,128]{4,3,2,1,0:T(8,128)(2,1)S(1)}, bf16[4,2,2,16,128]{4,3,2,1,0:T(8,128)(2,1)S(1)}, u32[]{:S(2)}, u32[]{:S(2)}) %collective-permute-start.11) | collective-permute-done | bytes 65568 | tf_op jit(solution)/shard_map/ppermute | solution.py:408
  255.2 2.1 pool.1.pool_ref
  257.3 5.6 %collective-permute-start.18 = (bf16[4,2,2,64,128]{4,3,2,1,0:T(8,128)(2,1)}, bf16[4,2,2,64,128]{4,3,2,1,0:T(8,128)(2,1)S(1)}, u32[]{:S(2)}, u32[]{:S(2)}) collective-permute-start(bf16[4,2,2,64,128]{4,3,2,1,0:T(8,128)(2,1)} %pool.1.pool_ref), channel_id=1, source_target_pairs={{0,1},{1,0},{2,3},{3,2},{4,5},{5,4},{6,7},{7,6},{8,9},{9,8},{10,11... | collective-permute-start | bytes 786440 | tf_op jit(solution)/shard_map/ppermute | solution.py:31
  262.9 1.9 collective-permute-start.19
  267.1 5.4 %finish.1 = (f32[2,64,2048]{2,1,0:T(8,128)}, bf16[2,64,2048]{2,1,0:T(8,128)(2,1)}) custom-call(s32[9]{0:T(128)} %stack.46.p_ref, bf16[4,2,2,64,128]{4,3,2,1,0:T(8,128)(2,1)} %pool.1.pool_ref, bf16[4,2,2,64,128]{4,3,2,1,0:T(8,128)(2,1)} %bitcast.28, bf16[4,2,2,64,128]{4,3,2,1,0:T(8,128)(2,1)} %copy-done.15, bf16[4,2,2,64,128]{4,3,2,1,0:T(8,128)(2,1)} %copy-done.16, ...), custom_call_target="tpu_custom_call" | custom-call | tf_op jit(solution)/shard_map/finish/pallas_call | solution.py:325
  272.5 2.0 collective-permute-start.27
  274.6 2.0 collective-permute-done.27
  276.5 2.1 add_convert_fusion
  (92 shorter events, 18.4 us)
Async XLA Ops:
  3.6 16.6 %collective-permute-start.3 = (bf16[528,512]{1,0:T(8,128)(2,1)}, bf16[528,512]{1,0:T(8,128)(2,1)S(1)}, u32[]{:S(2)}, u32[]{:S(2)}) collective-permute-start(bf16[528,512]{1,0:T(8,128)(2,1)} %pad_maximum_fusion.2.refs_4_), channel_id=1, source_target_pairs={{0,8},{8,16},{16,24},{24,0},{1,9},{9,17},{17,25},{25,1},{2,10},{10... | collective-permute-start | bytes 1622024 | tf_op jit(solution)/shard_map/ppermute | solution.py:39
  6.8 15.3 %collective-permute-start.4 = (bf16[528,512]{1,0:T(8,128)(2,1)}, bf16[528,512]{1,0:T(8,128)(2,1)S(1)}, u32[]{:S(2)}, u32[]{:S(2)}) collective-permute-start(bf16[528,512]{1,0:T(8,128)(2,1)} %pad_maximum_fusion.2.refs_4_), channel_id=1, source_target_pairs={{0,24},{8,0},{16,8},{24,16},{1,25},{9,1},{17,9},{25,17},{2,26},{10... | collective-permute-start | bytes 1622024 | tf_op jit(solution)/shard_map/ppermute | solution.py:39
  20.2 56.7 %copy-start.1 = (bf16[528,512]{1,0:T(8,128)(2,1)}, bf16[528,512]{1,0:T(8,128)(2,1)S(1)}, u32[]{:S(2)}) copy-start(bf16[528,512]{1,0:T(8,128)(2,1)S(1)} %collective-permute-done.3.refs_5_) | copy-start | bytes 1622020
  20.2 15.5 %collective-permute-start.5 = (bf16[528,512]{1,0:T(8,128)(2,1)S(1)}, bf16[528,512]{1,0:T(8,128)(2,1)S(1)}, u32[]{:S(2)}, u32[]{:S(2)}) collective-permute-start(bf16[528,512]{1,0:T(8,128)(2,1)S(1)} %collective-permute-done.3.refs_5_), channel_id=1, source_target_pairs={{0,8},{8,16},{16,24},{24,0},{1,9},{9,17},{17,25},{25,1},{2,10},{10... | collective-permute-start | bytes 1622024 | tf_op jit(solution)/shard_map/ppermute | solution.py:54
  22.1 54.8 %copy-start.2 = (bf16[528,512]{1,0:T(8,128)(2,1)}, bf16[528,512]{1,0:T(8,128)(2,1)S(1)}, u32[]{:S(2)}) copy-start(bf16[528,512]{1,0:T(8,128)(2,1)S(1)} %collective-permute-done.4.refs_6_) | copy-start | bytes 1622020
  35.7 41.2 %copy-start.3 = (bf16[528,512]{1,0:T(8,128)(2,1)}, bf16[528,512]{1,0:T(8,128)(2,1)S(1)}, u32[]{:S(2)}) copy-start(bf16[528,512]{1,0:T(8,128)(2,1)S(1)} %collective-permute-done.5.refs_7_) | copy-start | bytes 1622020
  37.0 39.9 %collective-permute-start.7 = (bf16[1584,512]{1,0:T(8,128)(2,1)}, bf16[1584,512]{1,0:T(8,128)(2,1)S(1)}, u32[]{:S(2)}, u32[]{:S(2)}) collective-permute-start(bf16[1584,512]{1,0:T(8,128)(2,1)} %pad_maximum_fusion.1), channel_id=1, source_target_pairs={{0,1},{1,0},{2,3},{3,2},{4,5},{5,4},{6,7},{7,6},{8,9},{9,8},{10,11... | collective-permute-start | bytes 4866056 | tf_op jit(solution)/shard_map/ppermute | solution.py:31
  41.3 16.9 %collective-permute-start = (bf16[2,64,2048]{2,1,0:T(8,128)(2,1)}, bf16[2,64,2048]{2,1,0:T(8,128)(2,1)}, u32[]{:S(2)}, u32[]{:S(2)}) collective-permute-start(bf16[2,64,2048]{2,1,0:T(8,128)(2,1)} %refs_0_.3), channel_id=1, source_target_pairs={{0,2},{2,4},{4,6},{6,0},{1,3},{3,5},{5,7},{7,1},{8,10},{10,12},{12... | collective-permute-start | bytes 1572872 | tf_op jit(solution)/shard_map/ppermute | solution.py:39
  44.4 32.5 %collective-permute-start.6 = (bf16[528,512]{1,0:T(8,128)(2,1)}, bf16[528,512]{1,0:T(8,128)(2,1)}, u32[]{:S(2)}, u32[]{:S(2)}) collective-permute-start(bf16[528,512]{1,0:T(8,128)(2,1)} %pad_maximum_fusion.2.refs_4_), channel_id=1, source_target_pairs={{0,1},{1,0},{2,3},{3,2},{4,5},{5,4},{6,7},{7,6},{8,9},{9,8},{10,11... | collective-permute-start | bytes 1622024 | tf_op jit(solution)/shard_map/ppermute | solution.py:31
  46.6 15.5 %collective-permute-start.1 = (bf16[2,64,2048]{2,1,0:T(8,128)(2,1)}, bf16[2,64,2048]{2,1,0:T(8,128)(2,1)}, u32[]{:S(2)}, u32[]{:S(2)}) collective-permute-start(bf16[2,64,2048]{2,1,0:T(8,128)(2,1)} %refs_0_.3), channel_id=1, source_target_pairs={{0,6},{2,0},{4,2},{6,4},{1,7},{3,1},{5,3},{7,5},{8,14},{10,8},{12,... | collective-permute-start | bytes 1572872 | tf_op jit(solution)/shard_map/ppermute | solution.py:39
  58.2 16.0 %collective-permute-start.2 = (bf16[2,64,2048]{2,1,0:T(8,128)(2,1)}, bf16[2,64,2048]{2,1,0:T(8,128)(2,1)}, u32[]{:S(2)}, u32[]{:S(2)}) collective-permute-start(bf16[2,64,2048]{2,1,0:T(8,128)(2,1)} %collective-permute-done.x1.refs_1_), channel_id=1, source_target_pairs={{0,2},{2,4},{4,6},{6,0},{1,3},{3,5},{5,7},{7,1},{8,10},{10,12},{12... | collective-permute-start | bytes 1572872 | tf_op jit(solution)/shard_map/ppermute | solution.py:54
  83.2 81.0 %copy-start.18 = (bf16[128,512]{1,0:T(8,128)(2,1)S(1)}, bf16[128,512]{1,0:T(8,128)(2,1)}, u32[]{:S(2)}) copy-start(bf16[128,512]{1,0:T(8,128)(2,1)} %param.21) | copy-start | bytes 393220
  83.2 81.0 %copy-start.19 = (bf16[128,512]{1,0:T(8,128)(2,1)S(1)}, bf16[128,512]{1,0:T(8,128)(2,1)}, u32[]{:S(2)}) copy-start(bf16[128,512]{1,0:T(8,128)(2,1)} %param.20) | copy-start | bytes 393220
  142.4 63.4 %copy-start.7 = (bf16[16,144,128]{2,1,0:T(8,128)(2,1)}, bf16[16,144,128]{2,1,0:T(8,128)(2,1)S(1)}, u32[]{:S(2)}) copy-start(bf16[16,144,128]{2,1,0:T(8,128)(2,1)S(1)} %all_to_all.21.refs_0_) | copy-start | bytes 1769476
  142.4 15.2 %collective-permute-start.12 = (bf16[16,144,128]{2,1,0:T(8,128)(2,1)S(1)}, bf16[16,144,128]{2,1,0:T(8,128)(2,1)S(1)}, u32[]{:S(2)}, u32[]{:S(2)}) collective-permute-start(bf16[16,144,128]{2,1,0:T(8,128)(2,1)S(1)} %all_to_all.21.refs_0_), channel_id=1, source_target_pairs={{0,2},{2,4},{4,6},{6,0},{1,3},{3,5},{5,7},{7,1},{8,10},{10,12},{12... | collective-permute-start | bytes 1769480 | tf_op jit(solution)/shard_map/ppermute | solution.py:39
  144.6 14.9 %collective-permute-start.13 = (bf16[16,144,128]{2,1,0:T(8,128)(2,1)S(1)}, bf16[16,144,128]{2,1,0:T(8,128)(2,1)S(1)}, u32[]{:S(2)}, u32[]{:S(2)}) collective-permute-start(bf16[16,144,128]{2,1,0:T(8,128)(2,1)S(1)} %all_to_all.21.refs_0_), channel_id=1, source_target_pairs={{0,6},{2,0},{4,2},{6,4},{1,7},{3,1},{5,3},{7,5},{8,14},{10,8},{12,... | collective-permute-start | bytes 1769480 | tf_op jit(solution)/shard_map/ppermute | solution.py:39
  157.6 20.2 %copy-start.5 = (bf16[16,144,128]{2,1,0:T(8,128)(2,1)}, bf16[16,144,128]{2,1,0:T(8,128)(2,1)S(1)}, u32[]{:S(2)}) copy-start(bf16[16,144,128]{2,1,0:T(8,128)(2,1)S(1)} %collective-permute-done.12.refs_1_) | copy-start | bytes 1769476
  157.6 20.1 %collective-permute-start.14 = (bf16[8,144,128]{2,1,0:T(8,128)(2,1)S(1)}, bf16[8,144,128]{2,1,0:T(8,128)(2,1)S(1)}, u32[]{:S(2)}, u32[]{:S(2)}) collective-permute-start(bf16[8,144,128]{2,1,0:T(8,128)(2,1)S(1)} %slice.31), channel_id=1, source_target_pairs={{0,2},{2,4},{4,6},{6,0},{1,3},{3,5},{5,7},{7,1},{8,10},{10,12},{12... | collective-permute-start | bytes 884744 | tf_op jit(solution)/shard_map/ppermute | solution.py:44
  159.6 18.3 %copy-start.6 = (bf16[16,144,128]{2,1,0:T(8,128)(2,1)}, bf16[16,144,128]{2,1,0:T(8,128)(2,1)S(1)}, u32[]{:S(2)}) copy-start(bf16[16,144,128]{2,1,0:T(8,128)(2,1)S(1)} %collective-permute-done.13.refs_2_) | copy-start | bytes 1769476
  159.6 18.2 %collective-permute-start.15 = (bf16[8,144,128]{2,1,0:T(8,128)(2,1)S(1)}, bf16[8,144,128]{2,1,0:T(8,128)(2,1)S(1)}, u32[]{:S(2)}, u32[]{:S(2)}) collective-permute-start(bf16[8,144,128]{2,1,0:T(8,128)(2,1)S(1)} %slice.32), channel_id=1, source_target_pairs={{0,6},{2,0},{4,2},{6,4},{1,7},{3,1},{5,3},{7,5},{8,14},{10,8},{12,... | collective-permute-start | bytes 884744 | tf_op jit(solution)/shard_map/ppermute | solution.py:44
  164.3 22.0 %collective-permute-start.20 = (bf16[256,512]{1,0:T(8,128)(2,1)S(1)}, bf16[256,512]{1,0:T(8,128)(2,1)S(1)}, u32[]{:S(2)}, u32[]{:S(2)}) collective-permute-start(bf16[256,512]{1,0:T(8,128)(2,1)S(1)} %pad_maximum_fusion.3), channel_id=1, source_target_pairs={{0,8},{8,16},{16,24},{24,0},{1,9},{9,17},{17,25},{25,1},{2,10},{10... | collective-permute-start | bytes 786440 | tf_op jit(solution)/shard_map/ppermute | solution.py:39
  166.2 43.2 %collective-permute-start.21 = (bf16[256,512]{1,0:T(8,128)(2,1)S(1)}, bf16[256,512]{1,0:T(8,128)(2,1)}, u32[]{:S(2)}, u32[]{:S(2)}) collective-permute-start(bf16[256,512]{1,0:T(8,128)(2,1)S(1)} %pad_maximum_fusion.3), channel_id=1, source_target_pairs={{0,24},{8,0},{16,8},{24,16},{1,25},{9,1},{17,9},{25,17},{2,26},{10... | collective-permute-start | bytes 786440 | tf_op jit(solution)/shard_map/ppermute | solution.py:39
  175.7 12.5 %copy-start.22 = (bf16[2,1,2,2,64,128]{5,4,3,2,1,0:T(8,128)(2,1)S(1)}, bf16[2,1,2,2,64,128]{5,4,3,2,1,0:T(8,128)(2,1)}, u32[]{:S(2)}) copy-start(bf16[2,1,2,2,64,128]{5,4,3,2,1,0:T(8,128)(2,1)} %get-tuple-element.18) | copy-start | bytes 393220
  175.7 16.3 %collective-permute-start.8 = (bf16[2,1,2,2,64,128]{5,4,3,2,1,0:T(8,128)(2,1)}, bf16[2,1,2,2,64,128]{5,4,3,2,1,0:T(8,128)(2,1)S(1)}, u32[]{:S(2)}, u32[]{:S(2)}) collective-permute-start(bf16[2,1,2,2,64,128]{5,4,3,2,1,0:T(8,128)(2,1)} %get-tuple-element.17), channel_id=1, source_target_pairs={{0,6},{2,0},{4,2},{6,4},{1,7},{3,1},{5,3},{7,5},{8,14},{10,8},{12,... | collective-permute-start | bytes 393224 | tf_op jit(solution)/shard_map/ppermute | solution.py:399
  177.8 1.5 copy-start.10
  177.8 1.5 copy-start.11
  179.3 12.7 %copy-start.17 = (bf16[2,1,2,2,64,128]{5,4,3,2,1,0:T(8,128)(2,1)S(1)}, bf16[2,1,2,2,64,128]{5,4,3,2,1,0:T(8,128)(2,1)}, u32[]{:S(2)}) copy-start(bf16[2,1,2,2,64,128]{5,4,3,2,1,0:T(8,128)(2,1)} %get-tuple-element.16) | copy-start | bytes 393220
  179.3 12.7 %copy-start.21 = (bf16[2,1,2,2,64,128]{5,4,3,2,1,0:T(8,128)(2,1)S(1)}, bf16[2,1,2,2,64,128]{5,4,3,2,1,0:T(8,128)(2,1)}, u32[]{:S(2)}) copy-start(bf16[2,1,2,2,64,128]{5,4,3,2,1,0:T(8,128)(2,1)} %get-tuple-element.19) | copy-start | bytes 393220
  179.3 44.3 %collective-permute-start.17 = (bf16[48,144,128]{2,1,0:T(8,128)(2,1)}, bf16[48,144,128]{2,1,0:T(8,128)(2,1)}, u32[]{:S(2)}, u32[]{:S(2)}) collective-permute-start(bf16[48,144,128]{2,1,0:T(8,128)(2,1)} %pad_maximum_fusion), channel_id=1, source_target_pairs={{0,1},{1,0},{2,3},{3,2},{4,5},{5,4},{6,7},{7,6},{8,9},{9,8},{10,11... | collective-permute-start | bytes 5308424 | tf_op jit(solution)/shard_map/ppermute | solution.py:31
  186.3 24.1 %collective-permute-start.22 = (bf16[256,512]{1,0:T(8,128)(2,1)S(1)}, bf16[256,512]{1,0:T(8,128)(2,1)S(1)}, u32[]{:S(2)}, u32[]{:S(2)}) collective-permute-start(bf16[256,512]{1,0:T(8,128)(2,1)S(1)} %collective-permute-done.20), channel_id=1, source_target_pairs={{0,8},{8,16},{16,24},{24,0},{1,9},{9,17},{17,25},{25,1},{2,10},{10... | collective-permute-start | bytes 786440 | tf_op jit(solution)/shard_map/ppermute | solution.py:54
  188.2 8.1 %collective-permute-start.9 = (bf16[2,1,2,2,64,128]{5,4,3,2,1,0:T(8,128)(2,1)S(1)}, bf16[2,1,2,2,64,128]{5,4,3,2,1,0:T(8,128)(2,1)S(1)}, u32[]{:S(2)}, u32[]{:S(2)}) collective-permute-start(bf16[2,1,2,2,64,128]{5,4,3,2,1,0:T(8,128)(2,1)S(1)} %copy-done.22), channel_id=1, source_target_pairs={{0,2},{2,4},{4,6},{6,0},{1,3},{3,5},{5,7},{7,1},{8,10},{10,12},{12... | collective-permute-start | bytes 393224 | tf_op jit(solution)/shard_map/ppermute | solution.py:399
  192.1 8.2 %collective-permute-start.10 = (bf16[2,1,2,2,64,128]{5,4,3,2,1,0:T(8,128)(2,1)S(1)}, bf16[2,1,2,2,64,128]{5,4,3,2,1,0:T(8,128)(2,1)S(1)}, u32[]{:S(2)}, u32[]{:S(2)}) collective-permute-start(bf16[2,1,2,2,64,128]{5,4,3,2,1,0:T(8,128)(2,1)S(1)} %copy-done.21), channel_id=1, source_target_pairs={{0,4},{2,6},{4,0},{6,2},{1,5},{3,7},{5,1},{7,3},{8,12},{10,14},{12... | collective-permute-start | bytes 393224 | tf_op jit(solution)/shard_map/ppermute | solution.py:399
  201.0 47.6 %copy-start.9 = (bf16[4,2,2,64,128]{4,3,2,1,0:T(8,128)(2,1)}, bf16[4,2,2,64,128]{4,3,2,1,0:T(8,128)(2,1)S(1)}, u32[]{:S(2)}) copy-start(bf16[4,2,2,64,128]{4,3,2,1,0:T(8,128)(2,1)S(1)} %get-tuple-element.28.in_ref) | copy-start | bytes 786436
  201.0 22.6 %all-to-all-start.2 = ((bf16[16,64,128]{2,1,0:T(8,128)(2,1)}), bf16[16,64,128]{2,1,0:T(8,128)(2,1)S(1)}, u32[]{:S(2)}, u32[]{:S(2)}) async-start(bf16[16,64,128]{2,1,0:T(8,128)(2,1)} %bitcast.13), calls=%async_computation.2 | async-start | bytes 524288 | tf_op jit(solution)/shard_map/all_to_all | solution.py:405
  205.8 11.4 %collective-permute-start.16 = (bf16[16,144,128]{2,1,0:T(8,128)(2,1)S(1)}, bf16[16,144,128]{2,1,0:T(8,128)(2,1)}, u32[]{:S(2)}, u32[]{:S(2)}) collective-permute-start(bf16[16,144,128]{2,1,0:T(8,128)(2,1)S(1)} %all_to_all.21.refs_0_), channel_id=1, source_target_pairs={{0,1},{1,0},{2,3},{3,2},{4,5},{5,4},{6,7},{7,6},{8,9},{9,8},{10,11... | collective-permute-start | bytes 1769480 | tf_op jit(solution)/shard_map/ppermute | solution.py:31
  210.5 24.2 %copy-start.4 = (bf16[4,256,512]{2,1,0:T(8,128)(2,1)}, bf16[4,256,512]{2,1,0:T(8,128)(2,1)S(1)}, u32[]{:S(2)}) copy-start(bf16[4,256,512]{2,1,0:T(8,128)(2,1)S(1)} %bitcast_dynamic-update-slice_fusion.refs_0_) | copy-start | bytes 3145732
  210.5 30.4 %collective-permute-start.23 = (bf16[4,256,512]{2,1,0:T(8,128)(2,1)S(1)}, bf16[4,256,512]{2,1,0:T(8,128)(2,1)S(1)}, u32[]{:S(2)}, u32[]{:S(2)}) collective-permute-start(bf16[4,256,512]{2,1,0:T(8,128)(2,1)S(1)} %bitcast_dynamic-update-slice_fusion.refs_0_), channel_id=1, source_target_pairs={{0,2},{2,4},{4,6},{6,0},{1,3},{3,5},{5,7},{7,1},{8,10},{10,12},{12... | collective-permute-start | bytes 3145736 | tf_op jit(solution)/shard_map/ppermute | solution.py:39
  212.4 28.5 %collective-permute-start.24 = (bf16[4,256,512]{2,1,0:T(8,128)(2,1)S(1)}, bf16[4,256,512]{2,1,0:T(8,128)(2,1)}, u32[]{:S(2)}, u32[]{:S(2)}) collective-permute-start(bf16[4,256,512]{2,1,0:T(8,128)(2,1)S(1)} %bitcast_dynamic-update-slice_fusion.refs_0_), channel_id=1, source_target_pairs={{0,6},{2,0},{4,2},{6,4},{1,7},{3,1},{5,3},{7,5},{8,14},{10,8},{12,... | collective-permute-start | bytes 3145736 | tf_op jit(solution)/shard_map/ppermute | solution.py:39
  234.7 28.2 %all-to-all-start.3 = ((bf16[16,64,128]{2,1,0:T(8,128)(2,1)}), bf16[16,64,128]{2,1,0:T(8,128)(2,1)S(1)}, u32[]{:S(2)}, u32[]{:S(2)}) async-start(bf16[16,64,128]{2,1,0:T(8,128)(2,1)} %attend.1), calls=%async_computation.3 | async-start | bytes 524288 | tf_op jit(solution)/shard_map/all_to_all | solution.py:427
  240.9 25.4 %copy-start.8 = (bf16[4,256,512]{2,1,0:T(8,128)(2,1)}, bf16[4,256,512]{2,1,0:T(8,128)(2,1)S(1)}, u32[]{:S(2)}) copy-start(bf16[4,256,512]{2,1,0:T(8,128)(2,1)S(1)} %collective-permute-done.23.refs_1_) | copy-start | bytes 3145732
  241.0 23.9 %collective-permute-start.25 = (bf16[2,256,512]{2,1,0:T(8,128)(2,1)S(1)}, bf16[2,256,512]{2,1,0:T(8,128)(2,1)S(1)}, u32[]{:S(2)}, u32[]{:S(2)}) collective-permute-start(bf16[2,256,512]{2,1,0:T(8,128)(2,1)S(1)} %slice.26), channel_id=1, source_target_pairs={{0,2},{2,4},{4,6},{6,0},{1,3},{3,5},{5,7},{7,1},{8,10},{10,12},{12... | collective-permute-start | bytes 1572872 | tf_op jit(solution)/shard_map/ppermute | solution.py:44
  244.3 20.6 %collective-permute-start.26 = (bf16[2,256,512]{2,1,0:T(8,128)(2,1)S(1)}, bf16[2,256,512]{2,1,0:T(8,128)(2,1)}, u32[]{:S(2)}, u32[]{:S(2)}) collective-permute-start(bf16[2,256,512]{2,1,0:T(8,128)(2,1)S(1)} %slice.27), channel_id=1, source_target_pairs={{0,6},{2,0},{4,2},{6,4},{1,7},{3,1},{5,3},{7,5},{8,14},{10,8},{12,... | collective-permute-start | bytes 1572872 | tf_op jit(solution)/shard_map/ppermute | solution.py:44
  248.6 5.9 %collective-permute-start.11 = (bf16[4,2,2,16,128]{4,3,2,1,0:T(8,128)(2,1)S(1)}, bf16[4,2,2,16,128]{4,3,2,1,0:T(8,128)(2,1)S(1)}, u32[]{:S(2)}, u32[]{:S(2)}) collective-permute-start(bf16[4,2,2,16,128]{4,3,2,1,0:T(8,128)(2,1)S(1)} %slice.29), channel_id=1, source_target_pairs={{0,1},{1,2},{2,3},{3,4},{4,5},{5,6},{6,7},{7,32},{32,33},{33,34},{... | collective-permute-start | bytes 196616 | tf_op jit(solution)/shard_map/ppermute | solution.py:408
  257.3 7.6 %collective-permute-start.18 = (bf16[4,2,2,64,128]{4,3,2,1,0:T(8,128)(2,1)}, bf16[4,2,2,64,128]{4,3,2,1,0:T(8,128)(2,1)S(1)}, u32[]{:S(2)}, u32[]{:S(2)}) collective-permute-start(bf16[4,2,2,64,128]{4,3,2,1,0:T(8,128)(2,1)} %pool.1.pool_ref), channel_id=1, source_target_pairs={{0,1},{1,0},{2,3},{3,2},{4,5},{5,4},{6,7},{7,6},{8,9},{9,8},{10,11... | collective-permute-start | bytes 786440 | tf_op jit(solution)/shard_map/ppermute | solution.py:31
  262.9 3.4 %copy-start.12 = (bf16[16,64,128]{2,1,0:T(8,128)(2,1)}, bf16[16,64,128]{2,1,0:T(8,128)(2,1)S(1)}, u32[]{:S(2)}) copy-start(bf16[16,64,128]{2,1,0:T(8,128)(2,1)S(1)} %all-to-all-done.3) | copy-start | bytes 786436
  262.9 3.4 %collective-permute-start.19 = (bf16[4,2,2,64,128]{4,3,2,1,0:T(8,128)(2,1)S(1)}, bf16[4,2,2,64,128]{4,3,2,1,0:T(8,128)(2,1)S(1)}, u32[]{:S(2)}, u32[]{:S(2)}) collective-permute-start(bf16[4,2,2,64,128]{4,3,2,1,0:T(8,128)(2,1)S(1)} %bitcast.27), channel_id=1, source_target_pairs={{0,1},{1,0},{2,3},{3,2},{4,5},{5,4},{6,7},{7,6},{8,9},{9,8},{10,11... | collective-permute-start | bytes 786440 | tf_op jit(solution)/shard_map/ppermute | solution.py:31
  264.9 1.5 copy-start.15
  272.5 4.0 %collective-permute-start.27 = (bf16[2,64,2048]{2,1,0:T(8,128)(2,1)}, bf16[2,64,2048]{2,1,0:T(8,128)(2,1)S(1)}, u32[]{:S(2)}, u32[]{:S(2)}) collective-permute-start(bf16[2,64,2048]{2,1,0:T(8,128)(2,1)} %get-tuple-element.26), channel_id=1, source_target_pairs={{0,1},{1,0},{2,3},{3,2},{4,5},{5,4},{6,7},{7,6},{8,9},{9,8},{10,11... | collective-permute-start | bytes 1572872 | tf_op jit(solution)/shard_map/ppermute | solution.py:31
  (5 other events, 4.7 us)

commit v5 on v4

--- a/solution.py
+++ b/solution.py
@@ -54,40 +54,14 @@
     return (x, *near, lax.ppermute(near[0], axis, UP))
 
 
-def rms(x):
-    wide = x.astype(F32)
-    return lax.rsqrt(jnp.mean(wide * wide, axis=-1, keepdims=True) + EPS)
-
-
-def factors_of(rows_of):
-    seqs, rows, _ = rows_of[0].shape
-
-    def body(x0, x1, x2, x3, out_ref):
-        at = 0
-        for ref in (x0, x1, x2, x3):
-            for i in range(ref.shape[0]):
-                out_ref[at : at + rows] = rms(ref[i])
-                at += rows
-
-    return pl.pallas_call(
-        body,
-        in_specs=[whole()] * 4,
-        out_specs=whole(),
-        out_shape=jax.ShapeDtypeStruct((4 * seqs * rows, 1), F32),
-        compiler_params=params(),
-        name="factors",
-    )(*rows_of)
-
-
-def project(places, norm, rows_of, own, other, half, factors, split):
-    seqs, rows, _ = rows_of[0].shape
+def project(places, rows_of, own, other, half, factors, split):
+    seqs, rows, depth = rows_of[0].shape
     kinds = len(factors)
 
-    def body(p_ref, norm_ref, *refs):
-        xs, own_refs, other_refs, outs = refs[:4], refs[4:8], refs[8:10], refs[10:]
+    def body(p_ref, *refs):
+        xs, own_refs, other_refs, outs = refs[:4], refs[4:9], refs[9:11], refs[11:]
         deep = own_refs[0].shape[0] - GATE_ROWS
         tall = deep + GATE_ROWS
-        r = norm_ref[...]
         lane = lax.broadcasted_iota(jnp.int32, (GATE_ROWS, HD), 1)
         first_half = (lane < rows) == (p_ref[0] == 0)
         slabs = []
@@ -98,7 +72,14 @@
                     [ref[i, :, at] for ref in xs for i in range(ref.shape[0])], axis=0
                 )
             )
-        own = [ref[:deep, cols] for ref in own_refs]
+        squares = jnp.zeros((4 * seqs * rows, 1), F32)
+        for slab in slabs:
+            wide = slab.astype(F32)
+            squares = squares + jnp.sum(wide * wide, axis=-1, keepdims=True)
+        r = lax.rsqrt(squares * (1.0 / depth) + EPS)
+        own = [ref[:deep, cols] for ref in own_refs[:3]]
+        far = jnp.concatenate([ref[:, cols] for ref in own_refs[3:]], axis=0)
+        own.append(far[:deep])
         other = [other_refs[0][:deep, cols]]
         other += [other_refs[1][n * tall : n * tall + deep, cols] for n in range(3)]
         for ref, ws, head in (
@@ -149,7 +130,7 @@
         out_shape=[jax.ShapeDtypeStruct(sh, BF16) for sh in shapes],
         compiler_params=params(),
         name="project",
-    )(places, norm, *rows_of, *own, *other)
+    )(places, *rows_of, *own, *other)
     return outs
 
 
@@ -288,31 +269,27 @@
     )(first, rows_in, border, mix, scale)
 
 
-def finish(places, pooled, attn, pooled_pair, attn_pair, w):
+def finish(places, pooled, attn, own, other):
     nx, seqs, _, rows, _ = pooled.shape
-    ny, deep, wide = w[0].shape
-    own = seqs * rows
-
-    def body(p_ref, pool_ref, attn_ref, pool_pair_ref, attn_pair_ref, *refs):
-        out_ref, pair_ref = refs[5:]
+    ny, deep, wide = own[0].shape
+
+    def body(p_ref, pool_ref, attn_ref, *refs):
+        out_ref = refs[10]
         late = pl.program_id(0) >= ny // 2
-        c = p_ref[0]
-        total = jnp.zeros((2 * own, wide), F32)
-        for a in range(nx):
-            x = p_ref[1 + a]
-            left = jnp.concatenate(
-                [
-                    jnp.concatenate(
-                        [ref[x, i, c] for ref in two for i in range(seqs)], axis=0
-                    )
-                    for two in ((pool_ref, pool_pair_ref), (attn_ref, attn_pair_ref))
-                ],
-                axis=1,
-            )
-            right = refs[a][0] if a < 3 else jnp.where(late, refs[4][0], refs[3][0])
-            total = total + jnp.dot(left, right, preferred_element_type=F32)
-        out_ref[...] = total[:own].reshape(seqs, rows, wide)
-        pair_ref[...] = total[own:].astype(BF16).reshape(seqs, rows, wide)
+        total = jnp.zeros((seqs * rows, wide), F32)
+        for side, c in ((refs[:5], p_ref[0]), (refs[5:10], 1 - p_ref[0])):
+            for a in range(nx):
+                x = p_ref[1 + a]
+                left = jnp.concatenate(
+                    [
+                        jnp.concatenate([pool_ref[x, i, c] for i in range(seqs)], axis=0),
+                        jnp.concatenate([attn_ref[x, i, c] for i in range(seqs)], axis=0),
+                    ],
+                    axis=1,
+                )
+                right = side[a][0] if a < 3 else jnp.where(late, side[4][0], side[3][0])
+                total = total + jnp.dot(left, right, preferred_element_type=F32)
+        out_ref[...] = total.astype(BF16).reshape(seqs, rows, wide)
 
     half = ny // 2
     shape = (1, deep, wide)
@@ -320,17 +297,15 @@
         pl.BlockSpec(shape, lambda j: (jnp.minimum(j, half - 1), 0, 0)),
         pl.BlockSpec(shape, lambda j: (jnp.maximum(j - half, 0), 0, 0)),
     ]
-    out_spec = pl.BlockSpec((seqs, rows, wide), lambda j: (0, 0, j))
-    out = (seqs, rows, ny * wide)
     return pl.pallas_call(
         body,
         grid=(ny,),
-        in_specs=[whole(pltpu.SMEM)] + [whole()] * 4 + specs,
-        out_specs=[out_spec, out_spec],
-        out_shape=[jax.ShapeDtypeStruct(out, F32), jax.ShapeDtypeStruct(out, BF16)],
+        in_specs=[whole(pltpu.SMEM), whole(), whole()] + specs + specs,
+        out_specs=pl.BlockSpec((seqs, rows, wide), lambda j: (0, 0, j)),
+        out_shape=jax.ShapeDtypeStruct((seqs, rows, ny * wide), BF16),
         compiler_params=params(),
         name="finish",
-    )(places, pooled, attn, pooled_pair, attn_pair, *w)
+    )(places, pooled, attn, *own, *other)
 
 
 def after(x, *others):
@@ -374,7 +349,6 @@
     deep = w_key.shape[0]
     gain = lax.dynamic_slice_in_dim(norm_gain, y * deep, deep, 0)
     all_rows = ring_in_three(tokens, "tp_0")
-    norm = factors_of(all_rows)
     weights = jnp.concatenate([w_key, w_value, w_query, w_pool_in], axis=1)
     weights = (weights.astype(F32) * gain[:, None]).astype(BF16)
     here = lax.dynamic_slice_in_dim(gate_cache[:, 0], z * block, block, 1)
@@ -383,15 +357,15 @@
     middle = lax.reduce_precision(rest, 8, 7)
     parts = jnp.stack([high, middle, rest - middle], axis=1).astype(BF16)
     parts = jnp.pad(parts, ((0, 0), (0, 5), (0, 0))).reshape(GATE_ROWS, block)
-    own_w = ring_in_three(jnp.concatenate([weights, parts], axis=0), "fs")
+    own_w = ring_of_four(jnp.concatenate([weights, parts], axis=0), "fs")
     other_w = sibling(own_w[0])
     other_w = (other_w, sibling(jnp.concatenate(own_w[1:], axis=0)))
 
-    (kv,) = project(places, norm, all_rows, own_w, other_w, 0, (1.0, 1.0), False)
+    (kv,) = project(places, all_rows, own_w, other_w, 0, (1.0, 1.0), False)
     kv_here = lax.all_to_all(kv, "tp_0", 0, 0, tiled=True)
     kv = lax.all_to_all(kv_here.reshape(planes, 2 * rows + GATE_ROWS, HD), "sp", 0, 0, tiled=True)
     qp = project(
-        places, norm, all_rows, own_w, other_w, 1, (HD**-0.5 * LOG2E, 1.0), True
+        places, all_rows, own_w, other_w, 1, (HD**-0.5 * LOG2E, 1.0), True
     )
     got = [qp[0]]
     for piece, by in zip(qp[1:], (-1, 1, 2)):
@@ -410,7 +384,6 @@
     )
     first = (z * block + (2 * x + c) * rows).reshape(1).astype(jnp.int32)
     pooled = pool(first, pool_in, border, pool_mix, pool_scale.reshape(-1, HD))
-    pooled_pair = sibling(pooled)
 
     kv_own = ring_of_four(kv, "tp_0")
     kv_other = sibling(kv)
@@ -424,12 +397,12 @@
     attn = attend(places, q, kv_own, kv_other)
     out_near = lax.optimization_barrier((*out_near, attn))[:2]
     out_own = (o, *out_near, *relays(*out_near, "tp_0"))
+    out_other = [sibling(piece) for piece in out_own[1:3]]
+    out_other += [sibling(piece) for piece in out_own[3:]]
+    out_other = [sibling(o)] + out_other
     attn = lax.all_to_all(attn, "sp", 0, 0, tiled=True)
     attn = attn.reshape(chunks, seqs, 2, rows, HD)
-    mine, theirs = finish(
-        places, pooled, attn, pooled_pair, sibling(attn), out_own
-    )
-    return (mine + sibling(theirs).astype(F32)).astype(BF16)
+    return finish(places, pooled, attn, out_own, out_other)
 
 
 def solution(mesh):

time: 280 us -> 274 us (0.979)
  the two profiles are of different devices: /device:TPU:33 before, /device:TPU:16 now
where the time goes in v5:
time: 274 us; the launch traced here: 273 us
  starting transfers between devices  98.9 us (36%)
  waiting for transfers between devices  71.8 us (26%)
  blocking collectives  60.9 us (22%)
  Pallas kernels  28.4 us (10%)
  local copies, waits for them, and re-layouts  7.01 us (3%)
  other arithmetic  4.81 us (2%)
    all_to_all x1, blocking collectives, on_device(): lax.all_to_all(kv_here.reshape(planes, 2 * rows + GATE_ROWS, HD), 'sp', 0...  47.9 us
    ppermute x10, starting transfers between devices, hops(): return (lax.ppermute(x, axis, UP), lax.ppermute(x, axis, DOWN))  33.6 us
    ppermute x10, waiting for transfers between devices, hops(): return (lax.ppermute(x, axis, UP), lax.ppermute(x, axis, DOWN))  22.9 us
    ppermute x9, starting transfers between devices, sibling(): return lax.ppermute(x, 'tp_1', [(0, 1), (1, 0)])  18.6 us
    all_to_all x1, blocking collectives, on_device(): kv_here = lax.all_to_all(kv, 'tp_0', 0, 0, tiled=True)  13 us
    ppermute x3, starting transfers between devices, relays(): lax.ppermute(after[half:], axis, DOWN)  12.9 us
    ppermute x2, waiting for transfers between devices, ring_in_three(): return (x, *near, lax.ppermute(near[0], axis, UP))  12.7 us
    all_to_all x1, waiting for transfers between devices, on_device(): q = lax.all_to_all(q, 'sp', 0, 0, tiled=True)  11.5 us
  transfers between devices with their start and end apart: 33, of which 12 were waited for; matrix products, arithmetic and copies ran while one was open for 2% of the time, Pallas kernels for 6%

profile of v5, /device:TPU:16, one launch (start us, length us, event | category | flops | bytes accessed | tf_op | source)
XLA Modules:
  0.0 272.9 jit_solution(4100187873511138878)
XLA Ops:
  2.8 3.2 %collective-permute-start.3 = (bf16[528,512]{1,0:T(8,128)(2,1)S(1)}, bf16[528,512]{1,0:T(8,128)(2,1)S(1)}, u32[]{:S(2)}, u32[]{:S(2)}) collective-permute-start(bf16[528,512]{1,0:T(8,128)(2,1)S(1)} %pad_maximum_fusion.2.refs_4_), channel_id=1, source_target_pairs={{0,8},{8,16},{16,24},{24,0},{1,9},{9,17},{17,25},{25,1},{2,10},{10... | collective-permute-start | bytes 1622024 | tf_op jit(solution)/shard_map/ppermute | solution.py:39
  6.0 2.7 collective-permute-start.4
  8.7 10.1 %collective-permute-done.3.refs_5_ = bf16[528,512]{1,0:T(8,128)(2,1)S(1)} collective-permute-done((bf16[528,512]{1,0:T(8,128)(2,1)S(1)}, bf16[528,512]{1,0:T(8,128)(2,1)S(1)}, u32[]{:S(2)}, u32[]{:S(2)}) %collective-permute-start.3) | collective-permute-done | bytes 540704 | tf_op jit(solution)/shard_map/ppermute | solution.py:39
  18.8 3.2 %collective-permute-start.5 = (bf16[264,512]{1,0:T(8,128)(2,1)S(1)}, bf16[264,512]{1,0:T(8,128)(2,1)S(1)}, u32[]{:S(2)}, u32[]{:S(2)}) collective-permute-start(bf16[264,512]{1,0:T(8,128)(2,1)S(1)} %slice.36), channel_id=1, source_target_pairs={{0,8},{8,16},{16,24},{24,0},{1,9},{9,17},{17,25},{25,1},{2,10},{10... | collective-permute-start | bytes 811016 | tf_op jit(solution)/shard_map/ppermute | solution.py:44
  22.0 2.7 collective-permute-start.6
  24.7 3.4 %collective-permute-done.5.refs_7_ = bf16[264,512]{1,0:T(8,128)(2,1)S(1)} collective-permute-done((bf16[264,512]{1,0:T(8,128)(2,1)S(1)}, bf16[264,512]{1,0:T(8,128)(2,1)S(1)}, u32[]{:S(2)}, u32[]{:S(2)}) %collective-permute-start.5) | collective-permute-done | bytes 270368 | tf_op jit(solution)/shard_map/ppermute | solution.py:44
  28.0 3.0 %collective-permute-done.6.refs_8_ = bf16[264,512]{1,0:T(8,128)(2,1)S(1)} collective-permute-done((bf16[264,512]{1,0:T(8,128)(2,1)S(1)}, bf16[264,512]{1,0:T(8,128)(2,1)S(1)}, u32[]{:S(2)}, u32[]{:S(2)}) %collective-permute-start.6) | collective-permute-done | bytes 270368 | tf_op jit(solution)/shard_map/ppermute | solution.py:44
  34.9 3.4 %collective-permute-start = (bf16[2,64,2048]{2,1,0:T(8,128)(2,1)}, bf16[2,64,2048]{2,1,0:T(8,128)(2,1)}, u32[]{:S(2)}, u32[]{:S(2)}) collective-permute-start(bf16[2,64,2048]{2,1,0:T(8,128)(2,1)} %refs_0_.3), channel_id=1, source_target_pairs={{0,2},{2,4},{4,6},{6,0},{1,3},{3,5},{5,7},{7,1},{8,10},{10,12},{12... | collective-permute-start | bytes 1572872 | tf_op jit(solution)/shard_map/ppermute | solution.py:39
  38.4 2.1 collective-permute-start.7
  40.5 3.7 %collective-permute-start.1 = (bf16[2,64,2048]{2,1,0:T(8,128)(2,1)}, bf16[2,64,2048]{2,1,0:T(8,128)(2,1)}, u32[]{:S(2)}, u32[]{:S(2)}) collective-permute-start(bf16[2,64,2048]{2,1,0:T(8,128)(2,1)} %refs_0_.3), channel_id=1, source_target_pairs={{0,6},{2,0},{4,2},{6,4},{1,7},{3,1},{5,3},{7,5},{8,14},{10,8},{12,... | collective-permute-start | bytes 1572872 | tf_op jit(solution)/shard_map/ppermute | solution.py:39
  44.2 8.5 %collective-permute-done.refs_1_ = bf16[2,64,2048]{2,1,0:T(8,128)(2,1)} collective-permute-done((bf16[2,64,2048]{2,1,0:T(8,128)(2,1)}, bf16[2,64,2048]{2,1,0:T(8,128)(2,1)}, u32[]{:S(2)}, u32[]{:S(2)}) %collective-permute-start) | collective-permute-done | bytes 524320 | tf_op jit(solution)/shard_map/ppermute | solution.py:39
  52.7 2.2 collective-permute-start.2
  56.8 12.7 %collective-permute-done.2.refs_3_ = bf16[2,64,2048]{2,1,0:T(8,128)(2,1)} collective-permute-done((bf16[2,64,2048]{2,1,0:T(8,128)(2,1)}, bf16[2,64,2048]{2,1,0:T(8,128)(2,1)}, u32[]{:S(2)}, u32[]{:S(2)}) %collective-permute-start.2) | collective-permute-done | bytes 524320 | tf_op jit(solution)/shard_map/ppermute | solution.py:54
  70.8 5.0 %project.3 = bf16[4,2,2,144,128]{4,3,2,1,0:T(8,128)(2,1)} custom-call(s32[9]{0:T(128)} %stack.46.p_ref, bf16[2,64,2048]{2,1,0:T(8,128)(2,1)} %refs_0_.3, bf16[2,64,2048]{2,1,0:T(8,128)(2,1)} %collective-permute-done.refs_1_, bf16[2,64,2048]{2,1,0:T(8,128)(2,1)} %collective-permute-done.1.refs_2_, bf16[2,64,2048]{2,1,0:T(8,128)(2,1)} %collective-permute-done.2.refs_3_, ...), custom_call_target="tpu_custom_call" | custom-call | tf_op jit(solution)/shard_map/project/pallas_call | solution.py:126
  75.8 13.0 %all_to_all.20 = bf16[4,2,2,144,128]{4,3,2,1,0:T(8,128)(2,1)S(1)} all-to-all(bf16[4,2,2,144,128]{4,3,2,1,0:T(8,128)(2,1)} %project.3), channel_id=1, replica_groups=mesh['sp'=16,'fs'=4,'tp_0'=4,'tp_1'=2] {'tp_0'}, dimensions={0} | all-to-all | bytes 1179648 | tf_op jit(solution)/shard_map/all_to_all | solution.py:365
  88.8 47.9 %all_to_all.21.refs_0_ = bf16[16,144,128]{2,1,0:T(8,128)(2,1)S(1)} all-to-all(bf16[16,144,128]{2,1,0:T(8,128)(2,1)S(1)} %bitcast.26), channel_id=1, replica_groups=mesh['sp'=16,'fs'=4,'tp_0'=4,'tp_1'=2] {'sp'}, dimensions={0} | all-to-all | bytes 1179648 | tf_op jit(solution)/shard_map/all_to_all | solution.py:366
  136.7 2.5 collective-permute-start.13
  139.2 4.6 %collective-permute-start.14 = (bf16[16,144,128]{2,1,0:T(8,128)(2,1)S(1)}, bf16[16,144,128]{2,1,0:T(8,128)(2,1)S(1)}, u32[]{:S(2)}, u32[]{:S(2)}) collective-permute-start(bf16[16,144,128]{2,1,0:T(8,128)(2,1)S(1)} %all_to_all.21.refs_0_), channel_id=1, source_target_pairs={{0,6},{2,0},{4,2},{6,4},{1,7},{3,1},{5,3},{7,5},{8,14},{10,8},{12,... | collective-permute-start | bytes 1769480 | tf_op jit(solution)/shard_map/ppermute | solution.py:39
  143.8 4.7 %collective-permute-start.19 = (bf16[256,512]{1,0:T(8,128)(2,1)S(1)}, bf16[256,512]{1,0:T(8,128)(2,1)S(1)}, u32[]{:S(2)}, u32[]{:S(2)}) collective-permute-start(bf16[256,512]{1,0:T(8,128)(2,1)S(1)} %pad_maximum_fusion.3), channel_id=1, source_target_pairs={{0,8},{8,16},{16,24},{24,0},{1,9},{9,17},{17,25},{25,1},{2,10},{10... | collective-permute-start | bytes 786440 | tf_op jit(solution)/shard_map/ppermute | solution.py:39
  148.6 1.9 collective-permute-start.20
  150.6 3.1 %collective-permute-done.19 = bf16[256,512]{1,0:T(8,128)(2,1)S(1)} collective-permute-done((bf16[256,512]{1,0:T(8,128)(2,1)S(1)}, bf16[256,512]{1,0:T(8,128)(2,1)S(1)}, u32[]{:S(2)}, u32[]{:S(2)}) %collective-permute-start.19) | collective-permute-done | bytes 262176 | tf_op jit(solution)/shard_map/ppermute | solution.py:39
  153.7 4.4 %collective-permute-start.21 = (bf16[256,512]{1,0:T(8,128)(2,1)S(1)}, bf16[256,512]{1,0:T(8,128)(2,1)S(1)}, u32[]{:S(2)}, u32[]{:S(2)}) collective-permute-start(bf16[256,512]{1,0:T(8,128)(2,1)S(1)} %collective-permute-done.19), channel_id=1, source_target_pairs={{0,8},{8,16},{16,24},{24,0},{1,9},{9,17},{17,25},{25,1},{2,10},{10... | collective-permute-start | bytes 786440 | tf_op jit(solution)/shard_map/ppermute | solution.py:54
  158.1 1.9 collective-permute-start.15
  160.1 5.1 %collective-permute-start.16 = (bf16[8,144,128]{2,1,0:T(8,128)(2,1)S(1)}, bf16[8,144,128]{2,1,0:T(8,128)(2,1)S(1)}, u32[]{:S(2)}, u32[]{:S(2)}) collective-permute-start(bf16[8,144,128]{2,1,0:T(8,128)(2,1)S(1)} %slice.42), channel_id=1, source_target_pairs={{0,6},{2,0},{4,2},{6,4},{1,7},{3,1},{5,3},{7,5},{8,14},{10,8},{12,... | collective-permute-start | bytes 884744 | tf_op jit(solution)/shard_map/ppermute | solution.py:44
  165.3 4.9 %project.2 = (bf16[2,1,2,2,64,128]{5,4,3,2,1,0:T(8,128)(2,1)}, bf16[2,1,2,2,64,128]{5,4,3,2,1,0:T(8,128)(2,1)}, bf16[2,1,2,2,64,128]{5,4,3,2,1,0:T(8,128)(2,1)}, bf16[2,1,2,2,64,128]{5,4,3,2,1,0:T(8,128)(2,1)}) custom-call(s32[9]{0:T(128)} %stack.46.p_ref, bf16[2,64,2048]{2,1,0:T(8,128)(2,1)} %refs_0_.3, bf16[2,64,2048]{2,1,0:T(8,128)(2,1)} %collective-permute-done.refs_1_, ...), custom_call_target="tpu_custom_call" | custom-call | tf_op jit(solution)/shard_map/project/pallas_call | solution.py:126
  170.3 2.1 collective-permute-start.9
  175.8 3.9 %collective-permute-start.10 = (bf16[2,1,2,2,64,128]{5,4,3,2,1,0:T(8,128)(2,1)S(1)}, bf16[2,1,2,2,64,128]{5,4,3,2,1,0:T(8,128)(2,1)S(1)}, u32[]{:S(2)}, u32[]{:S(2)}) collective-permute-start(bf16[2,1,2,2,64,128]{5,4,3,2,1,0:T(8,128)(2,1)S(1)} %copy-done.22), channel_id=1, source_target_pairs={{0,2},{2,4},{4,6},{6,0},{1,3},{3,5},{5,7},{7,1},{8,10},{10,12},{12... | collective-permute-start | bytes 393224 | tf_op jit(solution)/shard_map/ppermute | solution.py:373
  179.8 2.2 collective-permute-start.11
  182.2 2.6 collective-permute-done.10
  184.9 3.9 %collective-permute-done.11 = bf16[2,1,2,2,64,128]{5,4,3,2,1,0:T(8,128)(2,1)S(1)} collective-permute-done((bf16[2,1,2,2,64,128]{5,4,3,2,1,0:T(8,128)(2,1)S(1)}, bf16[2,1,2,2,64,128]{5,4,3,2,1,0:T(8,128)(2,1)S(1)}, u32[]{:S(2)}, u32[]{:S(2)}) %collective-permute-start.11) | collective-permute-done | bytes 131104 | tf_op jit(solution)/shard_map/ppermute | solution.py:373
  188.8 2.2 collective-permute-start.22
  191.0 4.9 %collective-permute-start.23 = (bf16[4,256,512]{2,1,0:T(8,128)(2,1)S(1)}, bf16[4,256,512]{2,1,0:T(8,128)(2,1)S(1)}, u32[]{:S(2)}, u32[]{:S(2)}) collective-permute-start(bf16[4,256,512]{2,1,0:T(8,128)(2,1)S(1)} %bitcast_dynamic-update-slice_fusion.refs_0_), channel_id=1, source_target_pairs={{0,6},{2,0},{4,2},{6,4},{1,7},{3,1},{5,3},{7,5},{8,14},{10,8},{12,... | collective-permute-start | bytes 3145736 | tf_op jit(solution)/shard_map/ppermute | solution.py:39
  196.6 4.2 %all-to-all-start.2 = ((bf16[16,64,128]{2,1,0:T(8,128)(2,1)}), bf16[16,64,128]{2,1,0:T(8,128)(2,1)}, u32[]{:S(2)}, u32[]{:S(2)}) async-start(bf16[16,64,128]{2,1,0:T(8,128)(2,1)} %bitcast.28), calls=%async_computation.2 | async-start | bytes 524288 | tf_op jit(solution)/shard_map/all_to_all | solution.py:379
  200.9 1.9 collective-permute-start.17
  202.8 2.4 collective-permute-start.12
  205.2 2.1 collective-permute-start.26
  207.3 11.5 %all-to-all-done.2.q_ref = bf16[16,64,128]{2,1,0:T(8,128)(2,1)} async-done(((bf16[16,64,128]{2,1,0:T(8,128)(2,1)}), bf16[16,64,128]{2,1,0:T(8,128)(2,1)}, u32[]{:S(2)}, u32[]{:S(2)}) %all-to-all-start.2) | async-done | bytes 262176 | tf_op jit(solution)/shard_map/all_to_all | solution.py:379
  218.8 10.3 %attend.1 = bf16[16,64,128]{2,1,0:T(8,128)(2,1)} custom-call(s32[9]{0:T(128)} %stack.46.p_ref, bf16[16,64,128]{2,1,0:T(8,128)(2,1)} %all-to-all-done.2.q_ref, bf16[16,144,128]{2,1,0:T(8,128)(2,1)} %copy-done.11, bf16[16,144,128]{2,1,0:T(8,128)(2,1)} %copy-done.5, bf16[16,144,128]{2,1,0:T(8,128)(2,1)} %copy-done.6, bf16[8,144,128]{2,1,0:T(8,128)(2,1)} %copy-done.14, ...), custom_call_target="tpu_custom_call" | custom-call | tf_op jit(solution)/shard_map/attend/pallas_call | solution.py:221
  232.8 2.4 collective-permute-start.28
  235.2 1.9 collective-permute-start.24
  237.2 5.1 %collective-permute-start.25 = (bf16[2,256,512]{2,1,0:T(8,128)(2,1)}, bf16[2,256,512]{2,1,0:T(8,128)(2,1)}, u32[]{:S(2)}, u32[]{:S(2)}) collective-permute-start(bf16[2,256,512]{2,1,0:T(8,128)(2,1)} %slice.35), channel_id=1, source_target_pairs={{0,6},{2,0},{4,2},{6,4},{1,7},{3,1},{5,3},{7,5},{8,14},{10,8},{12,... | collective-permute-start | bytes 1572872 | tf_op jit(solution)/shard_map/ppermute | solution.py:44
  242.3 5.4 %all-to-all-start.3 = ((bf16[16,64,128]{2,1,0:T(8,128)(2,1)}), bf16[16,64,128]{2,1,0:T(8,128)(2,1)S(1)}, u32[]{:S(2)}, u32[]{:S(2)}) async-start(bf16[16,64,128]{2,1,0:T(8,128)(2,1)} %attend.1), calls=%async_computation.3 | async-start | bytes 524288 | tf_op jit(solution)/shard_map/all_to_all | solution.py:403
  247.8 4.7 %collective-permute-done.24.refs_3_ = bf16[2,256,512]{2,1,0:T(8,128)(2,1)} collective-permute-done((bf16[2,256,512]{2,1,0:T(8,128)(2,1)}, bf16[2,256,512]{2,1,0:T(8,128)(2,1)}, u32[]{:S(2)}, u32[]{:S(2)}) %collective-permute-start.24) | collective-permute-done | bytes 524320 | tf_op jit(solution)/shard_map/ppermute | solution.py:44
  252.5 1.9 collective-permute-start.29
  254.4 2.4 collective-permute-start.30
  256.9 2.1 pool.1.pool_ref
  259.0 7.0 %all-to-all-done.3 = bf16[16,64,128]{2,1,0:T(8,128)(2,1)S(1)} async-done(((bf16[16,64,128]{2,1,0:T(8,128)(2,1)}), bf16[16,64,128]{2,1,0:T(8,128)(2,1)S(1)}, u32[]{:S(2)}, u32[]{:S(2)}) %all-to-all-start.3) | async-done | bytes 262176 | tf_op jit(solution)/shard_map/all_to_all | solution.py:403
  266.7 6.0 %finish.1 = bf16[2,64,2048]{2,1,0:T(8,128)(2,1)} custom-call(s32[9]{0:T(128)} %stack.46.p_ref, bf16[4,2,2,64,128]{4,3,2,1,0:T(8,128)(2,1)} %pool.1.pool_ref, bf16[4,2,2,64,128]{4,3,2,1,0:T(8,128)(2,1)} %bitcast.27, bf16[4,256,512]{2,1,0:T(8,128)(2,1)} %copy-done.4, bf16[4,256,512]{2,1,0:T(8,128)(2,1)} %copy-done.9, bf16[4,256,512]{2,1,0:T(8,128)(2,1)} %copy-done.10, ...), custom_call_target="tpu_custom_call" | custom-call | tf_op jit(solution)/shard_map/finish/pallas_call | solution.py:300
  (98 shorter events, 18.9 us)
Async XLA Ops:
  2.8 35.5 %copy-start.3 = (bf16[528,512]{1,0:T(8,128)(2,1)}, bf16[528,512]{1,0:T(8,128)(2,1)S(1)}, u32[]{:S(2)}) copy-start(bf16[528,512]{1,0:T(8,128)(2,1)S(1)} %pad_maximum_fusion.2.refs_4_) | copy-start | bytes 1622020
  2.8 15.9 %collective-permute-start.3 = (bf16[528,512]{1,0:T(8,128)(2,1)S(1)}, bf16[528,512]{1,0:T(8,128)(2,1)S(1)}, u32[]{:S(2)}, u32[]{:S(2)}) collective-permute-start(bf16[528,512]{1,0:T(8,128)(2,1)S(1)} %pad_maximum_fusion.2.refs_4_), channel_id=1, source_target_pairs={{0,8},{8,16},{16,24},{24,0},{1,9},{9,17},{17,25},{25,1},{2,10},{10... | collective-permute-start | bytes 1622024 | tf_op jit(solution)/shard_map/ppermute | solution.py:39
  6.0 15.9 %collective-permute-start.4 = (bf16[528,512]{1,0:T(8,128)(2,1)S(1)}, bf16[528,512]{1,0:T(8,128)(2,1)S(1)}, u32[]{:S(2)}, u32[]{:S(2)}) collective-permute-start(bf16[528,512]{1,0:T(8,128)(2,1)S(1)} %pad_maximum_fusion.2.refs_4_), channel_id=1, source_target_pairs={{0,24},{8,0},{16,8},{24,16},{1,25},{9,1},{17,9},{25,17},{2,26},{10... | collective-permute-start | bytes 1622024 | tf_op jit(solution)/shard_map/ppermute | solution.py:39
  18.7 14.3 %copy-start = (bf16[528,512]{1,0:T(8,128)(2,1)}, bf16[528,512]{1,0:T(8,128)(2,1)S(1)}, u32[]{:S(2)}) copy-start(bf16[528,512]{1,0:T(8,128)(2,1)S(1)} %collective-permute-done.3.refs_5_) | copy-start | bytes 1622020
  18.8 9.3 %collective-permute-start.5 = (bf16[264,512]{1,0:T(8,128)(2,1)S(1)}, bf16[264,512]{1,0:T(8,128)(2,1)S(1)}, u32[]{:S(2)}, u32[]{:S(2)}) collective-permute-start(bf16[264,512]{1,0:T(8,128)(2,1)S(1)} %slice.36), channel_id=1, source_target_pairs={{0,8},{8,16},{16,24},{24,0},{1,9},{9,17},{17,25},{25,1},{2,10},{10... | collective-permute-start | bytes 811016 | tf_op jit(solution)/shard_map/ppermute | solution.py:44
  22.0 9.0 %collective-permute-start.6 = (bf16[264,512]{1,0:T(8,128)(2,1)S(1)}, bf16[264,512]{1,0:T(8,128)(2,1)S(1)}, u32[]{:S(2)}, u32[]{:S(2)}) collective-permute-start(bf16[264,512]{1,0:T(8,128)(2,1)S(1)} %slice.37), channel_id=1, source_target_pairs={{0,24},{8,0},{16,8},{24,16},{1,25},{9,1},{17,9},{25,17},{2,26},{10... | collective-permute-start | bytes 811016 | tf_op jit(solution)/shard_map/ppermute | solution.py:44
  28.0 41.5 %copy-start.7 = (bf16[264,512]{1,0:T(8,128)(2,1)}, bf16[264,512]{1,0:T(8,128)(2,1)S(1)}, u32[]{:S(2)}) copy-start(bf16[264,512]{1,0:T(8,128)(2,1)S(1)} %collective-permute-done.5.refs_7_) | copy-start | bytes 811012
  33.0 36.5 %collective-permute-start.8 = (bf16[1584,512]{1,0:T(8,128)(2,1)}, bf16[1584,512]{1,0:T(8,128)(2,1)S(1)}, u32[]{:S(2)}, u32[]{:S(2)}) collective-permute-start(bf16[1584,512]{1,0:T(8,128)(2,1)} %pad_maximum_fusion.1), channel_id=1, source_target_pairs={{0,1},{1,0},{2,3},{3,2},{4,5},{5,4},{6,7},{7,6},{8,9},{9,8},{10,11... | collective-permute-start | bytes 4866056 | tf_op jit(solution)/shard_map/ppermute | solution.py:31
  34.9 17.8 %collective-permute-start = (bf16[2,64,2048]{2,1,0:T(8,128)(2,1)}, bf16[2,64,2048]{2,1,0:T(8,128)(2,1)}, u32[]{:S(2)}, u32[]{:S(2)}) collective-permute-start(bf16[2,64,2048]{2,1,0:T(8,128)(2,1)} %refs_0_.3), channel_id=1, source_target_pairs={{0,2},{2,4},{4,6},{6,0},{1,3},{3,5},{5,7},{7,1},{8,10},{10,12},{12... | collective-permute-start | bytes 1572872 | tf_op jit(solution)/shard_map/ppermute | solution.py:39
  38.4 18.5 %collective-permute-start.7 = (bf16[528,512]{1,0:T(8,128)(2,1)S(1)}, bf16[528,512]{1,0:T(8,128)(2,1)S(1)}, u32[]{:S(2)}, u32[]{:S(2)}) collective-permute-start(bf16[528,512]{1,0:T(8,128)(2,1)S(1)} %pad_maximum_fusion.2.refs_4_), channel_id=1, source_target_pairs={{0,1},{1,0},{2,3},{3,2},{4,5},{5,4},{6,7},{7,6},{8,9},{9,8},{10,11... | collective-permute-start | bytes 1622024 | tf_op jit(solution)/shard_map/ppermute | solution.py:31
  40.5 16.3 %collective-permute-start.1 = (bf16[2,64,2048]{2,1,0:T(8,128)(2,1)}, bf16[2,64,2048]{2,1,0:T(8,128)(2,1)}, u32[]{:S(2)}, u32[]{:S(2)}) collective-permute-start(bf16[2,64,2048]{2,1,0:T(8,128)(2,1)} %refs_0_.3), channel_id=1, source_target_pairs={{0,6},{2,0},{4,2},{6,4},{1,7},{3,1},{5,3},{7,5},{8,14},{10,8},{12,... | collective-permute-start | bytes 1572872 | tf_op jit(solution)/shard_map/ppermute | solution.py:39
  52.7 16.9 %collective-permute-start.2 = (bf16[2,64,2048]{2,1,0:T(8,128)(2,1)}, bf16[2,64,2048]{2,1,0:T(8,128)(2,1)}, u32[]{:S(2)}, u32[]{:S(2)}) collective-permute-start(bf16[2,64,2048]{2,1,0:T(8,128)(2,1)} %collective-permute-done.refs_1_), channel_id=1, source_target_pairs={{0,2},{2,4},{4,6},{6,0},{1,3},{3,5},{5,7},{7,1},{8,10},{10,12},{12... | collective-permute-start | bytes 1572872 | tf_op jit(solution)/shard_map/ppermute | solution.py:54
  56.8 12.7 %copy-start.12 = (bf16[528,512]{1,0:T(8,128)(2,1)}, bf16[528,512]{1,0:T(8,128)(2,1)S(1)}, u32[]{:S(2)}) copy-start(bf16[528,512]{1,0:T(8,128)(2,1)S(1)} %collective-permute-done.7.refs_9_) | copy-start | bytes 1622020
  75.8 68.0 %copy-start.18 = (bf16[128,512]{1,0:T(8,128)(2,1)S(1)}, bf16[128,512]{1,0:T(8,128)(2,1)}, u32[]{:S(2)}) copy-start(bf16[128,512]{1,0:T(8,128)(2,1)} %param.21) | copy-start | bytes 393220
  75.8 68.0 %copy-start.19 = (bf16[128,512]{1,0:T(8,128)(2,1)S(1)}, bf16[128,512]{1,0:T(8,128)(2,1)}, u32[]{:S(2)}) copy-start(bf16[128,512]{1,0:T(8,128)(2,1)} %param.20) | copy-start | bytes 393220
  136.7 28.6 %copy-start.11 = (bf16[16,144,128]{2,1,0:T(8,128)(2,1)}, bf16[16,144,128]{2,1,0:T(8,128)(2,1)S(1)}, u32[]{:S(2)}) copy-start(bf16[16,144,128]{2,1,0:T(8,128)(2,1)S(1)} %all_to_all.21.refs_0_) | copy-start | bytes 1769476
  136.7 21.4 %collective-permute-start.13 = (bf16[16,144,128]{2,1,0:T(8,128)(2,1)S(1)}, bf16[16,144,128]{2,1,0:T(8,128)(2,1)S(1)}, u32[]{:S(2)}, u32[]{:S(2)}) collective-permute-start(bf16[16,144,128]{2,1,0:T(8,128)(2,1)S(1)} %all_to_all.21.refs_0_), channel_id=1, source_target_pairs={{0,2},{2,4},{4,6},{6,0},{1,3},{3,5},{5,7},{7,1},{8,10},{10,12},{12... | collective-permute-start | bytes 1769480 | tf_op jit(solution)/shard_map/ppermute | solution.py:39
  139.2 20.9 %collective-permute-start.14 = (bf16[16,144,128]{2,1,0:T(8,128)(2,1)S(1)}, bf16[16,144,128]{2,1,0:T(8,128)(2,1)S(1)}, u32[]{:S(2)}, u32[]{:S(2)}) collective-permute-start(bf16[16,144,128]{2,1,0:T(8,128)(2,1)S(1)} %all_to_all.21.refs_0_), channel_id=1, source_target_pairs={{0,6},{2,0},{4,2},{6,4},{1,7},{3,1},{5,3},{7,5},{8,14},{10,8},{12,... | collective-permute-start | bytes 1769480 | tf_op jit(solution)/shard_map/ppermute | solution.py:39
  143.8 9.9 %collective-permute-start.19 = (bf16[256,512]{1,0:T(8,128)(2,1)S(1)}, bf16[256,512]{1,0:T(8,128)(2,1)S(1)}, u32[]{:S(2)}, u32[]{:S(2)}) collective-permute-start(bf16[256,512]{1,0:T(8,128)(2,1)S(1)} %pad_maximum_fusion.3), channel_id=1, source_target_pairs={{0,8},{8,16},{16,24},{24,0},{1,9},{9,17},{17,25},{25,1},{2,10},{10... | collective-permute-start | bytes 786440 | tf_op jit(solution)/shard_map/ppermute | solution.py:39
  148.6 16.7 %collective-permute-start.20 = (bf16[256,512]{1,0:T(8,128)(2,1)S(1)}, bf16[256,512]{1,0:T(8,128)(2,1)S(1)}, u32[]{:S(2)}, u32[]{:S(2)}) collective-permute-start(bf16[256,512]{1,0:T(8,128)(2,1)S(1)} %pad_maximum_fusion.3), channel_id=1, source_target_pairs={{0,24},{8,0},{16,8},{24,16},{1,25},{9,1},{17,9},{25,17},{2,26},{10... | collective-permute-start | bytes 786440 | tf_op jit(solution)/shard_map/ppermute | solution.py:39
  153.7 22.1 %collective-permute-start.21 = (bf16[256,512]{1,0:T(8,128)(2,1)S(1)}, bf16[256,512]{1,0:T(8,128)(2,1)S(1)}, u32[]{:S(2)}, u32[]{:S(2)}) collective-permute-start(bf16[256,512]{1,0:T(8,128)(2,1)S(1)} %collective-permute-done.19), channel_id=1, source_target_pairs={{0,8},{8,16},{16,24},{24,0},{1,9},{9,17},{17,25},{25,1},{2,10},{10... | collective-permute-start | bytes 786440 | tf_op jit(solution)/shard_map/ppermute | solution.py:54
  158.1 14.3 %copy-start.5 = (bf16[16,144,128]{2,1,0:T(8,128)(2,1)}, bf16[16,144,128]{2,1,0:T(8,128)(2,1)S(1)}, u32[]{:S(2)}) copy-start(bf16[16,144,128]{2,1,0:T(8,128)(2,1)S(1)} %collective-permute-done.13.refs_1_) | copy-start | bytes 1769476
  158.1 14.2 %collective-permute-start.15 = (bf16[8,144,128]{2,1,0:T(8,128)(2,1)S(1)}, bf16[8,144,128]{2,1,0:T(8,128)(2,1)S(1)}, u32[]{:S(2)}, u32[]{:S(2)}) collective-permute-start(bf16[8,144,128]{2,1,0:T(8,128)(2,1)S(1)} %slice.41), channel_id=1, source_target_pairs={{0,2},{2,4},{4,6},{6,0},{1,3},{3,5},{5,7},{7,1},{8,10},{10,12},{12... | collective-permute-start | bytes 884744 | tf_op jit(solution)/shard_map/ppermute | solution.py:44
  160.1 12.3 %copy-start.6 = (bf16[16,144,128]{2,1,0:T(8,128)(2,1)}, bf16[16,144,128]{2,1,0:T(8,128)(2,1)S(1)}, u32[]{:S(2)}) copy-start(bf16[16,144,128]{2,1,0:T(8,128)(2,1)S(1)} %collective-permute-done.14.refs_2_) | copy-start | bytes 1769476
  160.1 12.2 %collective-permute-start.16 = (bf16[8,144,128]{2,1,0:T(8,128)(2,1)S(1)}, bf16[8,144,128]{2,1,0:T(8,128)(2,1)S(1)}, u32[]{:S(2)}, u32[]{:S(2)}) collective-permute-start(bf16[8,144,128]{2,1,0:T(8,128)(2,1)S(1)} %slice.42), channel_id=1, source_target_pairs={{0,6},{2,0},{4,2},{6,4},{1,7},{3,1},{5,3},{7,5},{8,14},{10,8},{12,... | collective-permute-start | bytes 884744 | tf_op jit(solution)/shard_map/ppermute | solution.py:44
  170.2 11.9 %copy-start.17 = (bf16[2,1,2,2,64,128]{5,4,3,2,1,0:T(8,128)(2,1)S(1)}, bf16[2,1,2,2,64,128]{5,4,3,2,1,0:T(8,128)(2,1)}, u32[]{:S(2)}) copy-start(bf16[2,1,2,2,64,128]{5,4,3,2,1,0:T(8,128)(2,1)} %get-tuple-element.14) | copy-start | bytes 393220
  170.3 11.9 %collective-permute-start.9 = (bf16[2,1,2,2,64,128]{5,4,3,2,1,0:T(8,128)(2,1)}, bf16[2,1,2,2,64,128]{5,4,3,2,1,0:T(8,128)(2,1)S(1)}, u32[]{:S(2)}, u32[]{:S(2)}) collective-permute-start(bf16[2,1,2,2,64,128]{5,4,3,2,1,0:T(8,128)(2,1)} %get-tuple-element.15), channel_id=1, source_target_pairs={{0,6},{2,0},{4,2},{6,4},{1,7},{3,1},{5,3},{7,5},{8,14},{10,8},{12,... | collective-permute-start | bytes 393224 | tf_op jit(solution)/shard_map/ppermute | solution.py:373
  173.8 45.0 %collective-permute-start.18 = (bf16[48,144,128]{2,1,0:T(8,128)(2,1)}, bf16[48,144,128]{2,1,0:T(8,128)(2,1)}, u32[]{:S(2)}, u32[]{:S(2)}) collective-permute-start(bf16[48,144,128]{2,1,0:T(8,128)(2,1)} %pad_maximum_fusion), channel_id=1, source_target_pairs={{0,1},{1,0},{2,3},{3,2},{4,5},{5,4},{6,7},{7,6},{8,9},{9,8},{10,11... | collective-permute-start | bytes 5308424 | tf_op jit(solution)/shard_map/ppermute | solution.py:31
  175.8 53.3 %copy-start.4 = (bf16[4,256,512]{2,1,0:T(8,128)(2,1)}, bf16[4,256,512]{2,1,0:T(8,128)(2,1)S(1)}, u32[]{:S(2)}) copy-start(bf16[4,256,512]{2,1,0:T(8,128)(2,1)S(1)} %bitcast_dynamic-update-slice_fusion.refs_0_) | copy-start | bytes 3145732
  175.8 9.0 %collective-permute-start.10 = (bf16[2,1,2,2,64,128]{5,4,3,2,1,0:T(8,128)(2,1)S(1)}, bf16[2,1,2,2,64,128]{5,4,3,2,1,0:T(8,128)(2,1)S(1)}, u32[]{:S(2)}, u32[]{:S(2)}) collective-permute-start(bf16[2,1,2,2,64,128]{5,4,3,2,1,0:T(8,128)(2,1)S(1)} %copy-done.22), channel_id=1, source_target_pairs={{0,2},{2,4},{4,6},{6,0},{1,3},{3,5},{5,7},{7,1},{8,10},{10,12},{12... | collective-permute-start | bytes 393224 | tf_op jit(solution)/shard_map/ppermute | solution.py:373
  179.8 9.0 %collective-permute-start.11 = (bf16[2,1,2,2,64,128]{5,4,3,2,1,0:T(8,128)(2,1)S(1)}, bf16[2,1,2,2,64,128]{5,4,3,2,1,0:T(8,128)(2,1)S(1)}, u32[]{:S(2)}, u32[]{:S(2)}) collective-permute-start(bf16[2,1,2,2,64,128]{5,4,3,2,1,0:T(8,128)(2,1)S(1)} %copy-done.21), channel_id=1, source_target_pairs={{0,4},{2,6},{4,0},{6,2},{1,5},{3,7},{5,1},{7,3},{8,12},{10,14},{12... | collective-permute-start | bytes 393224 | tf_op jit(solution)/shard_map/ppermute | solution.py:373
  188.8 40.3 %collective-permute-start.22 = (bf16[4,256,512]{2,1,0:T(8,128)(2,1)S(1)}, bf16[4,256,512]{2,1,0:T(8,128)(2,1)S(1)}, u32[]{:S(2)}, u32[]{:S(2)}) collective-permute-start(bf16[4,256,512]{2,1,0:T(8,128)(2,1)S(1)} %bitcast_dynamic-update-slice_fusion.refs_0_), channel_id=1, source_target_pairs={{0,2},{2,4},{4,6},{6,0},{1,3},{3,5},{5,7},{7,1},{8,10},{10,12},{12... | collective-permute-start | bytes 3145736 | tf_op jit(solution)/shard_map/ppermute | solution.py:39
  191.0 38.1 %collective-permute-start.23 = (bf16[4,256,512]{2,1,0:T(8,128)(2,1)S(1)}, bf16[4,256,512]{2,1,0:T(8,128)(2,1)S(1)}, u32[]{:S(2)}, u32[]{:S(2)}) collective-permute-start(bf16[4,256,512]{2,1,0:T(8,128)(2,1)S(1)} %bitcast_dynamic-update-slice_fusion.refs_0_), channel_id=1, source_target_pairs={{0,6},{2,0},{4,2},{6,4},{1,7},{3,1},{5,3},{7,5},{8,14},{10,8},{12,... | collective-permute-start | bytes 3145736 | tf_op jit(solution)/shard_map/ppermute | solution.py:39
  196.6 32.5 %copy-start.13 = (bf16[4,2,2,64,128]{4,3,2,1,0:T(8,128)(2,1)}, bf16[4,2,2,64,128]{4,3,2,1,0:T(8,128)(2,1)S(1)}, u32[]{:S(2)}) copy-start(bf16[4,2,2,64,128]{4,3,2,1,0:T(8,128)(2,1)S(1)} %get-tuple-element.24.in_ref) | copy-start | bytes 786436
  196.6 22.2 %all-to-all-start.2 = ((bf16[16,64,128]{2,1,0:T(8,128)(2,1)}), bf16[16,64,128]{2,1,0:T(8,128)(2,1)}, u32[]{:S(2)}, u32[]{:S(2)}) async-start(bf16[16,64,128]{2,1,0:T(8,128)(2,1)} %bitcast.28), calls=%async_computation.2 | async-start | bytes 524288 | tf_op jit(solution)/shard_map/all_to_all | solution.py:379
  200.9 4.4 %collective-permute-start.17 = (bf16[16,144,128]{2,1,0:T(8,128)(2,1)}, bf16[16,144,128]{2,1,0:T(8,128)(2,1)}, u32[]{:S(2)}, u32[]{:S(2)}) collective-permute-start(bf16[16,144,128]{2,1,0:T(8,128)(2,1)} %copy-done.11), channel_id=1, source_target_pairs={{0,1},{1,0},{2,3},{3,2},{4,5},{5,4},{6,7},{7,6},{8,9},{9,8},{10,11... | collective-permute-start | bytes 1769480 | tf_op jit(solution)/shard_map/ppermute | solution.py:31
  202.8 34.4 %collective-permute-start.12 = (bf16[4,2,2,16,128]{4,3,2,1,0:T(8,128)(2,1)S(1)}, bf16[4,2,2,16,128]{4,3,2,1,0:T(8,128)(2,1)S(1)}, u32[]{:S(2)}, u32[]{:S(2)}) collective-permute-start(bf16[4,2,2,16,128]{4,3,2,1,0:T(8,128)(2,1)S(1)} %slice.39), channel_id=1, source_target_pairs={{0,1},{1,2},{2,3},{3,4},{4,5},{5,6},{6,7},{7,32},{32,33},{33,34},{... | collective-permute-start | bytes 196616 | tf_op jit(solution)/shard_map/ppermute | solution.py:382
  205.2 53.8 %collective-permute-start.26 = (bf16[4,256,512]{2,1,0:T(8,128)(2,1)S(1)}, bf16[4,256,512]{2,1,0:T(8,128)(2,1)}, u32[]{:S(2)}, u32[]{:S(2)}) collective-permute-start(bf16[4,256,512]{2,1,0:T(8,128)(2,1)S(1)} %bitcast_dynamic-update-slice_fusion.refs_0_), channel_id=1, source_target_pairs={{0,1},{1,0},{2,3},{3,2},{4,5},{5,4},{6,7},{7,6},{8,9},{9,8},{10,11... | collective-permute-start | bytes 3145736 | tf_op jit(solution)/shard_map/ppermute | solution.py:31
  229.1 36.9 %copy-start.9 = (bf16[4,256,512]{2,1,0:T(8,128)(2,1)}, bf16[4,256,512]{2,1,0:T(8,128)(2,1)S(1)}, u32[]{:S(2)}) copy-start(bf16[4,256,512]{2,1,0:T(8,128)(2,1)S(1)} %collective-permute-done.22.refs_1_) | copy-start | bytes 3145732
  229.2 36.9 %copy-start.10 = (bf16[4,256,512]{2,1,0:T(8,128)(2,1)}, bf16[4,256,512]{2,1,0:T(8,128)(2,1)S(1)}, u32[]{:S(2)}) copy-start(bf16[4,256,512]{2,1,0:T(8,128)(2,1)S(1)} %collective-permute-done.23.refs_2_) | copy-start | bytes 3145732
  230.1 35.9 %collective-permute-start.27 = (bf16[4,256,512]{2,1,0:T(8,128)(2,1)S(1)}, bf16[4,256,512]{2,1,0:T(8,128)(2,1)}, u32[]{:S(2)}, u32[]{:S(2)}) collective-permute-start(bf16[4,256,512]{2,1,0:T(8,128)(2,1)S(1)} %collective-permute-done.22.refs_1_), channel_id=1, source_target_pairs={{0,1},{1,0},{2,3},{3,2},{4,5},{5,4},{6,7},{7,6},{8,9},{9,8},{10,11... | collective-permute-start | bytes 3145736 | tf_op jit(solution)/shard_map/ppermute | solution.py:31
  232.8 33.2 %collective-permute-start.28 = (bf16[4,256,512]{2,1,0:T(8,128)(2,1)S(1)}, bf16[4,256,512]{2,1,0:T(8,128)(2,1)}, u32[]{:S(2)}, u32[]{:S(2)}) collective-permute-start(bf16[4,256,512]{2,1,0:T(8,128)(2,1)S(1)} %collective-permute-done.23.refs_2_), channel_id=1, source_target_pairs={{0,1},{1,0},{2,3},{3,2},{4,5},{5,4},{6,7},{7,6},{8,9},{9,8},{10,11... | collective-permute-start | bytes 3145736 | tf_op jit(solution)/shard_map/ppermute | solution.py:31
  235.2 17.3 %collective-permute-start.24 = (bf16[2,256,512]{2,1,0:T(8,128)(2,1)}, bf16[2,256,512]{2,1,0:T(8,128)(2,1)}, u32[]{:S(2)}, u32[]{:S(2)}) collective-permute-start(bf16[2,256,512]{2,1,0:T(8,128)(2,1)} %slice.34), channel_id=1, source_target_pairs={{0,2},{2,4},{4,6},{6,0},{1,3},{3,5},{5,7},{7,1},{8,10},{10,12},{12... | collective-permute-start | bytes 1572872 | tf_op jit(solution)/shard_map/ppermute | solution.py:44
  237.2 19.7 %copy-start.20 = (bf16[4,2,2,16,128]{4,3,2,1,0:T(8,128)(2,1)}, bf16[4,2,2,16,128]{4,3,2,1,0:T(8,128)(2,1)S(1)}, u32[]{:S(2)}) copy-start(bf16[4,2,2,16,128]{4,3,2,1,0:T(8,128)(2,1)S(1)} %collective-permute-done.12.edge_ref) | copy-start | bytes 196612
  237.2 17.2 %collective-permute-start.25 = (bf16[2,256,512]{2,1,0:T(8,128)(2,1)}, bf16[2,256,512]{2,1,0:T(8,128)(2,1)}, u32[]{:S(2)}, u32[]{:S(2)}) collective-permute-start(bf16[2,256,512]{2,1,0:T(8,128)(2,1)} %slice.35), channel_id=1, source_target_pairs={{0,6},{2,0},{4,2},{6,4},{1,7},{3,1},{5,3},{7,5},{8,14},{10,8},{12,... | collective-permute-start | bytes 1572872 | tf_op jit(solution)/shard_map/ppermute | solution.py:44
  242.3 23.7 %all-to-all-start.3 = ((bf16[16,64,128]{2,1,0:T(8,128)(2,1)}), bf16[16,64,128]{2,1,0:T(8,128)(2,1)S(1)}, u32[]{:S(2)}, u32[]{:S(2)}) async-start(bf16[16,64,128]{2,1,0:T(8,128)(2,1)} %attend.1), calls=%async_computation.3 | async-start | bytes 524288 | tf_op jit(solution)/shard_map/all_to_all | solution.py:403
  252.5 13.5 %collective-permute-start.29 = (bf16[2,256,512]{2,1,0:T(8,128)(2,1)}, bf16[2,256,512]{2,1,0:T(8,128)(2,1)}, u32[]{:S(2)}, u32[]{:S(2)}) collective-permute-start(bf16[2,256,512]{2,1,0:T(8,128)(2,1)} %collective-permute-done.24.refs_3_), channel_id=1, source_target_pairs={{0,1},{1,0},{2,3},{3,2},{4,5},{5,4},{6,7},{7,6},{8,9},{9,8},{10,11... | collective-permute-start | bytes 1572872 | tf_op jit(solution)/shard_map/ppermute | solution.py:31
  254.4 11.6 %collective-permute-start.30 = (bf16[2,256,512]{2,1,0:T(8,128)(2,1)}, bf16[2,256,512]{2,1,0:T(8,128)(2,1)}, u32[]{:S(2)}, u32[]{:S(2)}) collective-permute-start(bf16[2,256,512]{2,1,0:T(8,128)(2,1)} %collective-permute-done.25.refs_4_), channel_id=1, source_target_pairs={{0,1},{1,0},{2,3},{3,2},{4,5},{5,4},{6,7},{7,6},{8,9},{9,8},{10,11... | collective-permute-start | bytes 1572872 | tf_op jit(solution)/shard_map/ppermute | solution.py:31
  (8 other events, 35.7 us)

commit v6 on v5

--- a/solution.py
+++ b/solution.py
@@ -59,7 +59,7 @@
     kinds = len(factors)
 
     def body(p_ref, *refs):
-        xs, own_refs, other_refs, outs = refs[:4], refs[4:9], refs[9:11], refs[11:]
+        xs, own_refs, other_refs, outs = refs[:5], refs[5:10], refs[10:12], refs[12:]
         deep = own_refs[0].shape[0] - GATE_ROWS
         tall = deep + GATE_ROWS
         lane = lax.broadcasted_iota(jnp.int32, (GATE_ROWS, HD), 1)
@@ -125,7 +125,7 @@
         shapes = [(4, seqs, 2, kinds * rows + GATE_ROWS, HD)]
     outs = pl.pallas_call(
         body,
-        in_specs=[whole(pltpu.SMEM)] + [whole()] * 11,
+        in_specs=[whole(pltpu.SMEM)] + [whole()] * 12,
         out_specs=[whole()] * len(shapes),
         out_shape=[jax.ShapeDtypeStruct(sh, BF16) for sh in shapes],
         compiler_params=params(),
@@ -348,7 +348,7 @@
 
     deep = w_key.shape[0]
     gain = lax.dynamic_slice_in_dim(norm_gain, y * deep, deep, 0)
-    all_rows = ring_in_three(tokens, "tp_0")
+    all_rows = ring_of_four(tokens, "tp_0")
     weights = jnp.concatenate([w_key, w_value, w_query, w_pool_in], axis=1)
     weights = (weights.astype(F32) * gain[:, None]).astype(BF16)
     here = lax.dynamic_slice_in_dim(gate_cache[:, 0], z * block, block, 1)

time: 274 us -> 273 us (level)
  waiting for transfers between devices: 71.8 us -> 63.1 us
  starting transfers between devices: 98.9 us -> 104 us
    ppermute x2 -> x1, waiting for transfers between devices: 12.7 us -> 0.01 us  [ring_in_three(): return (x, *near, lax.ppermute(near[0], axis, UP))]
    ppermute x3 -> x4, starting transfers between devices: 12.9 us -> 17.8 us  [relays(): lax.ppermute(after[half:], axis, DOWN)]
    ppermute x3 -> x4, waiting for transfers between devices: 8.08 us -> 10.7 us  [relays(): lax.ppermute(before[:half], axis, UP)]
    ppermute x3 -> x4, starting transfers between devices: 7.03 us -> 9.34 us  [relays(): lax.ppermute(before[:half], axis, UP)]
    ppermute x2 -> x1, starting transfers between devices: 6.56 us -> 4.38 us  [ring_in_three(): return (x, *near, lax.ppermute(near[0], axis, UP))]
  transfers between devices with their start and end apart: 33 -> 34, of which waited for: 12 -> 12; matrix products, arithmetic and copies ran while one was open for 2% -> 2% of each run, Pallas kernels for 6% -> 6%
where the time goes in v6:
time: 273 us; the launch traced here: 271 us
  starting transfers between devices  104 us (38%)
  waiting for transfers between devices  63.1 us (23%)
  blocking collectives  61.6 us (23%)
  Pallas kernels  28.4 us (10%)
  local copies, waits for them, and re-layouts  8.54 us (3%)
  other arithmetic  4.81 us (2%)
    all_to_all x1, blocking collectives, on_device(): lax.all_to_all(kv_here.reshape(planes, 2 * rows + GATE_ROWS, HD), 'sp', 0...  47.6 us
    ppermute x10, starting transfers between devices, hops(): return (lax.ppermute(x, axis, UP), lax.ppermute(x, axis, DOWN))  33.6 us
    ppermute x10, waiting for transfers between devices, hops(): return (lax.ppermute(x, axis, UP), lax.ppermute(x, axis, DOWN))  22.2 us
    ppermute x9, starting transfers between devices, sibling(): return lax.ppermute(x, 'tp_1', [(0, 1), (1, 0)])  18.4 us
    ppermute x4, starting transfers between devices, relays(): lax.ppermute(after[half:], axis, DOWN)  17.8 us
    all_to_all x1, blocking collectives, on_device(): kv_here = lax.all_to_all(kv, 'tp_0', 0, 0, tiled=True)  14 us
    all_to_all x1, waiting for transfers between devices, on_device(): q = lax.all_to_all(q, 'sp', 0, 0, tiled=True)  11.5 us
    ppermute x4, waiting for transfers between devices, relays(): lax.ppermute(before[:half], axis, UP)  10.7 us
  transfers between devices with their start and end apart: 34, of which 12 were waited for; matrix products, arithmetic and copies ran while one was open for 2% of the time, Pallas kernels for 6%

profile of v6, /device:TPU:16, one launch (start us, length us, event | category | flops | bytes accessed | tf_op | source)
XLA Modules:
  0.0 271.2 jit_solution(11644209387655627527)
XLA Ops:
  2.8 3.2 %collective-permute-start.4 = (bf16[528,512]{1,0:T(8,128)(2,1)S(1)}, bf16[528,512]{1,0:T(8,128)(2,1)S(1)}, u32[]{:S(2)}, u32[]{:S(2)}) collective-permute-start(bf16[528,512]{1,0:T(8,128)(2,1)S(1)} %pad_maximum_fusion.2.refs_5_), channel_id=1, source_target_pairs={{0,8},{8,16},{16,24},{24,0},{1,9},{9,17},{17,25},{25,1},{2,10},{10... | collective-permute-start | bytes 1622024 | tf_op jit(solution)/shard_map/ppermute | solution.py:39
  6.0 2.7 collective-permute-start.5
  8.7 10.1 %collective-permute-done.4.refs_6_ = bf16[528,512]{1,0:T(8,128)(2,1)S(1)} collective-permute-done((bf16[528,512]{1,0:T(8,128)(2,1)S(1)}, bf16[528,512]{1,0:T(8,128)(2,1)S(1)}, u32[]{:S(2)}, u32[]{:S(2)}) %collective-permute-start.4) | collective-permute-done | bytes 540704 | tf_op jit(solution)/shard_map/ppermute | solution.py:39
  18.8 3.3 %collective-permute-start.6 = (bf16[264,512]{1,0:T(8,128)(2,1)S(1)}, bf16[264,512]{1,0:T(8,128)(2,1)S(1)}, u32[]{:S(2)}, u32[]{:S(2)}) collective-permute-start(bf16[264,512]{1,0:T(8,128)(2,1)S(1)} %slice.46), channel_id=1, source_target_pairs={{0,8},{8,16},{16,24},{24,0},{1,9},{9,17},{17,25},{25,1},{2,10},{10... | collective-permute-start | bytes 811016 | tf_op jit(solution)/shard_map/ppermute | solution.py:44
  22.1 2.7 collective-permute-start.7
  24.8 3.4 %collective-permute-done.6.refs_8_ = bf16[264,512]{1,0:T(8,128)(2,1)S(1)} collective-permute-done((bf16[264,512]{1,0:T(8,128)(2,1)S(1)}, bf16[264,512]{1,0:T(8,128)(2,1)S(1)}, u32[]{:S(2)}, u32[]{:S(2)}) %collective-permute-start.6) | collective-permute-done | bytes 270368 | tf_op jit(solution)/shard_map/ppermute | solution.py:44
  28.2 3.0 %collective-permute-done.7.refs_9_ = bf16[264,512]{1,0:T(8,128)(2,1)S(1)} collective-permute-done((bf16[264,512]{1,0:T(8,128)(2,1)S(1)}, bf16[264,512]{1,0:T(8,128)(2,1)S(1)}, u32[]{:S(2)}, u32[]{:S(2)}) %collective-permute-start.7) | collective-permute-done | bytes 270368 | tf_op jit(solution)/shard_map/ppermute | solution.py:44
  35.1 3.4 %collective-permute-start = (bf16[2,64,2048]{2,1,0:T(8,128)(2,1)S(1)}, bf16[2,64,2048]{2,1,0:T(8,128)(2,1)S(1)}, u32[]{:S(2)}, u32[]{:S(2)}) collective-permute-start(bf16[2,64,2048]{2,1,0:T(8,128)(2,1)S(1)} %copy-done.14), channel_id=1, source_target_pairs={{0,2},{2,4},{4,6},{6,0},{1,3},{3,5},{5,7},{7,1},{8,10},{10,12},{12... | collective-permute-start | bytes 1572872 | tf_op jit(solution)/shard_map/ppermute | solution.py:39
  38.5 3.7 %collective-permute-start.1 = (bf16[2,64,2048]{2,1,0:T(8,128)(2,1)S(1)}, bf16[2,64,2048]{2,1,0:T(8,128)(2,1)S(1)}, u32[]{:S(2)}, u32[]{:S(2)}) collective-permute-start(bf16[2,64,2048]{2,1,0:T(8,128)(2,1)S(1)} %copy-done.14), channel_id=1, source_target_pairs={{0,6},{2,0},{4,2},{6,4},{1,7},{3,1},{5,3},{7,5},{8,14},{10,8},{12,... | collective-permute-start | bytes 1572872 | tf_op jit(solution)/shard_map/ppermute | solution.py:39
  42.1 1.9 collective-permute-start.8
  44.1 8.4 %collective-permute-done.refs_1_ = bf16[2,64,2048]{2,1,0:T(8,128)(2,1)S(1)} collective-permute-done((bf16[2,64,2048]{2,1,0:T(8,128)(2,1)S(1)}, bf16[2,64,2048]{2,1,0:T(8,128)(2,1)S(1)}, u32[]{:S(2)}, u32[]{:S(2)}) %collective-permute-start) | collective-permute-done | bytes 524320 | tf_op jit(solution)/shard_map/ppermute | solution.py:39
  53.3 2.2 collective-permute-start.2
  56.3 4.9 %collective-permute-start.3 = (bf16[1,64,2048]{2,1,0:T(8,128)(2,1)}, bf16[1,64,2048]{2,1,0:T(8,128)(2,1)}, u32[]{:S(2)}, u32[]{:S(2)}) collective-permute-start(bf16[1,64,2048]{2,1,0:T(8,128)(2,1)} %slice.45), channel_id=1, source_target_pairs={{0,6},{2,0},{4,2},{6,4},{1,7},{3,1},{5,3},{7,5},{8,14},{10,8},{12,... | collective-permute-start | bytes 786440 | tf_op jit(solution)/shard_map/ppermute | solution.py:44
  61.8 2.6 collective-permute-done.2.refs_3_
  64.4 2.1 collective-permute-done.3.refs_4_
  67.7 5.0 %project.3 = bf16[4,2,2,144,128]{4,3,2,1,0:T(8,128)(2,1)} custom-call(s32[9]{0:T(128)} %stack.46.p_ref, bf16[2,64,2048]{2,1,0:T(8,128)(2,1)} %refs_0_.3, bf16[2,64,2048]{2,1,0:T(8,128)(2,1)} %copy-done.7, bf16[2,64,2048]{2,1,0:T(8,128)(2,1)} %copy-done.8, bf16[1,64,2048]{2,1,0:T(8,128)(2,1)} %copy-done.18, ...), custom_call_target="tpu_custom_call" | custom-call | tf_op jit(solution)/shard_map/project/pallas_call | solution.py:126
  72.8 14.0 %all_to_all.20 = bf16[4,2,2,144,128]{4,3,2,1,0:T(8,128)(2,1)S(1)} all-to-all(bf16[4,2,2,144,128]{4,3,2,1,0:T(8,128)(2,1)} %project.3), channel_id=1, replica_groups=mesh['sp'=16,'fs'=4,'tp_0'=4,'tp_1'=2] {'tp_0'}, dimensions={0} | all-to-all | bytes 1179648 | tf_op jit(solution)/shard_map/all_to_all | solution.py:365
  86.7 47.6 %all_to_all.21.refs_0_ = bf16[16,144,128]{2,1,0:T(8,128)(2,1)S(1)} all-to-all(bf16[16,144,128]{2,1,0:T(8,128)(2,1)S(1)} %bitcast.26), channel_id=1, replica_groups=mesh['sp'=16,'fs'=4,'tp_0'=4,'tp_1'=2] {'sp'}, dimensions={0} | all-to-all | bytes 1179648 | tf_op jit(solution)/shard_map/all_to_all | solution.py:366
  134.4 2.5 collective-permute-start.14
  136.8 4.6 %collective-permute-start.15 = (bf16[16,144,128]{2,1,0:T(8,128)(2,1)S(1)}, bf16[16,144,128]{2,1,0:T(8,128)(2,1)S(1)}, u32[]{:S(2)}, u32[]{:S(2)}) collective-permute-start(bf16[16,144,128]{2,1,0:T(8,128)(2,1)S(1)} %all_to_all.21.refs_0_), channel_id=1, source_target_pairs={{0,6},{2,0},{4,2},{6,4},{1,7},{3,1},{5,3},{7,5},{8,14},{10,8},{12,... | collective-permute-start | bytes 1769480 | tf_op jit(solution)/shard_map/ppermute | solution.py:39
  141.5 4.7 %collective-permute-start.20 = (bf16[256,512]{1,0:T(8,128)(2,1)S(1)}, bf16[256,512]{1,0:T(8,128)(2,1)S(1)}, u32[]{:S(2)}, u32[]{:S(2)}) collective-permute-start(bf16[256,512]{1,0:T(8,128)(2,1)S(1)} %pad_maximum_fusion.3), channel_id=1, source_target_pairs={{0,8},{8,16},{16,24},{24,0},{1,9},{9,17},{17,25},{25,1},{2,10},{10... | collective-permute-start | bytes 786440 | tf_op jit(solution)/shard_map/ppermute | solution.py:39
  146.2 1.9 collective-permute-start.21
  148.3 3.7 %collective-permute-done.20 = bf16[256,512]{1,0:T(8,128)(2,1)S(1)} collective-permute-done((bf16[256,512]{1,0:T(8,128)(2,1)S(1)}, bf16[256,512]{1,0:T(8,128)(2,1)S(1)}, u32[]{:S(2)}, u32[]{:S(2)}) %collective-permute-start.20) | collective-permute-done | bytes 262176 | tf_op jit(solution)/shard_map/ppermute | solution.py:39
  152.0 4.4 %collective-permute-start.22 = (bf16[256,512]{1,0:T(8,128)(2,1)S(1)}, bf16[256,512]{1,0:T(8,128)(2,1)S(1)}, u32[]{:S(2)}, u32[]{:S(2)}) collective-permute-start(bf16[256,512]{1,0:T(8,128)(2,1)S(1)} %collective-permute-done.20), channel_id=1, source_target_pairs={{0,8},{8,16},{16,24},{24,0},{1,9},{9,17},{17,25},{25,1},{2,10},{10... | collective-permute-start | bytes 786440 | tf_op jit(solution)/shard_map/ppermute | solution.py:54
  158.4 5.1 %collective-permute-start.17 = (bf16[8,144,128]{2,1,0:T(8,128)(2,1)S(1)}, bf16[8,144,128]{2,1,0:T(8,128)(2,1)S(1)}, u32[]{:S(2)}, u32[]{:S(2)}) collective-permute-start(bf16[8,144,128]{2,1,0:T(8,128)(2,1)S(1)} %slice.52), channel_id=1, source_target_pairs={{0,6},{2,0},{4,2},{6,4},{1,7},{3,1},{5,3},{7,5},{8,14},{10,8},{12,... | collective-permute-start | bytes 884744 | tf_op jit(solution)/shard_map/ppermute | solution.py:44
  163.6 4.9 %project.2 = (bf16[2,1,2,2,64,128]{5,4,3,2,1,0:T(8,128)(2,1)}, bf16[2,1,2,2,64,128]{5,4,3,2,1,0:T(8,128)(2,1)}, bf16[2,1,2,2,64,128]{5,4,3,2,1,0:T(8,128)(2,1)}, bf16[2,1,2,2,64,128]{5,4,3,2,1,0:T(8,128)(2,1)}) custom-call(s32[9]{0:T(128)} %stack.46.p_ref, bf16[2,64,2048]{2,1,0:T(8,128)(2,1)} %refs_0_.3, bf16[2,64,2048]{2,1,0:T(8,128)(2,1)} %copy-done.7, ...), custom_call_target="tpu_custom_call" | custom-call | tf_op jit(solution)/shard_map/project/pallas_call | solution.py:126
  168.5 2.1 collective-permute-start.10
  174.1 3.9 %collective-permute-start.11 = (bf16[2,1,2,2,64,128]{5,4,3,2,1,0:T(8,128)(2,1)S(1)}, bf16[2,1,2,2,64,128]{5,4,3,2,1,0:T(8,128)(2,1)S(1)}, u32[]{:S(2)}, u32[]{:S(2)}) collective-permute-start(bf16[2,1,2,2,64,128]{5,4,3,2,1,0:T(8,128)(2,1)S(1)} %copy-done.25), channel_id=1, source_target_pairs={{0,2},{2,4},{4,6},{6,0},{1,3},{3,5},{5,7},{7,1},{8,10},{10,12},{12... | collective-permute-start | bytes 393224 | tf_op jit(solution)/shard_map/ppermute | solution.py:373
  178.1 2.1 collective-permute-start.12
  180.4 2.7 collective-permute-done.11
  183.2 3.9 %collective-permute-done.12 = bf16[2,1,2,2,64,128]{5,4,3,2,1,0:T(8,128)(2,1)S(1)} collective-permute-done((bf16[2,1,2,2,64,128]{5,4,3,2,1,0:T(8,128)(2,1)S(1)}, bf16[2,1,2,2,64,128]{5,4,3,2,1,0:T(8,128)(2,1)S(1)}, u32[]{:S(2)}, u32[]{:S(2)}) %collective-permute-start.12) | collective-permute-done | bytes 131104 | tf_op jit(solution)/shard_map/ppermute | solution.py:373
  187.1 2.2 collective-permute-start.23
  189.3 4.9 %collective-permute-start.24 = (bf16[4,256,512]{2,1,0:T(8,128)(2,1)S(1)}, bf16[4,256,512]{2,1,0:T(8,128)(2,1)S(1)}, u32[]{:S(2)}, u32[]{:S(2)}) collective-permute-start(bf16[4,256,512]{2,1,0:T(8,128)(2,1)S(1)} %bitcast_dynamic-update-slice_fusion.refs_0_), channel_id=1, source_target_pairs={{0,6},{2,0},{4,2},{6,4},{1,7},{3,1},{5,3},{7,5},{8,14},{10,8},{12,... | collective-permute-start | bytes 3145736 | tf_op jit(solution)/shard_map/ppermute | solution.py:39
  194.9 4.2 %all-to-all-start.2 = ((bf16[16,64,128]{2,1,0:T(8,128)(2,1)}), bf16[16,64,128]{2,1,0:T(8,128)(2,1)}, u32[]{:S(2)}, u32[]{:S(2)}) async-start(bf16[16,64,128]{2,1,0:T(8,128)(2,1)} %bitcast.28), calls=%async_computation.2 | async-start | bytes 524288 | tf_op jit(solution)/shard_map/all_to_all | solution.py:379
  199.1 1.9 collective-permute-start.18
  201.1 2.4 collective-permute-start.13
  203.5 2.1 collective-permute-start.27
  205.6 11.5 %all-to-all-done.2.q_ref = bf16[16,64,128]{2,1,0:T(8,128)(2,1)} async-done(((bf16[16,64,128]{2,1,0:T(8,128)(2,1)}), bf16[16,64,128]{2,1,0:T(8,128)(2,1)}, u32[]{:S(2)}, u32[]{:S(2)}) %all-to-all-start.2) | async-done | bytes 262176 | tf_op jit(solution)/shard_map/all_to_all | solution.py:379
  217.1 10.3 %attend.1 = bf16[16,64,128]{2,1,0:T(8,128)(2,1)} custom-call(s32[9]{0:T(128)} %stack.46.p_ref, bf16[16,64,128]{2,1,0:T(8,128)(2,1)} %all-to-all-done.2.q_ref, bf16[16,144,128]{2,1,0:T(8,128)(2,1)} %copy-done.13, bf16[16,144,128]{2,1,0:T(8,128)(2,1)} %copy-done.5, bf16[16,144,128]{2,1,0:T(8,128)(2,1)} %copy-done.6, bf16[8,144,128]{2,1,0:T(8,128)(2,1)} %copy-done.16, ...), custom_call_target="tpu_custom_call" | custom-call | tf_op jit(solution)/shard_map/attend/pallas_call | solution.py:221
  231.1 2.4 collective-permute-start.29
  233.5 1.9 collective-permute-start.25
  235.5 5.1 %collective-permute-start.26 = (bf16[2,256,512]{2,1,0:T(8,128)(2,1)}, bf16[2,256,512]{2,1,0:T(8,128)(2,1)}, u32[]{:S(2)}, u32[]{:S(2)}) collective-permute-start(bf16[2,256,512]{2,1,0:T(8,128)(2,1)} %slice.43), channel_id=1, source_target_pairs={{0,6},{2,0},{4,2},{6,4},{1,7},{3,1},{5,3},{7,5},{8,14},{10,8},{12,... | collective-permute-start | bytes 1572872 | tf_op jit(solution)/shard_map/ppermute | solution.py:44
  240.6 5.4 %all-to-all-start.3 = ((bf16[16,64,128]{2,1,0:T(8,128)(2,1)}), bf16[16,64,128]{2,1,0:T(8,128)(2,1)S(1)}, u32[]{:S(2)}, u32[]{:S(2)}) async-start(bf16[16,64,128]{2,1,0:T(8,128)(2,1)} %attend.1), calls=%async_computation.3 | async-start | bytes 524288 | tf_op jit(solution)/shard_map/all_to_all | solution.py:403
  246.1 4.7 %collective-permute-done.25.refs_3_ = bf16[2,256,512]{2,1,0:T(8,128)(2,1)} collective-permute-done((bf16[2,256,512]{2,1,0:T(8,128)(2,1)}, bf16[2,256,512]{2,1,0:T(8,128)(2,1)}, u32[]{:S(2)}, u32[]{:S(2)}) %collective-permute-start.25) | collective-permute-done | bytes 524320 | tf_op jit(solution)/shard_map/ppermute | solution.py:44
  252.7 2.4 collective-permute-start.31
  255.2 2.1 pool.1.pool_ref
  257.3 7.0 %all-to-all-done.3 = bf16[16,64,128]{2,1,0:T(8,128)(2,1)S(1)} async-done(((bf16[16,64,128]{2,1,0:T(8,128)(2,1)}), bf16[16,64,128]{2,1,0:T(8,128)(2,1)S(1)}, u32[]{:S(2)}, u32[]{:S(2)}) %all-to-all-start.3) | async-done | bytes 262176 | tf_op jit(solution)/shard_map/all_to_all | solution.py:403
  265.0 6.0 %finish.1 = bf16[2,64,2048]{2,1,0:T(8,128)(2,1)} custom-call(s32[9]{0:T(128)} %stack.46.p_ref, bf16[4,2,2,64,128]{4,3,2,1,0:T(8,128)(2,1)} %pool.1.pool_ref, bf16[4,2,2,64,128]{4,3,2,1,0:T(8,128)(2,1)} %bitcast.27, bf16[4,256,512]{2,1,0:T(8,128)(2,1)} %copy-done.4, bf16[4,256,512]{2,1,0:T(8,128)(2,1)} %copy-done.11, bf16[4,256,512]{2,1,0:T(8,128)(2,1)} %copy-done.12, ...), custom_call_target="tpu_custom_call" | custom-call | tf_op jit(solution)/shard_map/finish/pallas_call | solution.py:300
  (108 shorter events, 23.0 us)
Async XLA Ops:
  2.8 39.3 %copy-start.3 = (bf16[528,512]{1,0:T(8,128)(2,1)}, bf16[528,512]{1,0:T(8,128)(2,1)S(1)}, u32[]{:S(2)}) copy-start(bf16[528,512]{1,0:T(8,128)(2,1)S(1)} %pad_maximum_fusion.2.refs_5_) | copy-start | bytes 1622020
  2.8 15.9 %collective-permute-start.4 = (bf16[528,512]{1,0:T(8,128)(2,1)S(1)}, bf16[528,512]{1,0:T(8,128)(2,1)S(1)}, u32[]{:S(2)}, u32[]{:S(2)}) collective-permute-start(bf16[528,512]{1,0:T(8,128)(2,1)S(1)} %pad_maximum_fusion.2.refs_5_), channel_id=1, source_target_pairs={{0,8},{8,16},{16,24},{24,0},{1,9},{9,17},{17,25},{25,1},{2,10},{10... | collective-permute-start | bytes 1622024 | tf_op jit(solution)/shard_map/ppermute | solution.py:39
  6.0 16.1 %collective-permute-start.5 = (bf16[528,512]{1,0:T(8,128)(2,1)S(1)}, bf16[528,512]{1,0:T(8,128)(2,1)S(1)}, u32[]{:S(2)}, u32[]{:S(2)}) collective-permute-start(bf16[528,512]{1,0:T(8,128)(2,1)S(1)} %pad_maximum_fusion.2.refs_5_), channel_id=1, source_target_pairs={{0,24},{8,0},{16,8},{24,16},{1,25},{9,1},{17,9},{25,17},{2,26},{10... | collective-permute-start | bytes 1622024 | tf_op jit(solution)/shard_map/ppermute | solution.py:39
  18.7 14.4 %copy-start = (bf16[528,512]{1,0:T(8,128)(2,1)}, bf16[528,512]{1,0:T(8,128)(2,1)S(1)}, u32[]{:S(2)}) copy-start(bf16[528,512]{1,0:T(8,128)(2,1)S(1)} %collective-permute-done.4.refs_6_) | copy-start | bytes 1622020
  18.8 16.3 %copy-start.14 = (bf16[2,64,2048]{2,1,0:T(8,128)(2,1)S(1)}, bf16[2,64,2048]{2,1,0:T(8,128)(2,1)}, u32[]{:S(2)}) copy-start(bf16[2,64,2048]{2,1,0:T(8,128)(2,1)} %refs_0_.3) | copy-start | bytes 1572868
  18.8 9.4 %collective-permute-start.6 = (bf16[264,512]{1,0:T(8,128)(2,1)S(1)}, bf16[264,512]{1,0:T(8,128)(2,1)S(1)}, u32[]{:S(2)}, u32[]{:S(2)}) collective-permute-start(bf16[264,512]{1,0:T(8,128)(2,1)S(1)} %slice.46), channel_id=1, source_target_pairs={{0,8},{8,16},{16,24},{24,0},{1,9},{9,17},{17,25},{25,1},{2,10},{10... | collective-permute-start | bytes 811016 | tf_op jit(solution)/shard_map/ppermute | solution.py:44
  22.1 9.0 %collective-permute-start.7 = (bf16[264,512]{1,0:T(8,128)(2,1)S(1)}, bf16[264,512]{1,0:T(8,128)(2,1)S(1)}, u32[]{:S(2)}, u32[]{:S(2)}) collective-permute-start(bf16[264,512]{1,0:T(8,128)(2,1)S(1)} %slice.47), channel_id=1, source_target_pairs={{0,24},{8,0},{16,8},{24,16},{1,25},{9,1},{17,9},{25,17},{2,26},{10... | collective-permute-start | bytes 811016 | tf_op jit(solution)/shard_map/ppermute | solution.py:44
  28.2 25.1 %copy-start.9 = (bf16[264,512]{1,0:T(8,128)(2,1)}, bf16[264,512]{1,0:T(8,128)(2,1)S(1)}, u32[]{:S(2)}) copy-start(bf16[264,512]{1,0:T(8,128)(2,1)S(1)} %collective-permute-done.6.refs_8_) | copy-start | bytes 811012
  33.1 33.4 %collective-permute-start.9 = (bf16[1584,512]{1,0:T(8,128)(2,1)}, bf16[1584,512]{1,0:T(8,128)(2,1)S(1)}, u32[]{:S(2)}, u32[]{:S(2)}) collective-permute-start(bf16[1584,512]{1,0:T(8,128)(2,1)} %pad_maximum_fusion.1), channel_id=1, source_target_pairs={{0,1},{1,0},{2,3},{3,2},{4,5},{5,4},{6,7},{7,6},{8,9},{9,8},{10,11... | collective-permute-start | bytes 4866056 | tf_op jit(solution)/shard_map/ppermute | solution.py:31
  35.1 17.4 %collective-permute-start = (bf16[2,64,2048]{2,1,0:T(8,128)(2,1)S(1)}, bf16[2,64,2048]{2,1,0:T(8,128)(2,1)S(1)}, u32[]{:S(2)}, u32[]{:S(2)}) collective-permute-start(bf16[2,64,2048]{2,1,0:T(8,128)(2,1)S(1)} %copy-done.14), channel_id=1, source_target_pairs={{0,2},{2,4},{4,6},{6,0},{1,3},{3,5},{5,7},{7,1},{8,10},{10,12},{12... | collective-permute-start | bytes 1572872 | tf_op jit(solution)/shard_map/ppermute | solution.py:39
  38.5 17.0 %collective-permute-start.1 = (bf16[2,64,2048]{2,1,0:T(8,128)(2,1)S(1)}, bf16[2,64,2048]{2,1,0:T(8,128)(2,1)S(1)}, u32[]{:S(2)}, u32[]{:S(2)}) collective-permute-start(bf16[2,64,2048]{2,1,0:T(8,128)(2,1)S(1)} %copy-done.14), channel_id=1, source_target_pairs={{0,6},{2,0},{4,2},{6,4},{1,7},{3,1},{5,3},{7,5},{8,14},{10,8},{12,... | collective-permute-start | bytes 1572872 | tf_op jit(solution)/shard_map/ppermute | solution.py:39
  42.1 19.7 %collective-permute-start.8 = (bf16[528,512]{1,0:T(8,128)(2,1)S(1)}, bf16[528,512]{1,0:T(8,128)(2,1)}, u32[]{:S(2)}, u32[]{:S(2)}) collective-permute-start(bf16[528,512]{1,0:T(8,128)(2,1)S(1)} %pad_maximum_fusion.2.refs_5_), channel_id=1, source_target_pairs={{0,1},{1,0},{2,3},{3,2},{4,5},{5,4},{6,7},{7,6},{8,9},{9,8},{10,11... | collective-permute-start | bytes 1622024 | tf_op jit(solution)/shard_map/ppermute | solution.py:31
  52.5 14.0 %copy-start.7 = (bf16[2,64,2048]{2,1,0:T(8,128)(2,1)}, bf16[2,64,2048]{2,1,0:T(8,128)(2,1)S(1)}, u32[]{:S(2)}) copy-start(bf16[2,64,2048]{2,1,0:T(8,128)(2,1)S(1)} %collective-permute-done.refs_1_) | copy-start | bytes 1572868
  53.3 11.2 %collective-permute-start.2 = (bf16[1,64,2048]{2,1,0:T(8,128)(2,1)}, bf16[1,64,2048]{2,1,0:T(8,128)(2,1)S(1)}, u32[]{:S(2)}, u32[]{:S(2)}) collective-permute-start(bf16[1,64,2048]{2,1,0:T(8,128)(2,1)} %slice.44), channel_id=1, source_target_pairs={{0,2},{2,4},{4,6},{6,0},{1,3},{3,5},{5,7},{7,1},{8,10},{10,12},{12... | collective-permute-start | bytes 786440 | tf_op jit(solution)/shard_map/ppermute | solution.py:44
  56.3 10.2 %collective-permute-start.3 = (bf16[1,64,2048]{2,1,0:T(8,128)(2,1)}, bf16[1,64,2048]{2,1,0:T(8,128)(2,1)}, u32[]{:S(2)}, u32[]{:S(2)}) collective-permute-start(bf16[1,64,2048]{2,1,0:T(8,128)(2,1)} %slice.45), channel_id=1, source_target_pairs={{0,6},{2,0},{4,2},{6,4},{1,7},{3,1},{5,3},{7,5},{8,14},{10,8},{12,... | collective-permute-start | bytes 786440 | tf_op jit(solution)/shard_map/ppermute | solution.py:44
  72.8 68.7 %copy-start.21 = (bf16[128,512]{1,0:T(8,128)(2,1)S(1)}, bf16[128,512]{1,0:T(8,128)(2,1)}, u32[]{:S(2)}) copy-start(bf16[128,512]{1,0:T(8,128)(2,1)} %param.21) | copy-start | bytes 393220
  72.8 68.7 %copy-start.22 = (bf16[128,512]{1,0:T(8,128)(2,1)S(1)}, bf16[128,512]{1,0:T(8,128)(2,1)}, u32[]{:S(2)}) copy-start(bf16[128,512]{1,0:T(8,128)(2,1)} %param.20) | copy-start | bytes 393220
  134.4 29.2 %copy-start.13 = (bf16[16,144,128]{2,1,0:T(8,128)(2,1)}, bf16[16,144,128]{2,1,0:T(8,128)(2,1)S(1)}, u32[]{:S(2)}) copy-start(bf16[16,144,128]{2,1,0:T(8,128)(2,1)S(1)} %all_to_all.21.refs_0_) | copy-start | bytes 1769476
  134.4 22.0 %collective-permute-start.14 = (bf16[16,144,128]{2,1,0:T(8,128)(2,1)S(1)}, bf16[16,144,128]{2,1,0:T(8,128)(2,1)S(1)}, u32[]{:S(2)}, u32[]{:S(2)}) collective-permute-start(bf16[16,144,128]{2,1,0:T(8,128)(2,1)S(1)} %all_to_all.21.refs_0_), channel_id=1, source_target_pairs={{0,2},{2,4},{4,6},{6,0},{1,3},{3,5},{5,7},{7,1},{8,10},{10,12},{12... | collective-permute-start | bytes 1769480 | tf_op jit(solution)/shard_map/ppermute | solution.py:39
  136.8 21.5 %collective-permute-start.15 = (bf16[16,144,128]{2,1,0:T(8,128)(2,1)S(1)}, bf16[16,144,128]{2,1,0:T(8,128)(2,1)S(1)}, u32[]{:S(2)}, u32[]{:S(2)}) collective-permute-start(bf16[16,144,128]{2,1,0:T(8,128)(2,1)S(1)} %all_to_all.21.refs_0_), channel_id=1, source_target_pairs={{0,6},{2,0},{4,2},{6,4},{1,7},{3,1},{5,3},{7,5},{8,14},{10,8},{12,... | collective-permute-start | bytes 1769480 | tf_op jit(solution)/shard_map/ppermute | solution.py:39
  141.5 10.5 %collective-permute-start.20 = (bf16[256,512]{1,0:T(8,128)(2,1)S(1)}, bf16[256,512]{1,0:T(8,128)(2,1)S(1)}, u32[]{:S(2)}, u32[]{:S(2)}) collective-permute-start(bf16[256,512]{1,0:T(8,128)(2,1)S(1)} %pad_maximum_fusion.3), channel_id=1, source_target_pairs={{0,8},{8,16},{16,24},{24,0},{1,9},{9,17},{17,25},{25,1},{2,10},{10... | collective-permute-start | bytes 786440 | tf_op jit(solution)/shard_map/ppermute | solution.py:39
  146.2 17.4 %collective-permute-start.21 = (bf16[256,512]{1,0:T(8,128)(2,1)S(1)}, bf16[256,512]{1,0:T(8,128)(2,1)S(1)}, u32[]{:S(2)}, u32[]{:S(2)}) collective-permute-start(bf16[256,512]{1,0:T(8,128)(2,1)S(1)} %pad_maximum_fusion.3), channel_id=1, source_target_pairs={{0,24},{8,0},{16,8},{24,16},{1,25},{9,1},{17,9},{25,17},{2,26},{10... | collective-permute-start | bytes 786440 | tf_op jit(solution)/shard_map/ppermute | solution.py:39
  152.0 22.1 %collective-permute-start.22 = (bf16[256,512]{1,0:T(8,128)(2,1)S(1)}, bf16[256,512]{1,0:T(8,128)(2,1)S(1)}, u32[]{:S(2)}, u32[]{:S(2)}) collective-permute-start(bf16[256,512]{1,0:T(8,128)(2,1)S(1)} %collective-permute-done.20), channel_id=1, source_target_pairs={{0,8},{8,16},{16,24},{24,0},{1,9},{9,17},{17,25},{25,1},{2,10},{10... | collective-permute-start | bytes 786440 | tf_op jit(solution)/shard_map/ppermute | solution.py:54
  156.4 14.3 %copy-start.5 = (bf16[16,144,128]{2,1,0:T(8,128)(2,1)}, bf16[16,144,128]{2,1,0:T(8,128)(2,1)S(1)}, u32[]{:S(2)}) copy-start(bf16[16,144,128]{2,1,0:T(8,128)(2,1)S(1)} %collective-permute-done.14.refs_1_) | copy-start | bytes 1769476
  156.4 14.2 %collective-permute-start.16 = (bf16[8,144,128]{2,1,0:T(8,128)(2,1)S(1)}, bf16[8,144,128]{2,1,0:T(8,128)(2,1)S(1)}, u32[]{:S(2)}, u32[]{:S(2)}) collective-permute-start(bf16[8,144,128]{2,1,0:T(8,128)(2,1)S(1)} %slice.51), channel_id=1, source_target_pairs={{0,2},{2,4},{4,6},{6,0},{1,3},{3,5},{5,7},{7,1},{8,10},{10,12},{12... | collective-permute-start | bytes 884744 | tf_op jit(solution)/shard_map/ppermute | solution.py:44
  158.4 12.2 %collective-permute-start.17 = (bf16[8,144,128]{2,1,0:T(8,128)(2,1)S(1)}, bf16[8,144,128]{2,1,0:T(8,128)(2,1)S(1)}, u32[]{:S(2)}, u32[]{:S(2)}) collective-permute-start(bf16[8,144,128]{2,1,0:T(8,128)(2,1)S(1)} %slice.52), channel_id=1, source_target_pairs={{0,6},{2,0},{4,2},{6,4},{1,7},{3,1},{5,3},{7,5},{8,14},{10,8},{12,... | collective-permute-start | bytes 884744 | tf_op jit(solution)/shard_map/ppermute | solution.py:44
  168.5 11.8 %collective-permute-start.10 = (bf16[2,1,2,2,64,128]{5,4,3,2,1,0:T(8,128)(2,1)}, bf16[2,1,2,2,64,128]{5,4,3,2,1,0:T(8,128)(2,1)S(1)}, u32[]{:S(2)}, u32[]{:S(2)}) collective-permute-start(bf16[2,1,2,2,64,128]{5,4,3,2,1,0:T(8,128)(2,1)} %get-tuple-element.15), channel_id=1, source_target_pairs={{0,6},{2,0},{4,2},{6,4},{1,7},{3,1},{5,3},{7,5},{8,14},{10,8},{12,... | collective-permute-start | bytes 393224 | tf_op jit(solution)/shard_map/ppermute | solution.py:373
  172.1 45.0 %collective-permute-start.19 = (bf16[48,144,128]{2,1,0:T(8,128)(2,1)}, bf16[48,144,128]{2,1,0:T(8,128)(2,1)}, u32[]{:S(2)}, u32[]{:S(2)}) collective-permute-start(bf16[48,144,128]{2,1,0:T(8,128)(2,1)} %pad_maximum_fusion), channel_id=1, source_target_pairs={{0,1},{1,0},{2,3},{3,2},{4,5},{5,4},{6,7},{7,6},{8,9},{9,8},{10,11... | collective-permute-start | bytes 5308424 | tf_op jit(solution)/shard_map/ppermute | solution.py:31
  174.1 53.3 %copy-start.4 = (bf16[4,256,512]{2,1,0:T(8,128)(2,1)}, bf16[4,256,512]{2,1,0:T(8,128)(2,1)S(1)}, u32[]{:S(2)}) copy-start(bf16[4,256,512]{2,1,0:T(8,128)(2,1)S(1)} %bitcast_dynamic-update-slice_fusion.refs_0_) | copy-start | bytes 3145732
  174.1 9.0 %collective-permute-start.11 = (bf16[2,1,2,2,64,128]{5,4,3,2,1,0:T(8,128)(2,1)S(1)}, bf16[2,1,2,2,64,128]{5,4,3,2,1,0:T(8,128)(2,1)S(1)}, u32[]{:S(2)}, u32[]{:S(2)}) collective-permute-start(bf16[2,1,2,2,64,128]{5,4,3,2,1,0:T(8,128)(2,1)S(1)} %copy-done.25), channel_id=1, source_target_pairs={{0,2},{2,4},{4,6},{6,0},{1,3},{3,5},{5,7},{7,1},{8,10},{10,12},{12... | collective-permute-start | bytes 393224 | tf_op jit(solution)/shard_map/ppermute | solution.py:373
  178.1 9.0 %collective-permute-start.12 = (bf16[2,1,2,2,64,128]{5,4,3,2,1,0:T(8,128)(2,1)S(1)}, bf16[2,1,2,2,64,128]{5,4,3,2,1,0:T(8,128)(2,1)S(1)}, u32[]{:S(2)}, u32[]{:S(2)}) collective-permute-start(bf16[2,1,2,2,64,128]{5,4,3,2,1,0:T(8,128)(2,1)S(1)} %copy-done.24), channel_id=1, source_target_pairs={{0,4},{2,6},{4,0},{6,2},{1,5},{3,7},{5,1},{7,3},{8,12},{10,14},{12... | collective-permute-start | bytes 393224 | tf_op jit(solution)/shard_map/ppermute | solution.py:373
  187.1 40.3 %collective-permute-start.23 = (bf16[4,256,512]{2,1,0:T(8,128)(2,1)S(1)}, bf16[4,256,512]{2,1,0:T(8,128)(2,1)S(1)}, u32[]{:S(2)}, u32[]{:S(2)}) collective-permute-start(bf16[4,256,512]{2,1,0:T(8,128)(2,1)S(1)} %bitcast_dynamic-update-slice_fusion.refs_0_), channel_id=1, source_target_pairs={{0,2},{2,4},{4,6},{6,0},{1,3},{3,5},{5,7},{7,1},{8,10},{10,12},{12... | collective-permute-start | bytes 3145736 | tf_op jit(solution)/shard_map/ppermute | solution.py:39
  189.3 38.1 %collective-permute-start.24 = (bf16[4,256,512]{2,1,0:T(8,128)(2,1)S(1)}, bf16[4,256,512]{2,1,0:T(8,128)(2,1)S(1)}, u32[]{:S(2)}, u32[]{:S(2)}) collective-permute-start(bf16[4,256,512]{2,1,0:T(8,128)(2,1)S(1)} %bitcast_dynamic-update-slice_fusion.refs_0_), channel_id=1, source_target_pairs={{0,6},{2,0},{4,2},{6,4},{1,7},{3,1},{5,3},{7,5},{8,14},{10,8},{12,... | collective-permute-start | bytes 3145736 | tf_op jit(solution)/shard_map/ppermute | solution.py:39
  194.9 32.5 %copy-start.15 = (bf16[4,2,2,64,128]{4,3,2,1,0:T(8,128)(2,1)}, bf16[4,2,2,64,128]{4,3,2,1,0:T(8,128)(2,1)S(1)}, u32[]{:S(2)}) copy-start(bf16[4,2,2,64,128]{4,3,2,1,0:T(8,128)(2,1)S(1)} %get-tuple-element.24.in_ref) | copy-start | bytes 786436
  194.9 22.1 %all-to-all-start.2 = ((bf16[16,64,128]{2,1,0:T(8,128)(2,1)}), bf16[16,64,128]{2,1,0:T(8,128)(2,1)}, u32[]{:S(2)}, u32[]{:S(2)}) async-start(bf16[16,64,128]{2,1,0:T(8,128)(2,1)} %bitcast.28), calls=%async_computation.2 | async-start | bytes 524288 | tf_op jit(solution)/shard_map/all_to_all | solution.py:379
  199.1 4.4 %collective-permute-start.18 = (bf16[16,144,128]{2,1,0:T(8,128)(2,1)}, bf16[16,144,128]{2,1,0:T(8,128)(2,1)}, u32[]{:S(2)}, u32[]{:S(2)}) collective-permute-start(bf16[16,144,128]{2,1,0:T(8,128)(2,1)} %copy-done.13), channel_id=1, source_target_pairs={{0,1},{1,0},{2,3},{3,2},{4,5},{5,4},{6,7},{7,6},{8,9},{9,8},{10,11... | collective-permute-start | bytes 1769480 | tf_op jit(solution)/shard_map/ppermute | solution.py:31
  201.1 34.4 %collective-permute-start.13 = (bf16[4,2,2,16,128]{4,3,2,1,0:T(8,128)(2,1)S(1)}, bf16[4,2,2,16,128]{4,3,2,1,0:T(8,128)(2,1)S(1)}, u32[]{:S(2)}, u32[]{:S(2)}) collective-permute-start(bf16[4,2,2,16,128]{4,3,2,1,0:T(8,128)(2,1)S(1)} %slice.49), channel_id=1, source_target_pairs={{0,1},{1,2},{2,3},{3,4},{4,5},{5,6},{6,7},{7,32},{32,33},{33,34},{... | collective-permute-start | bytes 196616 | tf_op jit(solution)/shard_map/ppermute | solution.py:382
  203.5 53.8 %collective-permute-start.27 = (bf16[4,256,512]{2,1,0:T(8,128)(2,1)S(1)}, bf16[4,256,512]{2,1,0:T(8,128)(2,1)}, u32[]{:S(2)}, u32[]{:S(2)}) collective-permute-start(bf16[4,256,512]{2,1,0:T(8,128)(2,1)S(1)} %bitcast_dynamic-update-slice_fusion.refs_0_), channel_id=1, source_target_pairs={{0,1},{1,0},{2,3},{3,2},{4,5},{5,4},{6,7},{7,6},{8,9},{9,8},{10,11... | collective-permute-start | bytes 3145736 | tf_op jit(solution)/shard_map/ppermute | solution.py:31
  227.4 36.9 %copy-start.11 = (bf16[4,256,512]{2,1,0:T(8,128)(2,1)}, bf16[4,256,512]{2,1,0:T(8,128)(2,1)S(1)}, u32[]{:S(2)}) copy-start(bf16[4,256,512]{2,1,0:T(8,128)(2,1)S(1)} %collective-permute-done.23.refs_1_) | copy-start | bytes 3145732
  227.4 36.9 %copy-start.12 = (bf16[4,256,512]{2,1,0:T(8,128)(2,1)}, bf16[4,256,512]{2,1,0:T(8,128)(2,1)S(1)}, u32[]{:S(2)}) copy-start(bf16[4,256,512]{2,1,0:T(8,128)(2,1)S(1)} %collective-permute-done.24.refs_2_) | copy-start | bytes 3145732
  228.4 35.9 %collective-permute-start.28 = (bf16[4,256,512]{2,1,0:T(8,128)(2,1)S(1)}, bf16[4,256,512]{2,1,0:T(8,128)(2,1)}, u32[]{:S(2)}, u32[]{:S(2)}) collective-permute-start(bf16[4,256,512]{2,1,0:T(8,128)(2,1)S(1)} %collective-permute-done.23.refs_1_), channel_id=1, source_target_pairs={{0,1},{1,0},{2,3},{3,2},{4,5},{5,4},{6,7},{7,6},{8,9},{9,8},{10,11... | collective-permute-start | bytes 3145736 | tf_op jit(solution)/shard_map/ppermute | solution.py:31
  231.1 33.2 %collective-permute-start.29 = (bf16[4,256,512]{2,1,0:T(8,128)(2,1)S(1)}, bf16[4,256,512]{2,1,0:T(8,128)(2,1)}, u32[]{:S(2)}, u32[]{:S(2)}) collective-permute-start(bf16[4,256,512]{2,1,0:T(8,128)(2,1)S(1)} %collective-permute-done.24.refs_2_), channel_id=1, source_target_pairs={{0,1},{1,0},{2,3},{3,2},{4,5},{5,4},{6,7},{7,6},{8,9},{9,8},{10,11... | collective-permute-start | bytes 3145736 | tf_op jit(solution)/shard_map/ppermute | solution.py:31
  233.5 17.3 %collective-permute-start.25 = (bf16[2,256,512]{2,1,0:T(8,128)(2,1)}, bf16[2,256,512]{2,1,0:T(8,128)(2,1)}, u32[]{:S(2)}, u32[]{:S(2)}) collective-permute-start(bf16[2,256,512]{2,1,0:T(8,128)(2,1)} %slice.42), channel_id=1, source_target_pairs={{0,2},{2,4},{4,6},{6,0},{1,3},{3,5},{5,7},{7,1},{8,10},{10,12},{12... | collective-permute-start | bytes 1572872 | tf_op jit(solution)/shard_map/ppermute | solution.py:44
  235.5 19.7 %copy-start.23 = (bf16[4,2,2,16,128]{4,3,2,1,0:T(8,128)(2,1)}, bf16[4,2,2,16,128]{4,3,2,1,0:T(8,128)(2,1)S(1)}, u32[]{:S(2)}) copy-start(bf16[4,2,2,16,128]{4,3,2,1,0:T(8,128)(2,1)S(1)} %collective-permute-done.13.edge_ref) | copy-start | bytes 196612
  235.5 17.2 %collective-permute-start.26 = (bf16[2,256,512]{2,1,0:T(8,128)(2,1)}, bf16[2,256,512]{2,1,0:T(8,128)(2,1)}, u32[]{:S(2)}, u32[]{:S(2)}) collective-permute-start(bf16[2,256,512]{2,1,0:T(8,128)(2,1)} %slice.43), channel_id=1, source_target_pairs={{0,6},{2,0},{4,2},{6,4},{1,7},{3,1},{5,3},{7,5},{8,14},{10,8},{12,... | collective-permute-start | bytes 1572872 | tf_op jit(solution)/shard_map/ppermute | solution.py:44
  240.6 23.6 %all-to-all-start.3 = ((bf16[16,64,128]{2,1,0:T(8,128)(2,1)}), bf16[16,64,128]{2,1,0:T(8,128)(2,1)S(1)}, u32[]{:S(2)}, u32[]{:S(2)}) async-start(bf16[16,64,128]{2,1,0:T(8,128)(2,1)} %attend.1), calls=%async_computation.3 | async-start | bytes 524288 | tf_op jit(solution)/shard_map/all_to_all | solution.py:403
  250.8 13.5 %collective-permute-start.30 = (bf16[2,256,512]{2,1,0:T(8,128)(2,1)}, bf16[2,256,512]{2,1,0:T(8,128)(2,1)}, u32[]{:S(2)}, u32[]{:S(2)}) collective-permute-start(bf16[2,256,512]{2,1,0:T(8,128)(2,1)} %collective-permute-done.25.refs_3_), channel_id=1, source_target_pairs={{0,1},{1,0},{2,3},{3,2},{4,5},{5,4},{6,7},{7,6},{8,9},{9,8},{10,11... | collective-permute-start | bytes 1572872 | tf_op jit(solution)/shard_map/ppermute | solution.py:31
  252.7 11.6 %collective-permute-start.31 = (bf16[2,256,512]{2,1,0:T(8,128)(2,1)}, bf16[2,256,512]{2,1,0:T(8,128)(2,1)}, u32[]{:S(2)}, u32[]{:S(2)}) collective-permute-start(bf16[2,256,512]{2,1,0:T(8,128)(2,1)} %collective-permute-done.26.refs_4_), channel_id=1, source_target_pairs={{0,1},{1,0},{2,3},{3,2},{4,5},{5,4},{6,7},{7,6},{8,9},{9,8},{10,11... | collective-permute-start | bytes 1572872 | tf_op jit(solution)/shard_map/ppermute | solution.py:31
  (12 other events, 73.0 us)
